TPU v7x, 512 devices: a whole 4x4x16 slice. The times are simulated.
512 devices in a mesh: sp: 32 (over z, core), tp: 16 (over y, x).
Axes of the slice: x: 4, y: 4, z: 16, core: 2. Of those that a mesh axis runs over, the one named last changes fastest.
Arguments:
- layer_input: bfloat16 [8192, 2048], P('sp', 'tp'), may hold values from -6 to 6
- doc_ids: int32 [8192], P('sp'), may hold values from 0 to 7, never falling along the last dimension, each value on 1 to 1536 neighbouring positions
- routes: int32 [8192, 2], P('sp'), may hold values from 0 to 31, all different within a row; in each aligned block of 256 rows (0 to 255, 256 to 511, ...) at most 22 rows name the same one
- route_weight: float32 [8192, 2], P('sp'), may hold values from 0.2 to 2
- pool_weight: bfloat16 [4, 512, 512], replicated, may hold values from -0.25 to 0.25
- pool_scale: float32 [2048], replicated, may hold values from 0.1 to 1.9
- norm1_gain: float32 [2048], replicated, may hold values from 0.3 to 3
- norm1_bias: float32 [2048], replicated, may hold values from -3 to 3
- expert_gate: bfloat16 [32, 2048, 2048], P('sp', None, 'tp'), may hold values from -0.125 to 0.125
- expert_up: bfloat16 [32, 2048, 2048], P('sp', None, 'tp'), may hold values from -0.125 to 0.125
- expert_down: bfloat16 [32, 2048, 2048], P('sp', 'tp'), may hold values from -0.125 to 0.125
- shared_gate: bfloat16 [2048, 1024], P(None, 'tp'), may hold values from -0.125 to 0.125
- shared_up: bfloat16 [2048, 1024], P(None, 'tp'), may hold values from -0.125 to 0.125
- shared_down: bfloat16 [1024, 2048], P('tp'), may hold values from -0.1875 to 0.1875
- norm2_gain: float32 [2048], P('tp'), may hold values from 0.1 to 1.9
- norm2_bias: float32 [2048], P('tp'), may hold values from -3 to 3
Outputs:
- settled: bfloat16 [8192, 2048], P('sp', 'tp')
Inputs may be any that keep to these rules, and one draw needn't show every extreme that they name: `routes`: in each aligned block of 256 rows no expert is named by more than 22 picks, a bound that some block reaches. `doc_ids`: never falling along the positions; each document spans 1 to 1536 positions.
All inputs are finite; a program needn't handle non-finite values.
Results may differ from a plain program's by a relative error of at most 0.013.
Values may be sent and summed in bfloat16 or wider, within the bound.
No kernel may reach another device: no remote copies, remote signals or barrier semaphores. Data moves between devices by JAX's collectives and lax.ppermute only.
A program may use at most 64 MiB of HBM per device.

v0:
```python
import jax
import jax.numpy as jnp
from jax import lax
from jax.experimental import pallas as pl
from jax.experimental.pallas import tpu as pltpu
from jax.sharding import Mesh
from jax.sharding import PartitionSpec as P


RESIDUAL_SCALE = 2.0**0.5
NORM_EPS = 1e-05
HALO = 16
F32 = jnp.float32
BF16 = jnp.bfloat16
VMEM = pl.BlockSpec(memory_space=pltpu.VMEM)
HBM = pl.BlockSpec(memory_space=pltpu.HBM)

TOKENS_HERE = 256
EXPERTS = 32
LANES = 128
QUARTER = 512
MODEL = 2048
SLOTS_SENT = 8
SLOTS_USED = 6
ROUTED_ROWS = EXPERTS * SLOTS_USED
SHARED_ROWS = 128
UP_AT = 2048
DOWN_AT = 4096
PACKED = 6144
SHARED_UNITS = 64


def iota(shape, dim):
    return lax.broadcasted_iota(jnp.int32, shape, dim)


def side(parts):
    return jnp.concatenate(parts, axis=1)


def four(a):
    return jnp.concatenate([a, a, a, a], axis=1)


def as_column(row):
    return jnp.broadcast_to(row, (LANES, row.shape[1])).T


def chosen(mask):
    return mask.astype(F32).astype(BF16)


def row_stats(values):
    lane = iota((values.shape[0], LANES), 1)
    total = jnp.sum(values, axis=1, keepdims=True)
    squares = jnp.sum(values * values, axis=1, keepdims=True)
    return jnp.where(lane == 0, total, jnp.where(lane == 1, squares, 0.0)).T


def mean_and_scale(total):
    mean = total[0:1] / MODEL
    var = total[1:2] / MODEL - mean * mean
    return as_column(mean), as_column(lax.rsqrt(var + NORM_EPS))


def ranks_of(routes):
    expert = iota((EXPERTS, TOKENS_HERE), 0)
    picks = [routes[k : k + 1] == expert for k in range(2)]
    named = chosen(picks[0] | picks[1])
    earlier = chosen(iota((TOKENS_HERE, TOKENS_HERE), 0) < iota((TOKENS_HERE, TOKENS_HERE), 1))
    counts = jnp.dot(named, earlier, preferred_element_type=F32)
    return [
        jnp.sum(jnp.where(p, counts, 0.0), axis=0, keepdims=True).astype(jnp.int32) for p in picks
    ]


def pack_body(gate, up, down, sgate, sup, sdown, out, shared_out, buf, shared_buf, sems):
    def moves(i):
        here = pl.ds(i * UP_AT, UP_AT)
        return pltpu.make_async_copy((gate, up)[i], buf.at[here], sems.at[i])

    def sends(i):
        here = pl.ds(i * UP_AT, UP_AT)
        return pltpu.make_async_copy(buf.at[here], out.at[here], sems.at[2 + i])

    moves(0).start()
    moves(1).start()
    for b in range(16):
        at = DOWN_AT + b * LANES
        buf[at : at + LANES, :] = down[:, b * LANES : (b + 1) * LANES]
    sends(2).start()
    for i, part in enumerate((sgate, sup, sdown)):
        shared_buf[i * SHARED_UNITS : (i + 1) * SHARED_UNITS, :] = part[...]
    last = pltpu.make_async_copy(shared_buf, shared_out, sems.at[5])
    last.start()
    for i in range(2):
        moves(i).wait()
        sends(i).start()
    for i in range(3):
        sends(i).wait()
    last.wait()


def mixer_body(at, near, halo, docs, weight, scale, first_out, stats_out):
    group = at[0]
    own = side([near[i] for i in range(4)]).astype(F32)
    head = side([halo[i] for i in range(4)]).astype(F32)
    ext = jnp.concatenate([head, own], axis=0)
    marks = jnp.concatenate(
        [halo[4].astype(F32), as_column((docs[...] + 1).astype(F32))], axis=0
    )
    running = ext
    members = jnp.ones(marks.shape, F32)
    for step in range(4):
        by = 1 << step
        on = (group >= step).astype(F32)
        inside = jnp.where(pltpu.roll(marks, by, 0) == marks, on, 0.0)
        running = running + four(inside) * pltpu.roll(running, by, 0)
        members = members + inside * pltpu.roll(members, by, 0)
    mixed = (running / four(members) - ext)[HALO:].astype(BF16)
    projected = jnp.dot(mixed, weight[0], preferred_element_type=F32)
    first = RESIDUAL_SCALE * own + projected * scale[...]
    first_out[...] = first
    stats = row_stats(first)[0:8]
    for i in range(4):
        stats_out[i] = stats


def dispatch_body(at, first, stats, gain, bias, routes, send, normed_out, own):
    x = at[1]
    mean, inv = mean_and_scale(stats[0] + stats[1] + stats[2] + stats[3])
    normed = ((first[...] - four(mean)) * four(inv) * gain[...] + bias[...]).astype(BF16)
    normed_out[...] = normed
    named = routes[...]
    dests = []
    for k, rank in enumerate(ranks_of(named)):
        slot = named[k : k + 1] * SLOTS_SENT + (rank >> 2)
        dests.append(jnp.where((rank & 3) == x, slot, -1))
    slot = iota((EXPERTS * SLOTS_SENT, TOKENS_HERE), 0)
    pick = chosen((slot == dests[0]) | (slot == dests[1]))
    send[...] = jnp.dot(pick, normed, preferred_element_type=F32).astype(BF16)
    mine = normed[:, 0:LANES]
    for i in range(1, 4):
        mine = jnp.where(x == i, normed[:, i * LANES : (i + 1) * LANES], mine)
    own[...] = mine


def compact_body(rows, normed, out):
    shape = (ROUTED_ROWS, EXPERTS * SLOTS_SENT)
    came = iota(shape, 1)
    within = came & 7
    goes = SLOTS_USED * (came >> 3) + within
    keep = chosen((iota(shape, 0) == goes) & (within < SLOTS_USED))
    packed = jnp.dot(keep, rows[...], preferred_element_type=F32).astype(BF16)
    for i in range(4):
        out[i, 0:ROUTED_ROWS, :] = packed
        out[i, ROUTED_ROWS:, :] = normed[(i & 1) * SHARED_ROWS : ((i & 1) + 1) * SHARED_ROWS, :]


def expert_body(rows, w0, w1, w2, w3, s0, s1, out, xv, wv, sv, sems):
    plan = [(rows, xv), (w0, wv.at[0]), (w1, wv.at[1]), (w2, wv.at[2]), (w3, wv.at[3])]
    plan += [(s0, sv.at[0]), (s1, sv.at[1])]
    copies = [pltpu.make_async_copy(s, d, sems.at[i]) for i, (s, d) in enumerate(plan)]
    for c in copies:
        c.start()
    copies[0].wait()
    tokens = side([xv[i, 0:ROUTED_ROWS, :] for i in range(4)])
    hidden = []
    for c in range(4):
        copies[c + 1].wait()
        both = side([wv[c, 0:UP_AT, :], wv[c, UP_AT:DOWN_AT, :]])
        parts = jnp.dot(tokens, both, preferred_element_type=F32)
        hidden.append((jax.nn.silu(parts[:, :LANES]) * parts[:, LANES:]).astype(BF16))
    hidden = side(hidden)
    copies[5].wait()
    copies[6].wait()
    shared = side([xv[i, ROUTED_ROWS:, :] for i in range(4)])

    def units(i, lanes):
        here = slice(i * SHARED_UNITS, (i + 1) * SHARED_UNITS)
        return jnp.concatenate([sv[0, here, lanes], sv[1, here, lanes]], axis=0)

    contract = (((1,), (1,)), ((), ()))
    every = slice(0, MODEL)
    sg = lax.dot_general(shared, units(0, every), contract, preferred_element_type=F32)
    su = lax.dot_general(shared, units(1, every), contract, preferred_element_type=F32)
    shared_hidden = (jax.nn.silu(sg) * su).astype(BF16)

    def block(c, b):
        at = DOWN_AT + b * LANES
        return wv[c, at : at + LANES, :]

    for b in range(0, 16, 2):
        down = jnp.concatenate([side([block(c, b), block(c, b + 1)]) for c in range(4)], axis=0)
        part = jnp.dot(hidden, down, preferred_element_type=F32).astype(BF16)
        out[b, 0:ROUTED_ROWS, :] = part[:, :LANES]
        out[b + 1, 0:ROUTED_ROWS, :] = part[:, LANES:]
        down = units(2, slice(b * LANES, (b + 2) * LANES))
        part = jnp.dot(shared_hidden, down, preferred_element_type=F32).astype(BF16)
        out[b, ROUTED_ROWS:, :] = part[:, :LANES]
        out[b + 1, ROUTED_ROWS:, :] = part[:, LANES:]


def return_body(parts, send, shared):
    routed = []
    for x in range(4):
        total = parts[x, 0:ROUTED_ROWS, :].astype(F32)
        for y in range(1, 4):
            total = total + parts[4 * y + x, 0:ROUTED_ROWS, :].astype(F32)
        routed.append(total.astype(BF16))
    for half in range(2):
        total = jnp.zeros((SHARED_ROWS, LANES), F32)
        for y in (half, half + 2):
            for x in range(4):
                total = total + parts[4 * y + x, ROUTED_ROWS:, :].astype(F32)
        shared[half * SHARED_ROWS : (half + 1) * SHARED_ROWS, :] = total
    rows = jnp.concatenate(routed, axis=0)
    count = 4 * ROUTED_ROWS
    came = iota((1, count), 1)
    x = (
        (came >= ROUTED_ROWS).astype(jnp.int32)
        + (came >= 2 * ROUTED_ROWS).astype(jnp.int32)
        + (came >= 3 * ROUTED_ROWS).astype(jnp.int32)
    )
    within = came - ROUTED_ROWS * x
    source = (within * 10923) >> 16
    goes = 18 * source + 6 * x + within
    move = chosen(iota((count, count), 0) == goes)
    send[...] = jnp.dot(move, rows, preferred_element_type=F32).astype(BF16)


def combine_body(rows, routes, weight, own, shared, second_out, stats_out):
    named = routes[...]
    scale = weight[...]
    slot = iota((4 * ROUTED_ROWS, TOKENS_HERE), 0)
    taken = jnp.zeros(slot.shape, F32)
    for k, rank in enumerate(ranks_of(named)):
        at = named[k : k + 1] * (4 * SLOTS_USED) + SLOTS_USED * (rank & 3) + (rank >> 2)
        taken = jnp.where(slot == at, scale[k : k + 1], taken)
    high = taken.astype(BF16)
    low = (taken - high.astype(F32)).astype(BF16)
    contract = (((0,), (0,)), ((), ()))
    mix = lax.dot_general(high, rows[...], contract, preferred_element_type=F32)
    mix = mix + lax.dot_general(low, rows[...], contract, preferred_element_type=F32)
    second = RESIDUAL_SCALE * own[...].astype(F32) + mix + shared[...]
    second_out[...] = second
    stats = row_stats(second)[0:2]
    for i in range(16):
        stats_out[i] = stats


def settle_body(second, stats, gain, bias, out):
    total = stats[0]
    for i in range(1, 16):
        total = total + stats[i]
    mean, inv = mean_and_scale(total)
    out[...] = ((second[...] - mean) * inv * gain[...] + bias[...]).astype(BF16)


def struct(shape, dtype):
    return jax.ShapeDtypeStruct(shape, dtype)


def exchange(parts, axes):
    return lax.all_to_all(parts, axes, split_axis=0, concat_axis=0, tiled=True)


def around(shard, by):
    return lax.ppermute(shard, "x", [(i, (i + by) % 4) for i in range(4)])


def kernel(body, **options):
    return pl.pallas_call(body, **options)


def layer(
    layer_input,
    doc_ids,
    routes,
    route_weight,
    pool_weight,
    pool_scale,
    norm1_gain,
    norm1_bias,
    expert_gate,
    expert_up,
    expert_down,
    shared_gate,
    shared_up,
    shared_down,
    norm2_gain,
    norm2_bias,
):
    at = jnp.stack([lax.axis_index("y"), lax.axis_index("x")]).astype(jnp.int32)
    near = exchange(jnp.broadcast_to(layer_input, (4, *layer_input.shape)), "x")
    packed, shared_packed = kernel(
        pack_body,
        out_shape=[struct((PACKED, LANES), BF16), struct((3 * SHARED_UNITS, MODEL), BF16)],
        in_specs=[HBM, HBM, VMEM, VMEM, VMEM, VMEM],
        out_specs=[HBM, HBM],
        scratch_shapes=[
            pltpu.VMEM((PACKED, LANES), BF16),
            pltpu.VMEM((3 * SHARED_UNITS, MODEL), BF16),
            pltpu.SemaphoreType.DMA((6,)),
        ],
        cost_estimate=pl.CostEstimate(
            flops=10_000_000, bytes_accessed=4 * PACKED * LANES, transcendentals=0
        ),
    )(expert_gate[0], expert_up[0], expert_down[0], shared_gate.T, shared_up.T, shared_down)
    packed, shared_packed, near = lax.optimization_barrier((packed, shared_packed, near))
    marks = jnp.broadcast_to((doc_ids[-HALO:] + 1).astype(BF16)[:, None], (HALO, LANES))
    tail = jnp.concatenate([near[:, -HALO:, :], marks[None]], axis=0)
    following = [(i, i + 1) for i in range(lax.axis_size("sp") - 1)]
    halo = lax.ppermute(tail, "sp", following)
    from_left = around(packed, 1)
    from_right = around(packed, -1)
    first, stats = kernel(
        mixer_body,
        grid_spec=pltpu.PrefetchScalarGridSpec(
            num_scalar_prefetch=1,
            grid=(1,),
            in_specs=[
                pl.BlockSpec((4, TOKENS_HERE, LANES), lambda i, w: (0, 0, 0)),
                pl.BlockSpec((5, HALO, LANES), lambda i, w: (0, 0, 0)),
                pl.BlockSpec((1, TOKENS_HERE), lambda i, w: (0, 0)),
                pl.BlockSpec((1, QUARTER, QUARTER), lambda i, w: (w[0], 0, 0)),
                pl.BlockSpec((1, QUARTER), lambda i, w: (0, w[0])),
            ],
            out_specs=[
                pl.BlockSpec((TOKENS_HERE, QUARTER), lambda i, w: (0, 0)),
                pl.BlockSpec((4, 8, TOKENS_HERE), lambda i, w: (0, 0, 0)),
            ],
        ),
        out_shape=[
            struct((TOKENS_HERE, QUARTER), F32),
            struct((4, 8, TOKENS_HERE), F32),
        ],
    )(at, near, halo, doc_ids[None], pool_weight, pool_scale[None])
    later, first = lax.optimization_barrier((packed, first))
    from_across = around(later, 2)
    stats = exchange(stats, "y")
    send, normed, own = kernel(
        dispatch_body,
        grid_spec=pltpu.PrefetchScalarGridSpec(
            num_scalar_prefetch=1,
            grid=(1,),
            in_specs=[
                pl.BlockSpec((TOKENS_HERE, QUARTER), lambda i, w: (0, 0)),
                pl.BlockSpec((4, 8, TOKENS_HERE), lambda i, w: (0, 0, 0)),
                pl.BlockSpec((1, QUARTER), lambda i, w: (0, w[0])),
                pl.BlockSpec((1, QUARTER), lambda i, w: (0, w[0])),
                pl.BlockSpec((2, TOKENS_HERE), lambda i, w: (0, 0)),
            ],
            out_specs=[
                pl.BlockSpec((EXPERTS * SLOTS_SENT, QUARTER), lambda i, w: (0, 0)),
                pl.BlockSpec((TOKENS_HERE, QUARTER), lambda i, w: (0, 0)),
                pl.BlockSpec((TOKENS_HERE, LANES), lambda i, w: (0, 0)),
            ],
        ),
        out_shape=[
            struct((EXPERTS * SLOTS_SENT, QUARTER), BF16),
            struct((TOKENS_HERE, QUARTER), BF16),
            struct((TOKENS_HERE, LANES), BF16),
        ],
    )(at, first, stats, norm1_gain[None], norm1_bias[None], routes.T)
    shared_later, send = lax.optimization_barrier((shared_packed, send))
    from_pair = lax.ppermute(shared_later, "y", [(i, i ^ 1) for i in range(4)])
    arrived = exchange(send.reshape(EXPERTS, SLOTS_SENT, QUARTER), "sp")
    gather_in = kernel(
        compact_body,
        out_shape=struct((4, ROUTED_ROWS + SHARED_ROWS, QUARTER), BF16),
        in_specs=[VMEM, VMEM],
        out_specs=VMEM,
    )(arrived.reshape(EXPERTS * SLOTS_SENT, QUARTER), normed)
    gathered = exchange(gather_in, "y")
    partial = kernel(
        expert_body,
        out_shape=struct((16, ROUTED_ROWS + SHARED_ROWS, LANES), BF16),
        in_specs=[HBM] * 7,
        out_specs=VMEM,
        scratch_shapes=[
            pltpu.VMEM((4, ROUTED_ROWS + SHARED_ROWS, QUARTER), BF16),
            pltpu.VMEM((4, PACKED, LANES), BF16),
            pltpu.VMEM((2, 3 * SHARED_UNITS, MODEL), BF16),
            pltpu.SemaphoreType.DMA((7,)),
        ],
        compiler_params=pltpu.CompilerParams(vmem_limit_bytes=40 * 1024 * 1024),
    )(gathered, packed, from_left, from_right, from_across, shared_packed, from_pair)
    parts = exchange(partial, ("y", "x"))
    back, shared_sum = kernel(
        return_body,
        out_shape=[
            struct((4 * ROUTED_ROWS, LANES), BF16),
            struct((TOKENS_HERE, LANES), F32),
        ],
        in_specs=[VMEM],
        out_specs=[VMEM, VMEM],
    )(parts)
    returned = exchange(back.reshape(EXPERTS, 4 * SLOTS_USED, LANES), "sp")
    second, row_sums = kernel(
        combine_body,
        out_shape=[struct((TOKENS_HERE, LANES), F32), struct((16, 2, TOKENS_HERE), F32)],
        in_specs=[VMEM] * 5,
        out_specs=[VMEM, VMEM],
    )(returned.reshape(4 * ROUTED_ROWS, LANES), routes.T, route_weight.T, own, shared_sum)
    row_sums = exchange(row_sums, ("y", "x"))
    return kernel(
        settle_body,
        out_shape=struct((TOKENS_HERE, LANES), BF16),
        in_specs=[VMEM] * 4,
        out_specs=VMEM,
    )(second, row_sums, norm2_gain[None], norm2_bias[None])


def solution(mesh):
    split = Mesh(mesh.devices.reshape(mesh.shape["sp"], 4, 4), ("sp", "y", "x"))
    tp = ("y", "x")
    placed = (
        P("sp", tp),
        P("sp"),
        P("sp", None),
        P("sp", None),
        P(),
        P(),
        P(),
        P(),
        P("sp", None, tp),
        P("sp", None, tp),
        P("sp", tp, None),
        P(None, tp),
        P(None, tp),
        P(tp, None),
        P(tp),
        P(tp),
    )
    return jax.shard_map(layer, mesh=split, in_specs=placed, out_specs=P("sp", tp), check_vma=False)
```

profile of v0, /device:TPU:1, one launch (start us, length us, event | category | flops | bytes accessed | tf_op | source)
XLA Modules:
  0.0 207.1 jit_solution(9362661246137817570)
XLA Ops:
  0.0 0.0 copy-start.8
  0.0 1.6 broadcast_in_dim.22
  1.6 4.8 %all-to-all-start = ((bf16[4,256,128]{2,1,0:T(8,128)(2,1)}), bf16[4,256,128]{2,1,0:T(8,128)(2,1)S(1)}, u32[]{:S(2)}, u32[]{:S(2)}) async-start(bf16[4,256,128]{2,1,0:T(8,128)(2,1)} %broadcast_in_dim.22), calls=%async_computation | async-start | bytes 524288 | tf_op jit(solution)/shard_map/all_to_all | solution.py:265
  6.4 3.8 %shard_map.154 = (bf16[6144,128]{1,0:T(8,128)(2,1)}, bf16[192,2048]{1,0:T(8,128)(2,1)}) custom-call(bf16[2048,128]{1,0:T(8,128)(2,1)} %bitcast.21, bf16[2048,128]{1,0:T(8,128)(2,1)} %bitcast.22, bf16[128,2048]{1,0:T(8,128)(2,1)} %bitcast.23, bf16[64,2048]{1,0:T(8,128)(2,1)} %bitcast.24, bf16[64,2048]{1,0:T(8,128)(2,1)} %bitcast.25, bf16[64,2048]{1,0:T(8,128)(2,1)} %sdown.1), custom_call_target="tpu_custom_call" | custom-call | flops 10000000 | bytes 3145728 | tf_op jit(solution)/shard_map/pallas_call | solution.py:296
  10.2 0.0 copy-done.8
  10.3 0.1 add_convert_fusion
  10.3 1.6 all-to-all-done.near
  12.0 0.0 copy-start.4
  12.0 0.1 broadcast_in_dim_broadcast_in_dim.2
  12.1 5.5 %collective-permute-start = (bf16[5,16,128]{2,1,0:T(8,128)(2,1)S(1)}, bf16[5,16,128]{2,1,0:T(8,128)(2,1)S(1)}, u32[]{:S(2)}, u32[]{:S(2)}) collective-permute-start(bf16[5,16,128]{2,1,0:T(8,128)(2,1)S(1)} %pad_maximum_fusion), channel_id=1, source_target_pairs={{0,16},{16,32},{32,48},{48,64},{64,80},{80,96},{96,112},{112,128},... | collective-permute-start | bytes 61448 | tf_op jit(solution)/shard_map/ppermute | solution.py:314
  17.6 0.6 pad_add_fusion.at
  18.2 2.3 %collective-permute-done.halo = bf16[5,16,128]{2,1,0:T(8,128)(2,1)S(1)} collective-permute-done((bf16[5,16,128]{2,1,0:T(8,128)(2,1)S(1)}, bf16[5,16,128]{2,1,0:T(8,128)(2,1)S(1)}, u32[]{:S(2)}, u32[]{:S(2)}) %collective-permute-start) | collective-permute-done | bytes 20512 | tf_op jit(solution)/shard_map/ppermute | solution.py:314
  20.5 0.0 copy-start.7
  20.5 0.0 copy-done.4
  20.5 0.6 copy-done.7
  21.2 0.0 copy-start
  21.2 3.4 %shard_map.155 = (f32[256,512]{1,0:T(8,128)}, f32[4,8,256]{2,1,0:T(8,128)}) custom-call(s32[2]{0:T(128)} %pad_add_fusion.at, bf16[4,256,128]{2,1,0:T(8,128)(2,1)} %copy-done.4, bf16[5,16,128]{2,1,0:T(8,128)(2,1)} %copy-done.7, s32[1,256]{1,0:T(1,128)} %bitcast.34, bf16[4,512,512]{2,1,0:T(8,128)(2,1)} %weight.1, f32[1,2048]{1,0:T(1,128)} %bitcast.28), custom_call_target="tpu_custom_call" | custom-call | tf_op jit(solution)/shard_map/pallas_call | solution.py:317
  24.5 3.3 %all-to-all-start.1 = ((f32[4,8,256]{2,1,0:T(8,128)}), f32[4,8,256]{2,1,0:T(8,128)S(1)}, u32[]{:S(2)}, u32[]{:S(2)}) async-start(f32[4,8,256]{2,1,0:T(8,128)} %get-tuple-element.30), calls=%async_computation.1 | async-start | bytes 65536 | tf_op jit(solution)/shard_map/all_to_all | solution.py:265
  27.8 4.3 %all-to-all-done.1.stats = f32[4,8,256]{2,1,0:T(8,128)S(1)} async-done(((f32[4,8,256]{2,1,0:T(8,128)}), f32[4,8,256]{2,1,0:T(8,128)S(1)}, u32[]{:S(2)}, u32[]{:S(2)}) %all-to-all-start.1) | async-done | bytes 32800 | tf_op jit(solution)/shard_map/all_to_all | solution.py:265
  32.1 0.0 copy-start.6
  32.1 0.6 copy-done.6
  32.7 2.9 %shard_map.156 = (bf16[256,512]{1,0:T(8,128)(2,1)}, bf16[256,512]{1,0:T(8,128)(2,1)}, bf16[256,128]{1,0:T(8,128)(2,1)}) custom-call(s32[2]{0:T(128)} %pad_add_fusion.at, f32[256,512]{1,0:T(8,128)} %get-tuple-element.29.first, f32[4,8,256]{2,1,0:T(8,128)} %copy-done.6, f32[1,2048]{1,0:T(1,128)} %bitcast.29, f32[1,2048]{1,0:T(1,128)} %bitcast.30, ...), custom_call_target="tpu_custom_call" | custom-call | tf_op jit(solution)/shard_map/pallas_call | solution.py:342
  35.6 17.5 %all-to-all-start.2 = ((bf16[32,8,512]{2,1,0:T(8,128)(2,1)}), bf16[32,8,512]{2,1,0:T(8,128)(2,1)S(1)}, u32[]{:S(2)}, u32[]{:S(2)}) async-start(bf16[32,8,512]{2,1,0:T(8,128)(2,1)} %bitcast.26), calls=%async_computation.2 | async-start | bytes 524288 | tf_op jit(solution)/shard_map/all_to_all | solution.py:265
  53.1 0.0 copy-done
  53.1 2.8 %collective-permute-start.2 = (bf16[6144,128]{1,0:T(8,128)(2,1)S(1)}, bf16[6144,128]{1,0:T(8,128)(2,1)}, u32[]{:S(2)}, u32[]{:S(2)}) collective-permute-start(bf16[6144,128]{1,0:T(8,128)(2,1)S(1)} %copy-done), channel_id=1, source_target_pairs={{0,3},{1,0},{2,1},{3,2},{4,7},{5,4},{6,5},{7,6},{8,11},{9,8},{10,9... | collective-permute-start | bytes 4718600 | tf_op jit(solution)/shard_map/ppermute | solution.py:269
  55.9 2.5 %collective-permute-start.1 = (bf16[6144,128]{1,0:T(8,128)(2,1)S(1)}, bf16[6144,128]{1,0:T(8,128)(2,1)}, u32[]{:S(2)}, u32[]{:S(2)}) collective-permute-start(bf16[6144,128]{1,0:T(8,128)(2,1)S(1)} %copy-done), channel_id=1, source_target_pairs={{0,1},{1,2},{2,3},{3,0},{4,5},{5,6},{6,7},{7,4},{8,9},{9,10},{10,1... | collective-permute-start | bytes 4718600 | tf_op jit(solution)/shard_map/ppermute | solution.py:269
  58.4 2.5 %collective-permute-start.3 = (bf16[6144,128]{1,0:T(8,128)(2,1)S(1)}, bf16[6144,128]{1,0:T(8,128)(2,1)}, u32[]{:S(2)}, u32[]{:S(2)}) collective-permute-start(bf16[6144,128]{1,0:T(8,128)(2,1)S(1)} %copy-done), channel_id=1, source_target_pairs={{0,2},{1,3},{2,0},{3,1},{4,6},{5,7},{6,4},{7,5},{8,10},{9,11},{10,... | collective-permute-start | bytes 4718600 | tf_op jit(solution)/shard_map/ppermute | solution.py:269
  60.9 14.4 %all-to-all-done.2 = bf16[32,8,512]{2,1,0:T(8,128)(2,1)S(1)} async-done(((bf16[32,8,512]{2,1,0:T(8,128)(2,1)}), bf16[32,8,512]{2,1,0:T(8,128)(2,1)S(1)}, u32[]{:S(2)}, u32[]{:S(2)}) %all-to-all-start.2) | async-done | bytes 262176 | tf_op jit(solution)/shard_map/all_to_all | solution.py:265
  75.4 0.0 copy-start.5
  75.4 0.7 copy-done.5
  76.1 2.3 %shard_map.157 = bf16[4,320,512]{2,1,0:T(8,128)(2,1)} custom-call(bf16[256,512]{1,0:T(8,128)(2,1)} %bitcast.19, bf16[256,512]{1,0:T(8,128)(2,1)} %get-tuple-element.33.normed), custom_call_target="tpu_custom_call" | custom-call | tf_op jit(solution)/shard_map/pallas_call | solution.py:369
  78.4 3.5 %all-to-all-start.3 = ((bf16[4,320,512]{2,1,0:T(8,128)(2,1)}), bf16[4,320,512]{2,1,0:T(8,128)(2,1)S(1)}, u32[]{:S(2)}, u32[]{:S(2)}) async-start(bf16[4,320,512]{2,1,0:T(8,128)(2,1)} %shard_map.157), calls=%async_computation.3 | async-start | bytes 2621440 | tf_op jit(solution)/shard_map/all_to_all | solution.py:265
  81.9 3.3 %collective-permute-start.4 = (bf16[192,2048]{1,0:T(8,128)(2,1)}, bf16[192,2048]{1,0:T(8,128)(2,1)S(1)}, u32[]{:S(2)}, u32[]{:S(2)}) collective-permute-start(bf16[192,2048]{1,0:T(8,128)(2,1)} %get-tuple-element.35.s0), channel_id=1, source_target_pairs={{0,4},{4,0},{8,12},{12,8},{1,5},{5,1},{9,13},{13,9},{2,6},{6,2},{1... | collective-permute-start | bytes 2359304 | tf_op jit(solution)/shard_map/ppermute | solution.py:367
  85.3 29.4 %collective-permute-done.4.s1 = bf16[192,2048]{1,0:T(8,128)(2,1)S(1)} collective-permute-done((bf16[192,2048]{1,0:T(8,128)(2,1)}, bf16[192,2048]{1,0:T(8,128)(2,1)S(1)}, u32[]{:S(2)}, u32[]{:S(2)}) %collective-permute-start.4) | collective-permute-done | bytes 786464 | tf_op jit(solution)/shard_map/ppermute | solution.py:367
  114.7 0.9 copy-done.2
  115.6 0.0 collective-permute-done.2.w2
  115.6 12.7 %collective-permute-done.1.w1 = bf16[6144,128]{1,0:T(8,128)(2,1)} collective-permute-done((bf16[6144,128]{1,0:T(8,128)(2,1)S(1)}, bf16[6144,128]{1,0:T(8,128)(2,1)}, u32[]{:S(2)}, u32[]{:S(2)}) %collective-permute-start.1) | collective-permute-done | bytes 1572896 | tf_op jit(solution)/shard_map/ppermute | solution.py:269
  128.3 0.0 collective-permute-done.3.w3
  128.3 0.0 all-to-all-done.3.rows
  128.3 1.1 copy-done.1
  129.4 1.1 copy-done.3
  130.6 4.4 %shard_map.158 = bf16[16,320,128]{2,1,0:T(8,128)(2,1)S(1)} custom-call(bf16[4,320,512]{2,1,0:T(8,128)(2,1)S(1)} %all-to-all-done.3.rows, bf16[6144,128]{1,0:T(8,128)(2,1)S(1)} %copy-done, bf16[6144,128]{1,0:T(8,128)(2,1)} %collective-permute-done.1.w1, bf16[6144,128]{1,0:T(8,128)(2,1)} %collective-permute-done.2.w2, ...), custom_call_target="tpu_custom_call" | custom-call | tf_op jit(solution)/shard_map/pallas_call | solution.py:376
  135.0 21.7 %all_to_all.35.parts = bf16[16,320,128]{2,1,0:T(8,128)(2,1)} all-to-all(bf16[16,320,128]{2,1,0:T(8,128)(2,1)S(1)} %shard_map.158), channel_id=1, replica_groups=mesh['sp'=32,'y'=4,'x'=4] {'y','x'}, dimensions={0} | all-to-all | bytes 2621440 | tf_op jit(solution)/shard_map/all_to_all | solution.py:265
  156.7 2.5 %shard_map.159 = (bf16[768,128]{1,0:T(8,128)(2,1)}, f32[256,128]{1,0:T(8,128)}) custom-call(bf16[16,320,128]{2,1,0:T(8,128)(2,1)} %all_to_all.35.parts), custom_call_target="tpu_custom_call" | custom-call | tf_op jit(solution)/shard_map/pallas_call | solution.py:390
  159.3 33.1 %all_to_all.36 = bf16[32,24,128]{2,1,0:T(8,128)(2,1)} all-to-all(bf16[32,24,128]{2,1,0:T(8,128)(2,1)} %bitcast.27), channel_id=1, replica_groups=mesh['sp'=32,'y'=4,'x'=4] {'sp'}, dimensions={0} | all-to-all | bytes 393216 | tf_op jit(solution)/shard_map/all_to_all | solution.py:265
  192.3 2.5 %shard_map.160 = (f32[256,128]{1,0:T(8,128)}, f32[16,2,256]{2,1,0:T(2,128)}) custom-call(bf16[768,128]{1,0:T(8,128)(2,1)} %bitcast.20, s32[2,256]{1,0:T(2,128)} %bitcast.32, f32[2,256]{1,0:T(2,128)} %bitcast.33, bf16[256,128]{1,0:T(8,128)(2,1)} %get-tuple-element.37.own, f32[256,128]{1,0:T(8,128)} %get-tuple-element.38.shared), custom_call_target="tpu_custom_call" | custom-call | tf_op jit(solution)/shard_map/pallas_call | solution.py:400
  194.8 10.6 %all_to_all.37.stats = f32[16,2,256]{2,1,0:T(2,128)} all-to-all(f32[16,2,256]{2,1,0:T(2,128)} %get-tuple-element.40), channel_id=1, replica_groups=mesh['sp'=32,'y'=4,'x'=4] {'y','x'}, dimensions={0} | all-to-all | bytes 65536 | tf_op jit(solution)/shard_map/all_to_all | solution.py:265
  205.4 1.7 shard_map.161
  (5 shorter events, 0.0 us)
Async XLA Ops:
  0.0 10.2 %copy-start.8 = (s32[256]{0:T(256)S(1)}, s32[256]{0:T(256)}, u32[]{:S(2)}) copy-start(s32[256]{0:T(256)} %param.17) | copy-start | bytes 3076
  1.6 10.4 %all-to-all-start = ((bf16[4,256,128]{2,1,0:T(8,128)(2,1)}), bf16[4,256,128]{2,1,0:T(8,128)(2,1)S(1)}, u32[]{:S(2)}, u32[]{:S(2)}) async-start(bf16[4,256,128]{2,1,0:T(8,128)(2,1)} %broadcast_in_dim.22), calls=%async_computation | async-start | bytes 524288 | tf_op jit(solution)/shard_map/all_to_all | solution.py:265
  12.0 8.6 %copy-start.4 = (bf16[4,256,128]{2,1,0:T(8,128)(2,1)}, bf16[4,256,128]{2,1,0:T(8,128)(2,1)S(1)}, u32[]{:S(2)}) copy-start(bf16[4,256,128]{2,1,0:T(8,128)(2,1)S(1)} %all-to-all-done.near) | copy-start | bytes 786436
  12.1 8.5 %collective-permute-start = (bf16[5,16,128]{2,1,0:T(8,128)(2,1)S(1)}, bf16[5,16,128]{2,1,0:T(8,128)(2,1)S(1)}, u32[]{:S(2)}, u32[]{:S(2)}) collective-permute-start(bf16[5,16,128]{2,1,0:T(8,128)(2,1)S(1)} %pad_maximum_fusion), channel_id=1, source_target_pairs={{0,16},{16,32},{32,48},{48,64},{64,80},{80,96},{96,112},{112,128},... | collective-permute-start | bytes 61448 | tf_op jit(solution)/shard_map/ppermute | solution.py:314
  20.5 0.6 copy-start.7
  21.2 32.0 %copy-start = (bf16[6144,128]{1,0:T(8,128)(2,1)S(1)}, bf16[6144,128]{1,0:T(8,128)(2,1)}, u32[]{:S(2)}) copy-start(bf16[6144,128]{1,0:T(8,128)(2,1)} %get-tuple-element.34.w0) | copy-start | bytes 4718596
  24.5 7.5 %all-to-all-start.1 = ((f32[4,8,256]{2,1,0:T(8,128)}), f32[4,8,256]{2,1,0:T(8,128)S(1)}, u32[]{:S(2)}, u32[]{:S(2)}) async-start(f32[4,8,256]{2,1,0:T(8,128)} %get-tuple-element.30), calls=%async_computation.1 | async-start | bytes 65536 | tf_op jit(solution)/shard_map/all_to_all | solution.py:265
  32.1 0.6 copy-start.6
  35.6 39.8 %all-to-all-start.2 = ((bf16[32,8,512]{2,1,0:T(8,128)(2,1)}), bf16[32,8,512]{2,1,0:T(8,128)(2,1)S(1)}, u32[]{:S(2)}, u32[]{:S(2)}) async-start(bf16[32,8,512]{2,1,0:T(8,128)(2,1)} %bitcast.26), calls=%async_computation.2 | async-start | bytes 524288 | tf_op jit(solution)/shard_map/all_to_all | solution.py:265
  53.1 62.5 %collective-permute-start.2 = (bf16[6144,128]{1,0:T(8,128)(2,1)S(1)}, bf16[6144,128]{1,0:T(8,128)(2,1)}, u32[]{:S(2)}, u32[]{:S(2)}) collective-permute-start(bf16[6144,128]{1,0:T(8,128)(2,1)S(1)} %copy-done), channel_id=1, source_target_pairs={{0,3},{1,0},{2,1},{3,2},{4,7},{5,4},{6,5},{7,6},{8,11},{9,8},{10,9... | collective-permute-start | bytes 4718600 | tf_op jit(solution)/shard_map/ppermute | solution.py:269
  55.9 72.4 %collective-permute-start.1 = (bf16[6144,128]{1,0:T(8,128)(2,1)S(1)}, bf16[6144,128]{1,0:T(8,128)(2,1)}, u32[]{:S(2)}, u32[]{:S(2)}) collective-permute-start(bf16[6144,128]{1,0:T(8,128)(2,1)S(1)} %copy-done), channel_id=1, source_target_pairs={{0,1},{1,2},{2,3},{3,0},{4,5},{5,6},{6,7},{7,4},{8,9},{9,10},{10,1... | collective-permute-start | bytes 4718600 | tf_op jit(solution)/shard_map/ppermute | solution.py:269
  58.4 69.9 %collective-permute-start.3 = (bf16[6144,128]{1,0:T(8,128)(2,1)S(1)}, bf16[6144,128]{1,0:T(8,128)(2,1)}, u32[]{:S(2)}, u32[]{:S(2)}) collective-permute-start(bf16[6144,128]{1,0:T(8,128)(2,1)S(1)} %copy-done), channel_id=1, source_target_pairs={{0,2},{1,3},{2,0},{3,1},{4,6},{5,7},{6,4},{7,5},{8,10},{9,11},{10,... | collective-permute-start | bytes 4718600 | tf_op jit(solution)/shard_map/ppermute | solution.py:269
  75.4 0.7 copy-start.5
  78.4 49.9 %all-to-all-start.3 = ((bf16[4,320,512]{2,1,0:T(8,128)(2,1)}), bf16[4,320,512]{2,1,0:T(8,128)(2,1)S(1)}, u32[]{:S(2)}, u32[]{:S(2)}) async-start(bf16[4,320,512]{2,1,0:T(8,128)(2,1)} %shard_map.157), calls=%async_computation.3 | async-start | bytes 2621440 | tf_op jit(solution)/shard_map/all_to_all | solution.py:265
  81.9 32.8 %collective-permute-start.4 = (bf16[192,2048]{1,0:T(8,128)(2,1)}, bf16[192,2048]{1,0:T(8,128)(2,1)S(1)}, u32[]{:S(2)}, u32[]{:S(2)}) collective-permute-start(bf16[192,2048]{1,0:T(8,128)(2,1)} %get-tuple-element.35.s0), channel_id=1, source_target_pairs={{0,4},{4,0},{8,12},{12,8},{1,5},{5,1},{9,13},{13,9},{2,6},{6,2},{1... | collective-permute-start | bytes 2359304 | tf_op jit(solution)/shard_map/ppermute | solution.py:367
  114.7 0.9 copy-start.2
  128.3 1.1 copy-start.1
  129.4 1.1 copy-start.3
where the time goes:
time: 208 us; the launch traced here: 207 us
  blocking collectives  65.3 us (31%)
  waiting for transfers between devices  64.8 us (31%)
  starting transfers between devices  45.8 us (22%)
  Pallas kernels  23.6 us (11%)
  local copies, waits for them, and re-layouts  6.77 us (3%)
    all_to_all x3, blocking collectives, exchange(): return lax.all_to_all(parts, axes, split_axis=0, concat_axis=0, tiled=True)  65.3 us
    ppermute x1, waiting for transfers between devices, layer(): from_pair = lax.ppermute(shared_later, 'y', [(i, i ^ 1) for i in range(4)])  29.4 us
    all_to_all x4, starting transfers between devices, exchange(): return lax.all_to_all(parts, axes, split_axis=0, concat_axis=0, tiled=True)  29.2 us
    all_to_all x4, waiting for transfers between devices, exchange(): return lax.all_to_all(parts, axes, split_axis=0, concat_axis=0, tiled=True)  20.3 us
    ppermute x3, waiting for transfers between devices, around(): return lax.ppermute(shard, 'x', [(i, (i + by) % 4) for i in range(4)])  12.7 us
    ppermute x3, starting transfers between devices, around(): return lax.ppermute(shard, 'x', [(i, (i + by) % 4) for i in range(4)])  7.81 us
    ppermute x1, starting transfers between devices, layer(): halo = lax.ppermute(tail, 'sp', following)  5.53 us
    unnamed x18, local copies, waits for them, and re-layouts  5.08 us
  transfers between devices with their start and end apart: 9, of which 6 were waited for; matrix products, arithmetic and copies ran while one was open for 0% of the time, Pallas kernels for 3%

commit v1 on v0

v1 whole, which is shorter than its diff:
```python
import jax
import jax.numpy as jnp
from jax import lax
from jax.experimental import pallas as pl
from jax.experimental.pallas import tpu as pltpu
from jax.sharding import Mesh
from jax.sharding import PartitionSpec as P


RESIDUAL_SCALE = 2.0**0.5
NORM_EPS = 1e-05
HALO = 16
F32 = jnp.float32
BF16 = jnp.bfloat16
VMEM = pl.BlockSpec(memory_space=pltpu.VMEM)
HELD = pl.BlockSpec(memory_space=pltpu.VMEM)
HBM = pl.BlockSpec(memory_space=pltpu.HBM)
SMEM = pl.BlockSpec(memory_space=pltpu.SMEM)

TOKENS_HERE = 256
EXPERTS = 32
LANES = 128
QUARTER = 512
MODEL = 2048
SLOTS_SENT = 8
SLOTS_USED = 6
ROUTED_ROWS = EXPERTS * SLOTS_USED
SHARED_ROWS = 128
UP_AT = 2048
DOWN_AT = 4096
PACKED = 6144
SHARED_UNITS = 64
RELAYED = PACKED // 2


def iota(shape, dim):
    return lax.broadcasted_iota(jnp.int32, shape, dim)


def side(parts):
    return jnp.concatenate(parts, axis=1)


def four(a):
    return jnp.concatenate([a, a, a, a], axis=1)


def as_column(row):
    return jnp.broadcast_to(row, (LANES, row.shape[1])).T


def chosen(mask):
    return mask.astype(F32).astype(BF16)


def sums(values):
    total = jnp.sum(values, axis=1, keepdims=True)
    return total, jnp.sum(values * values, axis=1, keepdims=True)


def row_stats(values):
    lane = iota((values.shape[0], LANES), 1)
    total, squares = sums(values)
    return jnp.where(lane == 0, total, jnp.where(lane == 1, squares, 0.0)).T


def mean_and_scale(total):
    mean = total[0:1] / MODEL
    var = total[1:2] / MODEL - mean * mean
    return as_column(mean), as_column(lax.rsqrt(var + NORM_EPS))


def ranks_of(routes):
    expert = iota((EXPERTS, TOKENS_HERE), 0)
    picks = [routes[k : k + 1] == expert for k in range(2)]
    named = chosen(picks[0] | picks[1])
    earlier = chosen(iota((TOKENS_HERE, TOKENS_HERE), 0) < iota((TOKENS_HERE, TOKENS_HERE), 1))
    counts = jnp.dot(named, earlier, preferred_element_type=F32)
    return [
        jnp.sum(jnp.where(p, counts, 0.0), axis=0, keepdims=True).astype(jnp.int32) for p in picks
    ]


def pack_body(gate, up, down, sgate, sup, sdown, low, high, shared_out, buf, shared_buf, sems):
    def moves(i):
        here = pl.ds(i * UP_AT, UP_AT)
        return pltpu.make_async_copy((gate, up)[i], buf.at[here], sems.at[i])

    def sends(i):
        here = pl.ds(i * RELAYED, RELAYED)
        return pltpu.make_async_copy(buf.at[here], (low, high)[i], sems.at[2 + i])

    moves(0).start()
    moves(1).start()
    for b in range(16):
        at = DOWN_AT + b * LANES
        buf[at : at + LANES, :] = down[:, b * LANES : (b + 1) * LANES]
    for i, part in enumerate((sgate, sup, sdown)):
        shared_buf[i * SHARED_UNITS : (i + 1) * SHARED_UNITS, :] = part[...]
    last = pltpu.make_async_copy(shared_buf, shared_out, sems.at[4])
    moves(0).wait()
    moves(1).wait()
    sends(0).start()
    sends(1).start()
    last.start()
    sends(0).wait()
    sends(1).wait()
    last.wait()


def spread_body(shard, out):
    for i in range(16):
        out[i] = shard[...]


def mixer_body(
    at,
    docs,
    routes,
    scale,
    gain,
    bias,
    near,
    halo,
    weight,
    send,
    normed,
    own,
    weight_v,
    first_v,
    sems,
):
    y, x = at[0], at[1]
    copies = [pltpu.make_async_copy(weight.at[g], weight_v.at[g], sems.at[g]) for g in range(4)]
    for c in copies:
        c.start()
    marks = jnp.concatenate(
        [halo[16].astype(F32), as_column((docs[...] + 1).astype(F32))], axis=0
    )
    members = jnp.ones(marks.shape, F32)
    insides, counts = [], []
    for step in range(4):
        inside = jnp.where(pltpu.roll(marks, 1 << step, 0) == marks, 1.0, 0.0)
        members = members + inside * pltpu.roll(members, 1 << step, 0)
        insides.append(four(inside))
        counts.append(four(members[HALO:]))
    total = jnp.zeros((TOKENS_HERE, 1), F32)
    squares = jnp.zeros((TOKENS_HERE, 1), F32)
    for g in range(4):
        lanes = slice(g * QUARTER, (g + 1) * QUARTER)
        head = side([halo[4 * g + i] for i in range(4)]).astype(F32)
        mine = side([near[4 * g + i] for i in range(4)]).astype(F32)
        running = jnp.concatenate([head, mine], axis=0)
        for step in range(g + 1):
            running = running + insides[step] * pltpu.roll(running, 1 << step, 0)
        mixed = (running[HALO:] / counts[g] - mine).astype(BF16)
        copies[g].wait()
        projected = jnp.dot(mixed, weight_v[g], preferred_element_type=F32)
        first = RESIDUAL_SCALE * mine + projected * scale[:, lanes]
        first_v[g] = first
        part, part_squares = sums(first)
        total = total + part
        squares = squares + part_squares
    mean = total / MODEL
    inv = lax.rsqrt(squares / MODEL - mean * mean + NORM_EPS)
    for g in range(4):
        lanes = slice(g * QUARTER, (g + 1) * QUARTER)
        normed[g] = ((first_v[g] - mean) * inv * gain[:, lanes] + bias[:, lanes]).astype(BF16)
    quarter = normed[y]
    named = routes[...]
    dests = []
    for k, rank in enumerate(ranks_of(named)):
        slot = named[k : k + 1] * SLOTS_SENT + (rank >> 2)
        dests.append(jnp.where((rank & 3) == x, slot, -1))
    slot = iota((EXPERTS * SLOTS_SENT, TOKENS_HERE), 0)
    pick = chosen((slot == dests[0]) | (slot == dests[1]))
    send[...] = jnp.dot(pick, quarter, preferred_element_type=F32).astype(BF16)
    mine = quarter[:, 0:LANES]
    for i in range(1, 4):
        mine = jnp.where(x == i, quarter[:, i * LANES : (i + 1) * LANES], mine)
    own[...] = mine


def compact_body(rows, out):
    shape = (ROUTED_ROWS, EXPERTS * SLOTS_SENT)
    came = iota(shape, 1)
    within = came & 7
    goes = SLOTS_USED * (came >> 3) + within
    keep = chosen((iota(shape, 0) == goes) & (within < SLOTS_USED))
    packed = jnp.dot(keep, rows[...], preferred_element_type=F32).astype(BF16)
    for i in range(4):
        out[i] = packed


def expert_body(
    at, rows, normed, *rest
):
    shards, (s0, s1, out, nv, wv, sv, sems) = rest[:8], rest[8:]
    half = pl.multiple_of((at[0] & 1) * SHARED_ROWS, SHARED_ROWS)
    plan = [
        (shard, wv.at[i // 2, pl.ds(i % 2 * RELAYED, RELAYED)]) for i, shard in enumerate(shards)
    ]
    plan += [
        (s0, sv.at[0]),
        (s1, sv.at[1]),
        (normed.at[:, pl.ds(half, SHARED_ROWS), :], nv),
    ]
    copies = [pltpu.make_async_copy(s, d, sems.at[i]) for i, (s, d) in enumerate(plan)]
    for c in copies:
        c.start()
    tokens = side([rows[i] for i in range(4)])
    hidden = []
    for c in range(4):
        copies[2 * c].wait()
        copies[2 * c + 1].wait()
        both = side([wv[c, 0:UP_AT, :], wv[c, UP_AT:DOWN_AT, :]])
        parts = jnp.dot(tokens, both, preferred_element_type=F32)
        hidden.append((jax.nn.silu(parts[:, :LANES]) * parts[:, LANES:]).astype(BF16))
    hidden = side(hidden)
    for c in copies[8:]:
        c.wait()
    shared = side([nv[i] for i in range(4)])

    def units(i, lanes):
        here = slice(i * SHARED_UNITS, (i + 1) * SHARED_UNITS)
        return jnp.concatenate([sv[0, here, lanes], sv[1, here, lanes]], axis=0)

    contract = (((1,), (1,)), ((), ()))
    every = slice(0, MODEL)
    sg = lax.dot_general(shared, units(0, every), contract, preferred_element_type=F32)
    su = lax.dot_general(shared, units(1, every), contract, preferred_element_type=F32)
    shared_hidden = (jax.nn.silu(sg) * su).astype(BF16)

    def block(c, b):
        at = DOWN_AT + b * LANES
        return wv[c, at : at + LANES, :]

    for b in range(0, 16, 2):
        down = jnp.concatenate([side([block(c, b), block(c, b + 1)]) for c in range(4)], axis=0)
        part = jnp.dot(hidden, down, preferred_element_type=F32).astype(BF16)
        out[b, 0:ROUTED_ROWS, :] = part[:, :LANES]
        out[b + 1, 0:ROUTED_ROWS, :] = part[:, LANES:]
        down = units(2, slice(b * LANES, (b + 2) * LANES))
        part = jnp.dot(shared_hidden, down, preferred_element_type=F32).astype(BF16)
        out[b, ROUTED_ROWS:, :] = part[:, :LANES]
        out[b + 1, ROUTED_ROWS:, :] = part[:, LANES:]


def return_body(parts, send, shared):
    routed = []
    for x in range(4):
        total = parts[x, 0:ROUTED_ROWS, :].astype(F32)
        for y in range(1, 4):
            total = total + parts[4 * y + x, 0:ROUTED_ROWS, :].astype(F32)
        routed.append(total.astype(BF16))
    for half in range(2):
        total = jnp.zeros((SHARED_ROWS, LANES), F32)
        for y in (half, half + 2):
            for x in range(4):
                total = total + parts[4 * y + x, ROUTED_ROWS:, :].astype(F32)
        shared[half * SHARED_ROWS : (half + 1) * SHARED_ROWS, :] = total
    rows = jnp.concatenate(routed, axis=0)
    count = 4 * ROUTED_ROWS
    came = iota((1, count), 1)
    x = (
        (came >= ROUTED_ROWS).astype(jnp.int32)
        + (came >= 2 * ROUTED_ROWS).astype(jnp.int32)
        + (came >= 3 * ROUTED_ROWS).astype(jnp.int32)
    )
    within = came - ROUTED_ROWS * x
    source = (within * 10923) >> 16
    goes = 18 * source + 6 * x + within
    move = chosen(iota((count, count), 0) == goes)
    send[...] = jnp.dot(move, rows, preferred_element_type=F32).astype(BF16)


def combine_body(rows, routes, weight, own, shared, second_out, stats_out):
    named = routes[...]
    scale = weight[...]
    slot = iota((4 * ROUTED_ROWS, TOKENS_HERE), 0)
    taken = jnp.zeros(slot.shape, F32)
    for k, rank in enumerate(ranks_of(named)):
        at = named[k : k + 1] * (4 * SLOTS_USED) + SLOTS_USED * (rank & 3) + (rank >> 2)
        taken = jnp.where(slot == at, scale[k : k + 1], taken)
    high = taken.astype(BF16)
    low = (taken - high.astype(F32)).astype(BF16)
    contract = (((0,), (0,)), ((), ()))
    mix = lax.dot_general(high, rows[...], contract, preferred_element_type=F32)
    mix = mix + lax.dot_general(low, rows[...], contract, preferred_element_type=F32)
    second = RESIDUAL_SCALE * own[...].astype(F32) + mix + shared[...]
    second_out[...] = second
    stats = row_stats(second)[0:2]
    for i in range(16):
        stats_out[i] = stats


def settle_body(second, stats, gain, bias, out):
    total = stats[0]
    for i in range(1, 16):
        total = total + stats[i]
    mean, inv = mean_and_scale(total)
    out[...] = ((second[...] - mean) * inv * gain[...] + bias[...]).astype(BF16)


def struct(shape, dtype):
    return pltpu.HBM(shape, dtype)


def exchange(parts, axes):
    return lax.all_to_all(parts, axes, split_axis=0, concat_axis=0, tiled=True)


def around(shard, by):
    return lax.ppermute(shard, "x", [(i, (i + by) % 4) for i in range(4)])


def kernel(body, in_specs, **options):
    call = pl.pallas_call(body, in_specs=in_specs, **options)
    places = {id(HELD): pltpu.VMEM, id(HBM): pltpu.HBM}

    def run(*args):
        args = [
            pltpu.with_memory_space_constraint(a, places[id(s)]) if id(s) in places else a
            for a, s in zip(args, in_specs, strict=True)
        ]
        return call(*args)

    return run


def layer(
    layer_input,
    doc_ids,
    routes,
    route_weight,
    pool_weight,
    pool_scale,
    norm1_gain,
    norm1_bias,
    expert_gate,
    expert_up,
    expert_down,
    shared_gate,
    shared_up,
    shared_down,
    norm2_gain,
    norm2_bias,
):
    at = jnp.stack([lax.axis_index("y"), lax.axis_index("x")]).astype(jnp.int32)
    spread = kernel(
        spread_body,
        out_shape=struct((16, TOKENS_HERE, LANES), BF16),
        in_specs=[VMEM],
        out_specs=VMEM,
    )(layer_input)
    near = exchange(spread, ("y", "x"))
    low, high, shared_packed = kernel(
        pack_body,
        out_shape=[
            struct((RELAYED, LANES), BF16),
            struct((RELAYED, LANES), BF16),
            struct((3 * SHARED_UNITS, MODEL), BF16),
        ],
        in_specs=[HBM, HBM, VMEM, VMEM, VMEM, VMEM],
        out_specs=[HBM] * 3,
        scratch_shapes=[
            pltpu.VMEM((PACKED, LANES), BF16),
            pltpu.VMEM((3 * SHARED_UNITS, MODEL), BF16),
            pltpu.SemaphoreType.DMA((5,)),
        ],
        cost_estimate=pl.CostEstimate(
            flops=10_000_000, bytes_accessed=4 * PACKED * LANES, transcendentals=0
        ),
    )(expert_gate[0], expert_up[0], expert_down[0], shared_gate.T, shared_up.T, shared_down)
    marks = jnp.broadcast_to((doc_ids[-HALO:] + 1).astype(BF16)[:, None], (HALO, LANES))
    tail = jnp.concatenate([near[:, -HALO:, :], marks[None]], axis=0)
    following = [(i, i + 1) for i in range(lax.axis_size("sp") - 1)]
    halo = lax.ppermute(tail, "sp", following)
    left_low = around(low, 1)
    right_high = around(high, -1)
    left_high = around(high, 1)
    right_low = around(low, -1)
    send, normed, own = kernel(
        mixer_body,
        in_specs=[SMEM] + [VMEM] * 5 + [HELD, HELD, HBM],
        out_specs=[VMEM] * 3,
        scratch_shapes=[
            pltpu.VMEM((4, QUARTER, QUARTER), BF16),
            pltpu.VMEM((4, TOKENS_HERE, QUARTER), F32),
            pltpu.SemaphoreType.DMA((4,)),
        ],
        out_shape=[
            struct((EXPERTS * SLOTS_SENT, QUARTER), BF16),
            struct((4, TOKENS_HERE, QUARTER), BF16),
            struct((TOKENS_HERE, LANES), BF16),
        ],
        compiler_params=pltpu.CompilerParams(vmem_limit_bytes=40 * 1024 * 1024),
    )(
        at,
        doc_ids[None],
        routes.T,
        pool_scale[None],
        norm1_gain[None],
        norm1_bias[None],
        near,
        halo,
        pool_weight,
    )
    shared_later, send = lax.optimization_barrier((shared_packed, send))
    from_pair = lax.ppermute(shared_later, "y", [(i, i ^ 1) for i in range(4)])
    across_low = around(left_low, 1)
    across_high = around(right_high, -1)
    arrived = exchange(send.reshape(EXPERTS, SLOTS_SENT, QUARTER), "sp")
    gather_in = kernel(
        compact_body,
        out_shape=struct((4, ROUTED_ROWS, QUARTER), BF16),
        in_specs=[HELD],
        out_specs=VMEM,
    )(arrived.reshape(EXPERTS * SLOTS_SENT, QUARTER))
    gathered = exchange(gather_in, "y")
    partial = kernel(
        expert_body,
        out_shape=struct((16, ROUTED_ROWS + SHARED_ROWS, LANES), BF16),
        in_specs=[SMEM, HELD] + [HBM] * 11,
        out_specs=VMEM,
        scratch_shapes=[
            pltpu.VMEM((4, SHARED_ROWS, QUARTER), BF16),
            pltpu.VMEM((4, PACKED, LANES), BF16),
            pltpu.VMEM((2, 3 * SHARED_UNITS, MODEL), BF16),
            pltpu.SemaphoreType.DMA((11,)),
        ],
        compiler_params=pltpu.CompilerParams(vmem_limit_bytes=40 * 1024 * 1024),
    )(
        at,
        gathered,
        normed,
        low,
        high,
        left_low,
        left_high,
        right_low,
        right_high,
        across_low,
        across_high,
        shared_packed,
        from_pair,
    )
    parts = exchange(partial, ("y", "x"))
    back, shared_sum = kernel(
        return_body,
        out_shape=[
            struct((4 * ROUTED_ROWS, LANES), BF16),
            struct((TOKENS_HERE, LANES), F32),
        ],
        in_specs=[HELD],
        out_specs=[VMEM, VMEM],
    )(parts)
    returned = exchange(back.reshape(EXPERTS, 4 * SLOTS_USED, LANES), "sp")
    second, row_sums = kernel(
        combine_body,
        out_shape=[struct((TOKENS_HERE, LANES), F32), struct((16, 2, TOKENS_HERE), F32)],
        in_specs=[HELD] + [VMEM] * 4,
        out_specs=[VMEM, VMEM],
    )(returned.reshape(4 * ROUTED_ROWS, LANES), routes.T, route_weight.T, own, shared_sum)
    row_sums = exchange(row_sums, ("y", "x"))
    return kernel(
        settle_body,
        out_shape=jax.ShapeDtypeStruct((TOKENS_HERE, LANES), BF16),
        in_specs=[VMEM, HELD, VMEM, VMEM],
        out_specs=VMEM,
    )(second, row_sums, norm2_gain[None], norm2_bias[None])


def solution(mesh):
    split = Mesh(mesh.devices.reshape(mesh.shape["sp"], 4, 4), ("sp", "y", "x"))
    tp = ("y", "x")
    placed = (
        P("sp", tp),
        P("sp"),
        P("sp", None),
        P("sp", None),
        P(),
        P(),
        P(),
        P(),
        P("sp", None, tp),
        P("sp", None, tp),
        P("sp", tp, None),
        P(None, tp),
        P(None, tp),
        P(tp, None),
        P(tp),
        P(tp),
    )
    return jax.shard_map(layer, mesh=split, in_specs=placed, out_specs=P("sp", tp), check_vma=False)
```

time: 208 us -> 192 us (0.923)
  waiting for transfers between devices: 64.8 us -> 43.6 us
  starting transfers between devices: 45.8 us -> 56 us
  local copies, waits for them, and re-layouts: 6.77 us -> 0.13 us
    ppermute x1, waiting for transfers between devices: 29.4 us -> 0.01 us  [layer(): from_pair = lax.ppermute(shared_later, 'y', [(i, i ^ 1) for i in range(4)])]
    ppermute x3 -> x6, waiting for transfers between devices: 12.7 us -> 31.8 us  [around(): return lax.ppermute(shard, 'x', [(i, (i + by) % 4) for i in range(4)])]
    ppermute x3 -> x6, starting transfers between devices: 7.81 us -> 18.3 us  [around(): return lax.ppermute(shard, 'x', [(i, (i + by) % 4) for i in range(4)])]
    all_to_all x4 -> x3, waiting for transfers between devices: 20.3 us -> 10.5 us  [exchange(): return lax.all_to_all(parts, axes, split_axis=0, concat_axis=0, tiled=True)]
    unnamed x18 -> x16, local copies, waits for them, and re-layouts: 5.08 us -> 0.04 us
    all_to_all x4 -> x3, starting transfers between devices: 29.2 us -> 28.4 us  [exchange(): return lax.all_to_all(parts, axes, split_axis=0, concat_axis=0, tiled=True)]
  transfers between devices with their start and end apart: 9 -> 11, of which waited for: 6 -> 6; matrix products, arithmetic and copies ran while one was open for 0% -> 0% of each run, Pallas kernels for 3% -> 3%
where the time goes in v1:
time: 192 us; the launch traced here: 191 us
  blocking collectives  66.4 us (35%)
  starting transfers between devices  56 us (29%)
  waiting for transfers between devices  43.6 us (23%)
  Pallas kernels  24.8 us (13%)
    all_to_all x3, blocking collectives, exchange(): return lax.all_to_all(parts, axes, split_axis=0, concat_axis=0, tiled=True)  66.4 us
    ppermute x6, waiting for transfers between devices, around(): return lax.ppermute(shard, 'x', [(i, (i + by) % 4) for i in range(4)])  31.8 us
    all_to_all x3, starting transfers between devices, exchange(): return lax.all_to_all(parts, axes, split_axis=0, concat_axis=0, tiled=True)  28.4 us
    pallas_call x8, Pallas kernels, run(): return call(*args)  24.8 us
    ppermute x6, starting transfers between devices, around(): return lax.ppermute(shard, 'x', [(i, (i + by) % 4) for i in range(4)])  18.3 us
    all_to_all x3, waiting for transfers between devices, exchange(): return lax.all_to_all(parts, axes, split_axis=0, concat_axis=0, tiled=True)  10.5 us
    ppermute x1, starting transfers between devices, layer(): halo = lax.ppermute(tail, 'sp', following)  7.44 us
  transfers between devices with their start and end apart: 11, of which 6 were waited for; matrix products, arithmetic and copies ran while one was open for 0% of the time, Pallas kernels for 3%

profile of v1, /device:TPU:1, one launch (start us, length us, event | category | flops | bytes accessed | tf_op | source)
XLA Modules:
  0.0 191.3 jit_solution(13141959654423467634)
XLA Ops:
  0.0 2.0 %shard_map.155 = bf16[16,256,128]{2,1,0:T(8,128)(2,1)} custom-call(bf16[256,128]{1,0:T(8,128)(2,1)} %shard.1), custom_call_target="tpu_custom_call" | custom-call | tf_op jit(solution)/shard_map/pallas_call | solution.py:326
  2.0 7.6 %all-to-all-start = ((bf16[16,256,128]{2,1,0:T(8,128)(2,1)}), bf16[16,256,128]{2,1,0:T(8,128)(2,1)S(1)}, u32[]{:S(2)}, u32[]{:S(2)}) async-start(bf16[16,256,128]{2,1,0:T(8,128)(2,1)} %shard_map.155), calls=%async_computation | async-start | bytes 2097152 | tf_op jit(solution)/shard_map/all_to_all | solution.py:310
  9.6 0.0 copy-start.4
  9.6 0.0 copy-start
  9.6 0.0 copy-start.1
  9.6 0.0 copy-start.2
  9.6 0.0 copy-start.3
  9.6 4.0 %shard_map.154 = (bf16[3072,128]{1,0:T(8,128)(2,1)}, bf16[3072,128]{1,0:T(8,128)(2,1)}, bf16[192,2048]{1,0:T(8,128)(2,1)}) custom-call(bf16[2048,128]{1,0:T(8,128)(2,1)} %bitcast.27, bf16[2048,128]{1,0:T(8,128)(2,1)} %bitcast.28, bf16[128,2048]{1,0:T(8,128)(2,1)} %bitcast.29, bf16[64,2048]{1,0:T(8,128)(2,1)} %bitcast.30, bf16[64,2048]{1,0:T(8,128)(2,1)} %bitcast.31, ...), custom_call_target="tpu_custom_call" | custom-call | flops 10000000 | bytes 3145728 | tf_op jit(solution)/shard_map/pallas_call | solution.py:326
  13.6 0.0 copy-done.4
  13.6 0.1 add_convert_fusion
  13.7 10.5 %all-to-all-done.near = bf16[16,256,128]{2,1,0:T(8,128)(2,1)S(1)} async-done(((bf16[16,256,128]{2,1,0:T(8,128)(2,1)}), bf16[16,256,128]{2,1,0:T(8,128)(2,1)S(1)}, u32[]{:S(2)}, u32[]{:S(2)}) %all-to-all-start) | async-done | bytes 1048608 | tf_op jit(solution)/shard_map/all_to_all | solution.py:310
  24.2 0.1 broadcast_in_dim_broadcast_in_dim.2
  24.3 7.4 %collective-permute-start = (bf16[17,16,128]{2,1,0:T(8,128)(2,1)S(1)}, bf16[17,16,128]{2,1,0:T(8,128)(2,1)S(1)}, u32[]{:S(2)}, u32[]{:S(2)}) collective-permute-start(bf16[17,16,128]{2,1,0:T(8,128)(2,1)S(1)} %pad_maximum_fusion), channel_id=1, source_target_pairs={{0,16},{16,32},{32,48},{48,64},{64,80},{80,96},{96,112},{112,128},... | collective-permute-start | bytes 208904 | tf_op jit(solution)/shard_map/ppermute | solution.py:378
  31.7 0.1 pad_add_fusion.at
  31.8 1.3 collective-permute-done.halo
  33.1 0.0 copy-done
  33.1 0.0 copy-done.1
  33.1 0.0 copy-done.2
  33.1 0.0 copy-done.3
  33.1 6.0 %shard_map.156 = (bf16[256,512]{1,0:T(8,128)(2,1)}, bf16[4,256,512]{2,1,0:T(8,128)(2,1)}, bf16[256,128]{1,0:T(8,128)(2,1)}) custom-call(s32[2]{0:T(128)S(1)} %pad_add_fusion.at, s32[1,256]{1,0:T(1,128)S(1)} %bitcast.26, s32[2,256]{1,0:T(2,128)S(1)} %bitcast.25, f32[1,2048]{1,0:T(1,128)S(1)} %bitcast.21, f32[1,2048]{1,0:T(1,128)S(1)} %bitcast.22, ...), custom_call_target="tpu_custom_call" | custom-call | tf_op jit(solution)/shard_map/pallas_call | solution.py:326
  39.1 17.3 %all-to-all-start.1 = ((bf16[32,8,512]{2,1,0:T(8,128)(2,1)}), bf16[32,8,512]{2,1,0:T(8,128)(2,1)S(1)}, u32[]{:S(2)}, u32[]{:S(2)}) async-start(bf16[32,8,512]{2,1,0:T(8,128)(2,1)} %bitcast.32), calls=%async_computation.1 | async-start | bytes 524288 | tf_op jit(solution)/shard_map/all_to_all | solution.py:310
  56.4 1.9 %collective-permute-start.1 = (bf16[3072,128]{1,0:T(8,128)(2,1)S(1)}, bf16[3072,128]{1,0:T(8,128)(2,1)}, u32[]{:S(2)}, u32[]{:S(2)}) collective-permute-start(bf16[3072,128]{1,0:T(8,128)(2,1)S(1)} %copy-done.5), channel_id=1, source_target_pairs={{0,1},{1,2},{2,3},{3,0},{4,5},{5,6},{6,7},{7,4},{8,9},{9,10},{10,1... | collective-permute-start | bytes 2359304 | tf_op jit(solution)/shard_map/ppermute | solution.py:314
  58.4 0.0 copy-done.6
  58.4 4.6 %collective-permute-start.4 = (bf16[3072,128]{1,0:T(8,128)(2,1)S(1)}, bf16[3072,128]{1,0:T(8,128)(2,1)}, u32[]{:S(2)}, u32[]{:S(2)}) collective-permute-start(bf16[3072,128]{1,0:T(8,128)(2,1)S(1)} %copy-done.6), channel_id=1, source_target_pairs={{0,3},{1,0},{2,1},{3,2},{4,7},{5,4},{6,5},{7,6},{8,11},{9,8},{10,9... | collective-permute-start | bytes 2359304 | tf_op jit(solution)/shard_map/ppermute | solution.py:314
  63.0 1.9 %collective-permute-start.3 = (bf16[3072,128]{1,0:T(8,128)(2,1)S(1)}, bf16[3072,128]{1,0:T(8,128)(2,1)}, u32[]{:S(2)}, u32[]{:S(2)}) collective-permute-start(bf16[3072,128]{1,0:T(8,128)(2,1)S(1)} %copy-done.5), channel_id=1, source_target_pairs={{0,3},{1,0},{2,1},{3,2},{4,7},{5,4},{6,5},{7,6},{8,11},{9,8},{10,9... | collective-permute-start | bytes 2359304 | tf_op jit(solution)/shard_map/ppermute | solution.py:314
  64.9 3.4 %collective-permute-start.2 = (bf16[3072,128]{1,0:T(8,128)(2,1)S(1)}, bf16[3072,128]{1,0:T(8,128)(2,1)}, u32[]{:S(2)}, u32[]{:S(2)}) collective-permute-start(bf16[3072,128]{1,0:T(8,128)(2,1)S(1)} %copy-done.6), channel_id=1, source_target_pairs={{0,1},{1,2},{2,3},{3,0},{4,5},{5,6},{6,7},{7,4},{8,9},{9,10},{10,1... | collective-permute-start | bytes 2359304 | tf_op jit(solution)/shard_map/ppermute | solution.py:314
  68.3 10.3 %collective-permute-done.1.rest_2_ = bf16[3072,128]{1,0:T(8,128)(2,1)} collective-permute-done((bf16[3072,128]{1,0:T(8,128)(2,1)S(1)}, bf16[3072,128]{1,0:T(8,128)(2,1)}, u32[]{:S(2)}, u32[]{:S(2)}) %collective-permute-start.1) | collective-permute-done | bytes 786464 | tf_op jit(solution)/shard_map/ppermute | solution.py:314
  78.5 1.9 collective-permute-start.5
  80.4 0.0 collective-permute-done.4.rest_5_
  80.4 4.6 %collective-permute-start.6 = (bf16[3072,128]{1,0:T(8,128)(2,1)}, bf16[3072,128]{1,0:T(8,128)(2,1)}, u32[]{:S(2)}, u32[]{:S(2)}) collective-permute-start(bf16[3072,128]{1,0:T(8,128)(2,1)} %collective-permute-done.4.rest_5_), channel_id=1, source_target_pairs={{0,3},{1,0},{2,1},{3,2},{4,7},{5,4},{6,5},{7,6},{8,11},{9,8},{10,9... | collective-permute-start | bytes 2359304 | tf_op jit(solution)/shard_map/ppermute | solution.py:314
  85.0 0.0 copy-done.7
  85.0 1.9 %collective-permute-start.7 = (bf16[192,2048]{1,0:T(8,128)(2,1)S(1)}, bf16[192,2048]{1,0:T(8,128)(2,1)}, u32[]{:S(2)}, u32[]{:S(2)}) collective-permute-start(bf16[192,2048]{1,0:T(8,128)(2,1)S(1)} %copy-done.7), channel_id=1, source_target_pairs={{0,4},{4,0},{8,12},{12,8},{1,5},{5,1},{9,13},{13,9},{2,6},{6,2},{1... | collective-permute-start | bytes 2359304 | tf_op jit(solution)/shard_map/ppermute | solution.py:410
  87.0 0.0 all-to-all-done.1
  87.0 1.1 shard_map.157
  88.1 3.5 %all-to-all-start.2 = ((bf16[4,192,512]{2,1,0:T(8,128)(2,1)}), bf16[4,192,512]{2,1,0:T(8,128)(2,1)S(1)}, u32[]{:S(2)}, u32[]{:S(2)}) async-start(bf16[4,192,512]{2,1,0:T(8,128)(2,1)} %shard_map.157), calls=%async_computation.2 | async-start | bytes 1572864 | tf_op jit(solution)/shard_map/all_to_all | solution.py:310
  91.6 4.6 %collective-permute-done.3.rest_4_ = bf16[3072,128]{1,0:T(8,128)(2,1)} collective-permute-done((bf16[3072,128]{1,0:T(8,128)(2,1)S(1)}, bf16[3072,128]{1,0:T(8,128)(2,1)}, u32[]{:S(2)}, u32[]{:S(2)}) %collective-permute-start.3) | collective-permute-done | bytes 786464 | tf_op jit(solution)/shard_map/ppermute | solution.py:314
  96.2 0.0 collective-permute-done.2.rest_3_
  96.2 16.0 %collective-permute-done.5.rest_6_ = bf16[3072,128]{1,0:T(8,128)(2,1)} collective-permute-done((bf16[3072,128]{1,0:T(8,128)(2,1)}, bf16[3072,128]{1,0:T(8,128)(2,1)}, u32[]{:S(2)}, u32[]{:S(2)}) %collective-permute-start.5) | collective-permute-done | bytes 786464 | tf_op jit(solution)/shard_map/ppermute | solution.py:314
  112.2 0.9 collective-permute-done.6.rest_7_
  113.1 0.0 collective-permute-done.7.rest_9_
  113.1 0.0 all-to-all-done.2.rows
  113.1 6.4 %shard_map.158 = bf16[16,320,128]{2,1,0:T(8,128)(2,1)} custom-call(s32[2]{0:T(128)S(1)} %pad_add_fusion.at, bf16[4,192,512]{2,1,0:T(8,128)(2,1)S(1)} %all-to-all-done.2.rows, bf16[4,256,512]{2,1,0:T(8,128)(2,1)} %get-tuple-element.20.normed, bf16[3072,128]{1,0:T(8,128)(2,1)} %get-tuple-element.21.rest_0_, bf16[3072,128]{1,0:T(8,128)(2,1)} %get-tuple-element.22.rest_1_, ...), custom_call_target="tpu_custom_call" | custom-call | tf_op jit(solution)/shard_map/pallas_call | solution.py:326
  119.6 23.4 %all_to_all.30.parts = bf16[16,320,128]{2,1,0:T(8,128)(2,1)S(1)} all-to-all(bf16[16,320,128]{2,1,0:T(8,128)(2,1)} %shard_map.158), channel_id=1, replica_groups=mesh['sp'=32,'y'=4,'x'=4] {'y','x'}, dimensions={0} | all-to-all | bytes 2621440 | tf_op jit(solution)/shard_map/all_to_all | solution.py:310
  142.9 1.2 shard_map.159
  144.2 33.1 %all_to_all.31 = bf16[32,24,128]{2,1,0:T(8,128)(2,1)S(1)} all-to-all(bf16[32,24,128]{2,1,0:T(8,128)(2,1)} %bitcast.33), channel_id=1, replica_groups=mesh['sp'=32,'y'=4,'x'=4] {'sp'}, dimensions={0} | all-to-all | bytes 393216 | tf_op jit(solution)/shard_map/all_to_all | solution.py:310
  177.3 2.4 %shard_map.160 = (f32[256,128]{1,0:T(8,128)}, f32[16,2,256]{2,1,0:T(2,128)}) custom-call(bf16[768,128]{1,0:T(8,128)(2,1)S(1)} %bitcast.20, s32[2,256]{1,0:T(2,128)} %bitcast.24, f32[2,256]{1,0:T(2,128)} %bitcast.34, bf16[256,128]{1,0:T(8,128)(2,1)} %get-tuple-element.25.own, f32[256,128]{1,0:T(8,128)} %get-tuple-element.26.shared), custom_call_target="tpu_custom_call" | custom-call | tf_op jit(solution)/shard_map/pallas_call | solution.py:326
  179.7 9.9 %all_to_all.32.stats = f32[16,2,256]{2,1,0:T(2,128)S(1)} all-to-all(f32[16,2,256]{2,1,0:T(2,128)} %get-tuple-element.28), channel_id=1, replica_groups=mesh['sp'=32,'y'=4,'x'=4] {'y','x'}, dimensions={0} | all-to-all | bytes 65536 | tf_op jit(solution)/shard_map/all_to_all | solution.py:310
  189.6 1.7 shard_map.161
  (6 shorter events, 0.0 us)
Async XLA Ops:
  2.0 22.2 %all-to-all-start = ((bf16[16,256,128]{2,1,0:T(8,128)(2,1)}), bf16[16,256,128]{2,1,0:T(8,128)(2,1)S(1)}, u32[]{:S(2)}, u32[]{:S(2)}) async-start(bf16[16,256,128]{2,1,0:T(8,128)(2,1)} %shard_map.155), calls=%async_computation | async-start | bytes 2097152 | tf_op jit(solution)/shard_map/all_to_all | solution.py:310
  9.6 4.0 %copy-start.4 = (s32[256]{0:T(256)S(1)}, s32[256]{0:T(256)}, u32[]{:S(2)}) copy-start(s32[256]{0:T(256)} %param.17) | copy-start | bytes 3076
  9.6 23.5 %copy-start = (f32[2048]{0:T(1024)S(1)}, f32[2048]{0:T(1024)}, u32[]{:S(2)}) copy-start(f32[2048]{0:T(1024)} %param.21) | copy-start | bytes 24580
  9.6 23.5 %copy-start.1 = (f32[2048]{0:T(1024)S(1)}, f32[2048]{0:T(1024)}, u32[]{:S(2)}) copy-start(f32[2048]{0:T(1024)} %param.22) | copy-start | bytes 24580
  9.6 23.5 %copy-start.2 = (f32[2048]{0:T(1024)S(1)}, f32[2048]{0:T(1024)}, u32[]{:S(2)}) copy-start(f32[2048]{0:T(1024)} %param.23) | copy-start | bytes 24580
  9.6 23.5 %copy-start.3 = (s32[256,2]{0,1:T(2,128)S(1)}, s32[256,2]{0,1:T(2,128)}, u32[]{:S(2)}) copy-start(s32[256,2]{0,1:T(2,128)} %param.18) | copy-start | bytes 6148
  24.3 8.8 %collective-permute-start = (bf16[17,16,128]{2,1,0:T(8,128)(2,1)S(1)}, bf16[17,16,128]{2,1,0:T(8,128)(2,1)S(1)}, u32[]{:S(2)}, u32[]{:S(2)}) collective-permute-start(bf16[17,16,128]{2,1,0:T(8,128)(2,1)S(1)} %pad_maximum_fusion), channel_id=1, source_target_pairs={{0,16},{16,32},{32,48},{48,64},{64,80},{80,96},{96,112},{112,128},... | collective-permute-start | bytes 208904 | tf_op jit(solution)/shard_map/ppermute | solution.py:378
  33.1 23.3 %copy-start.5 = (bf16[3072,128]{1,0:T(8,128)(2,1)S(1)}, bf16[3072,128]{1,0:T(8,128)(2,1)}, u32[]{:S(2)}) copy-start(bf16[3072,128]{1,0:T(8,128)(2,1)} %get-tuple-element.21.rest_0_) | copy-start | bytes 2359300
  33.1 25.3 %copy-start.6 = (bf16[3072,128]{1,0:T(8,128)(2,1)S(1)}, bf16[3072,128]{1,0:T(8,128)(2,1)}, u32[]{:S(2)}) copy-start(bf16[3072,128]{1,0:T(8,128)(2,1)} %get-tuple-element.22.rest_1_) | copy-start | bytes 2359300
  33.1 51.9 %copy-start.7 = (bf16[192,2048]{1,0:T(8,128)(2,1)S(1)}, bf16[192,2048]{1,0:T(8,128)(2,1)}, u32[]{:S(2)}) copy-start(bf16[192,2048]{1,0:T(8,128)(2,1)} %get-tuple-element.23.rest_8_) | copy-start | bytes 2359300
  39.1 47.9 %all-to-all-start.1 = ((bf16[32,8,512]{2,1,0:T(8,128)(2,1)}), bf16[32,8,512]{2,1,0:T(8,128)(2,1)S(1)}, u32[]{:S(2)}, u32[]{:S(2)}) async-start(bf16[32,8,512]{2,1,0:T(8,128)(2,1)} %bitcast.32), calls=%async_computation.1 | async-start | bytes 524288 | tf_op jit(solution)/shard_map/all_to_all | solution.py:310
  56.4 22.1 %collective-permute-start.1 = (bf16[3072,128]{1,0:T(8,128)(2,1)S(1)}, bf16[3072,128]{1,0:T(8,128)(2,1)}, u32[]{:S(2)}, u32[]{:S(2)}) collective-permute-start(bf16[3072,128]{1,0:T(8,128)(2,1)S(1)} %copy-done.5), channel_id=1, source_target_pairs={{0,1},{1,2},{2,3},{3,0},{4,5},{5,6},{6,7},{7,4},{8,9},{9,10},{10,1... | collective-permute-start | bytes 2359304 | tf_op jit(solution)/shard_map/ppermute | solution.py:314
  58.4 22.1 %collective-permute-start.4 = (bf16[3072,128]{1,0:T(8,128)(2,1)S(1)}, bf16[3072,128]{1,0:T(8,128)(2,1)}, u32[]{:S(2)}, u32[]{:S(2)}) collective-permute-start(bf16[3072,128]{1,0:T(8,128)(2,1)S(1)} %copy-done.6), channel_id=1, source_target_pairs={{0,3},{1,0},{2,1},{3,2},{4,7},{5,4},{6,5},{7,6},{8,11},{9,8},{10,9... | collective-permute-start | bytes 2359304 | tf_op jit(solution)/shard_map/ppermute | solution.py:314
  63.0 33.2 %collective-permute-start.3 = (bf16[3072,128]{1,0:T(8,128)(2,1)S(1)}, bf16[3072,128]{1,0:T(8,128)(2,1)}, u32[]{:S(2)}, u32[]{:S(2)}) collective-permute-start(bf16[3072,128]{1,0:T(8,128)(2,1)S(1)} %copy-done.5), channel_id=1, source_target_pairs={{0,3},{1,0},{2,1},{3,2},{4,7},{5,4},{6,5},{7,6},{8,11},{9,8},{10,9... | collective-permute-start | bytes 2359304 | tf_op jit(solution)/shard_map/ppermute | solution.py:314
  64.9 31.3 %collective-permute-start.2 = (bf16[3072,128]{1,0:T(8,128)(2,1)S(1)}, bf16[3072,128]{1,0:T(8,128)(2,1)}, u32[]{:S(2)}, u32[]{:S(2)}) collective-permute-start(bf16[3072,128]{1,0:T(8,128)(2,1)S(1)} %copy-done.6), channel_id=1, source_target_pairs={{0,1},{1,2},{2,3},{3,0},{4,5},{5,6},{6,7},{7,4},{8,9},{9,10},{10,1... | collective-permute-start | bytes 2359304 | tf_op jit(solution)/shard_map/ppermute | solution.py:314
  78.5 33.7 %collective-permute-start.5 = (bf16[3072,128]{1,0:T(8,128)(2,1)}, bf16[3072,128]{1,0:T(8,128)(2,1)}, u32[]{:S(2)}, u32[]{:S(2)}) collective-permute-start(bf16[3072,128]{1,0:T(8,128)(2,1)} %collective-permute-done.1.rest_2_), channel_id=1, source_target_pairs={{0,1},{1,2},{2,3},{3,0},{4,5},{5,6},{6,7},{7,4},{8,9},{9,10},{10,1... | collective-permute-start | bytes 2359304 | tf_op jit(solution)/shard_map/ppermute | solution.py:314
  80.4 32.7 %collective-permute-start.6 = (bf16[3072,128]{1,0:T(8,128)(2,1)}, bf16[3072,128]{1,0:T(8,128)(2,1)}, u32[]{:S(2)}, u32[]{:S(2)}) collective-permute-start(bf16[3072,128]{1,0:T(8,128)(2,1)} %collective-permute-done.4.rest_5_), channel_id=1, source_target_pairs={{0,3},{1,0},{2,1},{3,2},{4,7},{5,4},{6,5},{7,6},{8,11},{9,8},{10,9... | collective-permute-start | bytes 2359304 | tf_op jit(solution)/shard_map/ppermute | solution.py:314
  85.0 28.1 %collective-permute-start.7 = (bf16[192,2048]{1,0:T(8,128)(2,1)S(1)}, bf16[192,2048]{1,0:T(8,128)(2,1)}, u32[]{:S(2)}, u32[]{:S(2)}) collective-permute-start(bf16[192,2048]{1,0:T(8,128)(2,1)S(1)} %copy-done.7), channel_id=1, source_target_pairs={{0,4},{4,0},{8,12},{12,8},{1,5},{5,1},{9,13},{13,9},{2,6},{6,2},{1... | collective-permute-start | bytes 2359304 | tf_op jit(solution)/shard_map/ppermute | solution.py:410
  88.1 25.1 %all-to-all-start.2 = ((bf16[4,192,512]{2,1,0:T(8,128)(2,1)}), bf16[4,192,512]{2,1,0:T(8,128)(2,1)S(1)}, u32[]{:S(2)}, u32[]{:S(2)}) async-start(bf16[4,192,512]{2,1,0:T(8,128)(2,1)} %shard_map.157), calls=%async_computation.2 | async-start | bytes 1572864 | tf_op jit(solution)/shard_map/all_to_all | solution.py:310

commit v2 on v1

--- a/solution.py
+++ b/solution.py
@@ -15,6 +15,7 @@
 VMEM = pl.BlockSpec(memory_space=pltpu.VMEM)
 HELD = pl.BlockSpec(memory_space=pltpu.VMEM)
 HBM = pl.BlockSpec(memory_space=pltpu.HBM)
+ANY = pl.BlockSpec(memory_space=pl.ANY)
 SMEM = pl.BlockSpec(memory_space=pltpu.SMEM)
 
 TOKENS_HERE = 256
@@ -30,6 +31,7 @@
 DOWN_AT = 4096
 PACKED = 6144
 SHARED_UNITS = 64
+HALF_UNITS = SHARED_UNITS // 2
 RELAYED = PACKED // 2
 
 
@@ -81,36 +83,37 @@
     ]
 
 
-def pack_body(gate, up, down, sgate, sup, sdown, low, high, shared_out, buf, shared_buf, sems):
-    def moves(i):
-        here = pl.ds(i * UP_AT, UP_AT)
-        return pltpu.make_async_copy((gate, up)[i], buf.at[here], sems.at[i])
-
-    def sends(i):
-        here = pl.ds(i * RELAYED, RELAYED)
-        return pltpu.make_async_copy(buf.at[here], (low, high)[i], sems.at[2 + i])
-
-    moves(0).start()
-    moves(1).start()
+def pack_body(at, gate, up, down, sgate, sup, sdown, low, high, shared_out, half_out, sems):
+    core = pl.multiple_of(at[2] * HALF_UNITS, HALF_UNITS)
+    rest = DOWN_AT - RELAYED
+    plan = [
+        (gate, low.at[pl.ds(0, UP_AT)]),
+        (up.at[pl.ds(0, RELAYED - UP_AT)], low.at[pl.ds(UP_AT, RELAYED - UP_AT)]),
+        (up.at[pl.ds(RELAYED - UP_AT, rest)], high.at[pl.ds(0, rest)]),
+    ]
     for b in range(16):
-        at = DOWN_AT + b * LANES
-        buf[at : at + LANES, :] = down[:, b * LANES : (b + 1) * LANES]
+        lanes = pl.ds(b * LANES, LANES)
+        plan.append((down.at[:, lanes], high.at[pl.ds(rest + b * LANES, LANES)]))
     for i, part in enumerate((sgate, sup, sdown)):
-        shared_buf[i * SHARED_UNITS : (i + 1) * SHARED_UNITS, :] = part[...]
-    last = pltpu.make_async_copy(shared_buf, shared_out, sems.at[4])
-    moves(0).wait()
-    moves(1).wait()
-    sends(0).start()
-    sends(1).start()
-    last.start()
-    sends(0).wait()
-    sends(1).wait()
-    last.wait()
-
-
-def spread_body(shard, out):
-    for i in range(16):
-        out[i] = shard[...]
+        plan.append((part, shared_out.at[pl.ds(i * SHARED_UNITS, SHARED_UNITS)]))
+        mine = part.at[pl.ds(core, HALF_UNITS)]
+        plan.append((mine, half_out.at[pl.ds(i * HALF_UNITS, HALF_UNITS)]))
+    copies = [pltpu.make_async_copy(s, d, sems.at[i]) for i, (s, d) in enumerate(plan)]
+    for c in copies:
+        c.start()
+    for c in copies:
+        c.wait()
+
+
+def spread_body(shard, out, block, sems):
+    move = pltpu.make_async_copy(shard, block, sems.at[16])
+    move.start()
+    move.wait()
+    copies = [pltpu.make_async_copy(block, out.at[i], sems.at[i]) for i in range(16)]
+    for c in copies:
+        c.start()
+    for c in copies:
+        c.wait()
 
 
 def mixer_body(
@@ -192,58 +195,77 @@
         out[i] = packed
 
 
-def expert_body(
-    at, rows, normed, *rest
-):
-    shards, (s0, s1, out, nv, wv, sv, sems) = rest[:8], rest[8:]
+def shared_body(at, normed, s0, s1, s2, out, own_v, near_v, far_v, part_v, sems):
+    copies = [
+        pltpu.make_async_copy(source, target, sems.at[i])
+        for i, (source, target) in enumerate(((s0, own_v), (s1, near_v), (s2, far_v)))
+    ]
+    for c in copies:
+        c.start()
     half = pl.multiple_of((at[0] & 1) * SHARED_ROWS, SHARED_ROWS)
-    plan = [
-        (shard, wv.at[i // 2, pl.ds(i % 2 * RELAYED, RELAYED)]) for i, shard in enumerate(shards)
-    ]
-    plan += [
-        (s0, sv.at[0]),
-        (s1, sv.at[1]),
-        (normed.at[:, pl.ds(half, SHARED_ROWS), :], nv),
-    ]
-    copies = [pltpu.make_async_copy(s, d, sems.at[i]) for i, (s, d) in enumerate(plan)]
-    for c in copies:
-        c.start()
-    tokens = side([rows[i] for i in range(4)])
-    hidden = []
-    for c in range(4):
-        copies[2 * c].wait()
-        copies[2 * c + 1].wait()
-        both = side([wv[c, 0:UP_AT, :], wv[c, UP_AT:DOWN_AT, :]])
-        parts = jnp.dot(tokens, both, preferred_element_type=F32)
-        hidden.append((jax.nn.silu(parts[:, :LANES]) * parts[:, LANES:]).astype(BF16))
-    hidden = side(hidden)
-    for c in copies[8:]:
+    shared = side([normed[i, pl.ds(half, SHARED_ROWS), :] for i in range(4)])
+    for c in copies:
         c.wait()
-    shared = side([nv[i] for i in range(4)])
 
     def units(i, lanes):
         here = slice(i * SHARED_UNITS, (i + 1) * SHARED_UNITS)
-        return jnp.concatenate([sv[0, here, lanes], sv[1, here, lanes]], axis=0)
+        half = slice(i * HALF_UNITS, (i + 1) * HALF_UNITS)
+        return jnp.concatenate([own_v[here, lanes], near_v[half, lanes], far_v[half, lanes]], axis=0)
 
     contract = (((1,), (1,)), ((), ()))
     every = slice(0, MODEL)
     sg = lax.dot_general(shared, units(0, every), contract, preferred_element_type=F32)
     su = lax.dot_general(shared, units(1, every), contract, preferred_element_type=F32)
-    shared_hidden = (jax.nn.silu(sg) * su).astype(BF16)
+    hidden = (jax.nn.silu(sg) * su).astype(BF16)
+    for b in range(0, 16, 2):
+        down = units(2, slice(b * LANES, (b + 2) * LANES))
+        part = jnp.dot(hidden, down, preferred_element_type=F32).astype(BF16)
+        part_v[b] = part[:, :LANES]
+        part_v[b + 1] = part[:, LANES:]
+    send = pltpu.make_async_copy(part_v, out.at[:, pl.ds(ROUTED_ROWS, SHARED_ROWS), :], sems.at[3])
+    send.start()
+    send.wait()
+
+
+def expert_body(rows, low, high, w0, w1, w2, w3, w4, w5, begun, out, wv, part_v, sems):
+    moved = (w0, w1, w2, w3, w4, w5)
+    copies = [pltpu.make_async_copy(m, wv.at[i], sems.at[i]) for i, m in enumerate(moved)]
+    for c in copies:
+        c.start()
+
+    def lower(c, start, stop):
+        return wv[2 * c - 2, start:stop, :] if c else low[start:stop, :]
+
+    def upper(c, start, stop):
+        start, stop = start - RELAYED, stop - RELAYED
+        return wv[2 * c - 1, start:stop, :] if c else high[start:stop, :]
+
+    tokens = side([rows[i] for i in range(4)])
+    hidden = []
+    for c in range(4):
+        if c:
+            copies[2 * c - 2].wait()
+            copies[2 * c - 1].wait()
+        ups = [lower(c, UP_AT, RELAYED), upper(c, RELAYED, DOWN_AT)]
+        both = side([lower(c, 0, UP_AT), jnp.concatenate(ups, axis=0)])
+        parts = jnp.dot(tokens, both, preferred_element_type=F32)
+        hidden.append((jax.nn.silu(parts[:, :LANES]) * parts[:, LANES:]).astype(BF16))
+    hidden = side(hidden)
 
     def block(c, b):
-        at = DOWN_AT + b * LANES
-        return wv[c, at : at + LANES, :]
-
+        return upper(c, DOWN_AT + b * LANES, DOWN_AT + (b + 1) * LANES)
+
+    sends = []
     for b in range(0, 16, 2):
         down = jnp.concatenate([side([block(c, b), block(c, b + 1)]) for c in range(4)], axis=0)
         part = jnp.dot(hidden, down, preferred_element_type=F32).astype(BF16)
-        out[b, 0:ROUTED_ROWS, :] = part[:, :LANES]
-        out[b + 1, 0:ROUTED_ROWS, :] = part[:, LANES:]
-        down = units(2, slice(b * LANES, (b + 2) * LANES))
-        part = jnp.dot(shared_hidden, down, preferred_element_type=F32).astype(BF16)
-        out[b, ROUTED_ROWS:, :] = part[:, :LANES]
-        out[b + 1, ROUTED_ROWS:, :] = part[:, LANES:]
+        part_v[b] = part[:, :LANES]
+        part_v[b + 1] = part[:, LANES:]
+        target = out.at[pl.ds(b, 2), pl.ds(0, ROUTED_ROWS), :]
+        sends.append(pltpu.make_async_copy(part_v.at[pl.ds(b, 2)], target, sems.at[6 + b // 2]))
+        sends[-1].start()
+    for c in sends:
+        c.wait()
 
 
 def return_body(parts, send, shared):
@@ -274,7 +296,7 @@
     send[...] = jnp.dot(move, rows, preferred_element_type=F32).astype(BF16)
 
 
-def combine_body(rows, routes, weight, own, shared, second_out, stats_out):
+def weigh_body(routes, weight, high_out, low_out):
     named = routes[...]
     scale = weight[...]
     slot = iota((4 * ROUTED_ROWS, TOKENS_HERE), 0)
@@ -282,11 +304,15 @@
     for k, rank in enumerate(ranks_of(named)):
         at = named[k : k + 1] * (4 * SLOTS_USED) + SLOTS_USED * (rank & 3) + (rank >> 2)
         taken = jnp.where(slot == at, scale[k : k + 1], taken)
+    taken = taken.T
     high = taken.astype(BF16)
-    low = (taken - high.astype(F32)).astype(BF16)
-    contract = (((0,), (0,)), ((), ()))
-    mix = lax.dot_general(high, rows[...], contract, preferred_element_type=F32)
-    mix = mix + lax.dot_general(low, rows[...], contract, preferred_element_type=F32)
+    high_out[...] = high
+    low_out[...] = (taken - high.astype(F32)).astype(BF16)
+
+
+def combine_body(rows, high, low, own, shared, second_out, stats_out):
+    mix = jnp.dot(high[...], rows[...], preferred_element_type=F32)
+    mix = mix + jnp.dot(low[...], rows[...], preferred_element_type=F32)
     second = RESIDUAL_SCALE * own[...].astype(F32) + mix + shared[...]
     second_out[...] = second
     stats = row_stats(second)[0:2]
@@ -306,6 +332,10 @@
     return pltpu.HBM(shape, dtype)
 
 
+def held(shape, dtype):
+    return pltpu.VMEM(shape, dtype)
+
+
 def exchange(parts, axes):
     return lax.all_to_all(parts, axes, split_axis=0, concat_axis=0, tiled=True)
 
@@ -315,7 +345,8 @@
 
 
 def kernel(body, in_specs, **options):
-    call = pl.pallas_call(body, in_specs=in_specs, **options)
+    params = pltpu.CompilerParams(vmem_limit_bytes=24 * 1024 * 1024)
+    call = pl.pallas_call(body, in_specs=in_specs, compiler_params=params, **options)
     places = {id(HELD): pltpu.VMEM, id(HBM): pltpu.HBM}
 
     def run(*args):
@@ -346,32 +377,42 @@
     norm2_gain,
     norm2_bias,
 ):
-    at = jnp.stack([lax.axis_index("y"), lax.axis_index("x")]).astype(jnp.int32)
+    core = lax.axis_index("sp") & 1
+    at = jnp.stack([lax.axis_index("y"), lax.axis_index("x"), core]).astype(jnp.int32)
     spread = kernel(
         spread_body,
         out_shape=struct((16, TOKENS_HERE, LANES), BF16),
-        in_specs=[VMEM],
-        out_specs=VMEM,
+        in_specs=[HBM],
+        out_specs=HBM,
+        scratch_shapes=[
+            pltpu.VMEM((TOKENS_HERE, LANES), BF16),
+            pltpu.SemaphoreType.DMA((17,)),
+        ],
     )(layer_input)
     near = exchange(spread, ("y", "x"))
-    low, high, shared_packed = kernel(
+    low, high, shared_packed, shared_half = kernel(
         pack_body,
         out_shape=[
-            struct((RELAYED, LANES), BF16),
-            struct((RELAYED, LANES), BF16),
+            held((RELAYED, LANES), BF16),
+            held((RELAYED, LANES), BF16),
             struct((3 * SHARED_UNITS, MODEL), BF16),
-        ],
-        in_specs=[HBM, HBM, VMEM, VMEM, VMEM, VMEM],
-        out_specs=[HBM] * 3,
-        scratch_shapes=[
-            pltpu.VMEM((PACKED, LANES), BF16),
-            pltpu.VMEM((3 * SHARED_UNITS, MODEL), BF16),
-            pltpu.SemaphoreType.DMA((5,)),
-        ],
+            struct((3 * HALF_UNITS, MODEL), BF16),
+        ],
+        in_specs=[SMEM] + [HBM] * 6,
+        out_specs=[VMEM] * 4,
+        scratch_shapes=[pltpu.SemaphoreType.DMA((25,))],
         cost_estimate=pl.CostEstimate(
             flops=10_000_000, bytes_accessed=4 * PACKED * LANES, transcendentals=0
         ),
-    )(expert_gate[0], expert_up[0], expert_down[0], shared_gate.T, shared_up.T, shared_down)
+    )(
+        at,
+        expert_gate[0],
+        expert_up[0],
+        expert_down[0],
+        shared_gate.T,
+        shared_up.T,
+        shared_down,
+    )
     marks = jnp.broadcast_to((doc_ids[-HALO:] + 1).astype(BF16)[:, None], (HALO, LANES))
     tail = jnp.concatenate([near[:, -HALO:, :], marks[None]], axis=0)
     following = [(i, i + 1) for i in range(lax.axis_size("sp") - 1)]
@@ -391,10 +432,9 @@
         ],
         out_shape=[
             struct((EXPERTS * SLOTS_SENT, QUARTER), BF16),
-            struct((4, TOKENS_HERE, QUARTER), BF16),
-            struct((TOKENS_HERE, LANES), BF16),
-        ],
-        compiler_params=pltpu.CompilerParams(vmem_limit_bytes=40 * 1024 * 1024),
+            held((4, TOKENS_HERE, QUARTER), BF16),
+            held((TOKENS_HERE, LANES), BF16),
+        ],
     )(
         at,
         doc_ids[None],
@@ -406,8 +446,9 @@
         halo,
         pool_weight,
     )
-    shared_later, send = lax.optimization_barrier((shared_packed, send))
-    from_pair = lax.ppermute(shared_later, "y", [(i, i ^ 1) for i in range(4)])
+    from_pair = lax.ppermute(shared_half, "y", [(i, i ^ 1) for i in range(4)])
+    cores = [(i, i ^ 1) for i in range(lax.axis_size("sp"))]
+    from_core = lax.ppermute(from_pair, "sp", cores)
     across_low = around(left_low, 1)
     across_high = around(right_high, -1)
     arrived = exchange(send.reshape(EXPERTS, SLOTS_SENT, QUARTER), "sp")
@@ -418,22 +459,32 @@
         out_specs=VMEM,
     )(arrived.reshape(EXPERTS * SLOTS_SENT, QUARTER))
     gathered = exchange(gather_in, "y")
+    begun = kernel(
+        shared_body,
+        out_shape=struct((16, ROUTED_ROWS + SHARED_ROWS, LANES), BF16),
+        in_specs=[SMEM, HELD, HBM, HBM, ANY],
+        out_specs=HBM,
+        scratch_shapes=[
+            pltpu.VMEM((3 * SHARED_UNITS, MODEL), BF16),
+            pltpu.VMEM((3 * HALF_UNITS, MODEL), BF16),
+            pltpu.VMEM((3 * HALF_UNITS, MODEL), BF16),
+            pltpu.VMEM((16, SHARED_ROWS, LANES), BF16),
+            pltpu.SemaphoreType.DMA((4,)),
+        ],
+    )(at, normed, shared_packed, from_pair, from_core)
     partial = kernel(
         expert_body,
         out_shape=struct((16, ROUTED_ROWS + SHARED_ROWS, LANES), BF16),
-        in_specs=[SMEM, HELD] + [HBM] * 11,
-        out_specs=VMEM,
+        in_specs=[HELD] * 3 + [HBM] * 7,
+        out_specs=HBM,
         scratch_shapes=[
-            pltpu.VMEM((4, SHARED_ROWS, QUARTER), BF16),
-            pltpu.VMEM((4, PACKED, LANES), BF16),
-            pltpu.VMEM((2, 3 * SHARED_UNITS, MODEL), BF16),
-            pltpu.SemaphoreType.DMA((11,)),
-        ],
-        compiler_params=pltpu.CompilerParams(vmem_limit_bytes=40 * 1024 * 1024),
+            pltpu.VMEM((6, RELAYED, LANES), BF16),
+            pltpu.VMEM((16, ROUTED_ROWS, LANES), BF16),
+            pltpu.SemaphoreType.DMA((14,)),
+        ],
+        input_output_aliases={9: 0},
     )(
-        at,
         gathered,
-        normed,
         low,
         high,
         left_low,
@@ -442,31 +493,36 @@
         right_high,
         across_low,
         across_high,
-        shared_packed,
-        from_pair,
+        begun,
     )
     parts = exchange(partial, ("y", "x"))
     back, shared_sum = kernel(
         return_body,
         out_shape=[
             struct((4 * ROUTED_ROWS, LANES), BF16),
-            struct((TOKENS_HERE, LANES), F32),
+            held((TOKENS_HERE, LANES), F32),
         ],
         in_specs=[HELD],
         out_specs=[VMEM, VMEM],
     )(parts)
     returned = exchange(back.reshape(EXPERTS, 4 * SLOTS_USED, LANES), "sp")
+    high_weights, low_weights = kernel(
+        weigh_body,
+        out_shape=[held((TOKENS_HERE, 4 * ROUTED_ROWS), BF16)] * 2,
+        in_specs=[VMEM] * 2,
+        out_specs=[VMEM] * 2,
+    )(routes.T, route_weight.T)
     second, row_sums = kernel(
         combine_body,
-        out_shape=[struct((TOKENS_HERE, LANES), F32), struct((16, 2, TOKENS_HERE), F32)],
-        in_specs=[HELD] + [VMEM] * 4,
+        out_shape=[held((TOKENS_HERE, LANES), F32), struct((16, 2, TOKENS_HERE), F32)],
+        in_specs=[HELD] * 5,
         out_specs=[VMEM, VMEM],
-    )(returned.reshape(4 * ROUTED_ROWS, LANES), routes.T, route_weight.T, own, shared_sum)
+    )(returned.reshape(4 * ROUTED_ROWS, LANES), high_weights, low_weights, own, shared_sum)
     row_sums = exchange(row_sums, ("y", "x"))
     return kernel(
         settle_body,
         out_shape=jax.ShapeDtypeStruct((TOKENS_HERE, LANES), BF16),
-        in_specs=[VMEM, HELD, VMEM, VMEM],
+        in_specs=[HELD, HELD, VMEM, VMEM],
         out_specs=VMEM,
     )(second, row_sums, norm2_gain[None], norm2_bias[None])
 

time: 192 us -> 193 us (level)
  blocking collectives: 66.4 us -> 33.2 us
  starting transfers between devices: 56 us -> 76.3 us
  waiting for transfers between devices: 43.6 us -> 57 us
    all_to_all x3 -> x2, blocking collectives: 66.4 us -> 33.2 us  [exchange(): return lax.all_to_all(parts, axes, split_axis=0, concat_axis=0, tiled=True)]
    all_to_all x3 -> x4, waiting for transfers between devices: 10.5 us -> 32.8 us  [exchange(): return lax.all_to_all(parts, axes, split_axis=0, concat_axis=0, tiled=True)]
    all_to_all x3 -> x4, starting transfers between devices: 28.4 us -> 42.9 us  [exchange(): return lax.all_to_all(parts, axes, split_axis=0, concat_axis=0, tiled=True)]
    ppermute x6, waiting for transfers between devices: 31.8 us -> 21.3 us  [around(): return lax.ppermute(shard, 'x', [(i, (i + by) % 4) for i in range(4)])]
    ppermute x1 -> x2, starting transfers between devices: 1.92 us -> 6.45 us  [the longest x1 4.53 us: layer(): from_core = lax.ppermute(from_pair, 'sp', cores)]
    pallas_call x8 -> x10, Pallas kernels: 24.8 us -> 25.1 us  [run(): return call(*args)]
  transfers between devices with their start and end apart: 11 -> 13, of which waited for: 6 -> 7; matrix products, arithmetic and copies ran while one was open for 0% -> 0% of each run, Pallas kernels for 3% -> 5%
where the time goes in v2:
time: 193 us; the launch traced here: 192 us
  starting transfers between devices  76.3 us (40%)
  waiting for transfers between devices  57 us (30%)
  blocking collectives  33.2 us (17%)
  Pallas kernels  25.1 us (13%)
    all_to_all x4, starting transfers between devices, exchange(): return lax.all_to_all(parts, axes, split_axis=0, concat_axis=0, tiled=True)  42.9 us
    all_to_all x2, blocking collectives, exchange(): return lax.all_to_all(parts, axes, split_axis=0, concat_axis=0, tiled=True)  33.2 us
    all_to_all x4, waiting for transfers between devices, exchange(): return lax.all_to_all(parts, axes, split_axis=0, concat_axis=0, tiled=True)  32.8 us
    pallas_call x10, Pallas kernels, run(): return call(*args)  25.1 us
    ppermute x6, waiting for transfers between devices, around(): return lax.ppermute(shard, 'x', [(i, (i + by) % 4) for i in range(4)])  21.3 us
    ppermute x6, starting transfers between devices, around(): return lax.ppermute(shard, 'x', [(i, (i + by) % 4) for i in range(4)])  19.5 us
    ppermute x1, starting transfers between devices, layer(): halo = lax.ppermute(tail, 'sp', following)  7.44 us
    ppermute x1, starting transfers between devices, layer(): from_core = lax.ppermute(from_pair, 'sp', cores)  4.53 us
  transfers between devices with their start and end apart: 13, of which 7 were waited for; matrix products, arithmetic and copies ran while one was open for 0% of the time, Pallas kernels for 5%

profile of v2, /device:TPU:1, one launch (start us, length us, event | category | flops | bytes accessed | tf_op | source)
XLA Modules:
  0.0 192.1 jit_solution(13462404186896198179)
XLA Ops:
  0.0 2.0 %shard_map.154 = bf16[16,256,128]{2,1,0:T(8,128)(2,1)} custom-call(bf16[256,128]{1,0:T(8,128)(2,1)} %shard.1), custom_call_target="tpu_custom_call" | custom-call | tf_op jit(solution)/shard_map/pallas_call | solution.py:357
  2.0 0.0 copy-start.5
  2.0 0.0 copy-start
  2.0 0.0 copy-start.1
  2.0 0.0 copy-start.2
  2.0 0.0 copy-start.3
  2.0 7.7 %all-to-all-start = ((bf16[16,256,128]{2,1,0:T(8,128)(2,1)}), bf16[16,256,128]{2,1,0:T(8,128)(2,1)S(1)}, u32[]{:S(2)}, u32[]{:S(2)}) async-start(bf16[16,256,128]{2,1,0:T(8,128)(2,1)} %shard_map.154), calls=%async_computation | async-start | bytes 2097152 | tf_op jit(solution)/shard_map/all_to_all | solution.py:340
  9.8 0.0 copy-done.5
  9.8 0.1 add_convert_fusion
  9.9 14.5 %all-to-all-done.near = bf16[16,256,128]{2,1,0:T(8,128)(2,1)S(1)} async-done(((bf16[16,256,128]{2,1,0:T(8,128)(2,1)}), bf16[16,256,128]{2,1,0:T(8,128)(2,1)S(1)}, u32[]{:S(2)}, u32[]{:S(2)}) %all-to-all-start) | async-done | bytes 1048608 | tf_op jit(solution)/shard_map/all_to_all | solution.py:340
  24.4 0.1 broadcast_in_dim_broadcast_in_dim.2
  24.5 7.4 %collective-permute-start = (bf16[17,16,128]{2,1,0:T(8,128)(2,1)S(1)}, bf16[17,16,128]{2,1,0:T(8,128)(2,1)S(1)}, u32[]{:S(2)}, u32[]{:S(2)}) collective-permute-start(bf16[17,16,128]{2,1,0:T(8,128)(2,1)S(1)} %pad_maximum_fusion), channel_id=1, source_target_pairs={{0,16},{16,32},{32,48},{48,64},{64,80},{80,96},{96,112},{112,128},... | collective-permute-start | bytes 208904 | tf_op jit(solution)/shard_map/ppermute | solution.py:419
  31.9 0.1 pad_add_fusion.at
  32.0 1.3 collective-permute-done.halo
  33.3 0.0 copy-done.3
  33.3 5.8 %shard_map.155 = (bf16[256,512]{1,0:T(8,128)(2,1)}, bf16[4,256,512]{2,1,0:T(8,128)(2,1)S(1)}, bf16[256,128]{1,0:T(8,128)(2,1)S(1)}) custom-call(s32[3]{0:T(128)S(1)} %pad_add_fusion.at, s32[1,256]{1,0:T(1,128)S(1)} %bitcast.28, s32[2,256]{1,0:T(2,128)S(1)} %bitcast.25, f32[1,2048]{1,0:T(1,128)S(1)} %bitcast.22, f32[1,2048]{1,0:T(1,128)S(1)} %bitcast.23, ...), custom_call_target="tpu_custom_call" | custom-call | tf_op jit(solution)/shard_map/pallas_call | solution.py:357
  39.1 17.3 %all-to-all-start.1 = ((bf16[32,8,512]{2,1,0:T(8,128)(2,1)}), bf16[32,8,512]{2,1,0:T(8,128)(2,1)S(1)}, u32[]{:S(2)}, u32[]{:S(2)}) async-start(bf16[32,8,512]{2,1,0:T(8,128)(2,1)} %bitcast.36), calls=%async_computation.1 | async-start | bytes 524288 | tf_op jit(solution)/shard_map/all_to_all | solution.py:340
  56.4 3.8 %shard_map.157 = (bf16[3072,128]{1,0:T(8,128)(2,1)S(1)}, bf16[3072,128]{1,0:T(8,128)(2,1)}, bf16[192,2048]{1,0:T(8,128)(2,1)}, bf16[96,2048]{1,0:T(8,128)(2,1)}) custom-call(s32[3]{0:T(128)S(1)} %pad_add_fusion.at, bf16[2048,128]{1,0:T(8,128)(2,1)} %bitcast.31, bf16[2048,128]{1,0:T(8,128)(2,1)} %bitcast.32, bf16[128,2048]{1,0:T(8,128)(2,1)} %bitcast.33, ...), custom_call_target="tpu_custom_call" | custom-call | flops 10000000 | bytes 3145728 | tf_op jit(solution)/shard_map/pallas_call | solution.py:357
  60.2 1.9 collective-permute-start.1
  62.1 4.6 %collective-permute-start.4 = (bf16[3072,128]{1,0:T(8,128)(2,1)}, bf16[3072,128]{1,0:T(8,128)(2,1)}, u32[]{:S(2)}, u32[]{:S(2)}) collective-permute-start(bf16[3072,128]{1,0:T(8,128)(2,1)} %get-tuple-element.20.high), channel_id=1, source_target_pairs={{0,3},{1,0},{2,1},{3,2},{4,7},{5,4},{6,5},{7,6},{8,11},{9,8},{10,9... | collective-permute-start | bytes 2359304 | tf_op jit(solution)/shard_map/ppermute | solution.py:344
  66.7 1.9 %collective-permute-start.7 = (bf16[96,2048]{1,0:T(8,128)(2,1)}, bf16[96,2048]{1,0:T(8,128)(2,1)}, u32[]{:S(2)}, u32[]{:S(2)}) collective-permute-start(bf16[96,2048]{1,0:T(8,128)(2,1)} %get-tuple-element.23), channel_id=1, source_target_pairs={{0,4},{4,0},{8,12},{12,8},{1,5},{5,1},{9,13},{13,9},{2,6},{6,2},{1... | collective-permute-start | bytes 1179656 | tf_op jit(solution)/shard_map/ppermute | solution.py:449
  68.6 1.9 %collective-permute-start.2 = (bf16[3072,128]{1,0:T(8,128)(2,1)}, bf16[3072,128]{1,0:T(8,128)(2,1)}, u32[]{:S(2)}, u32[]{:S(2)}) collective-permute-start(bf16[3072,128]{1,0:T(8,128)(2,1)} %get-tuple-element.20.high), channel_id=1, source_target_pairs={{0,1},{1,2},{2,3},{3,0},{4,5},{5,6},{6,7},{7,4},{8,9},{9,10},{10,1... | collective-permute-start | bytes 2359304 | tf_op jit(solution)/shard_map/ppermute | solution.py:344
  70.5 4.6 %collective-permute-start.3 = (bf16[3072,128]{1,0:T(8,128)(2,1)S(1)}, bf16[3072,128]{1,0:T(8,128)(2,1)}, u32[]{:S(2)}, u32[]{:S(2)}) collective-permute-start(bf16[3072,128]{1,0:T(8,128)(2,1)S(1)} %get-tuple-element.19.low), channel_id=1, source_target_pairs={{0,3},{1,0},{2,1},{3,2},{4,7},{5,4},{6,5},{7,6},{8,11},{9,8},{10,9... | collective-permute-start | bytes 2359304 | tf_op jit(solution)/shard_map/ppermute | solution.py:344
  75.1 7.0 %collective-permute-done.1.w0 = bf16[3072,128]{1,0:T(8,128)(2,1)S(1)} collective-permute-done((bf16[3072,128]{1,0:T(8,128)(2,1)S(1)}, bf16[3072,128]{1,0:T(8,128)(2,1)S(1)}, u32[]{:S(2)}, u32[]{:S(2)}) %collective-permute-start.1) | collective-permute-done | bytes 786464 | tf_op jit(solution)/shard_map/ppermute | solution.py:344
  82.1 1.9 collective-permute-start.5
  84.1 0.0 collective-permute-done.4.w3
  84.1 4.6 %collective-permute-start.6 = (bf16[3072,128]{1,0:T(8,128)(2,1)}, bf16[3072,128]{1,0:T(8,128)(2,1)}, u32[]{:S(2)}, u32[]{:S(2)}) collective-permute-start(bf16[3072,128]{1,0:T(8,128)(2,1)} %collective-permute-done.4.w3), channel_id=1, source_target_pairs={{0,3},{1,0},{2,1},{3,2},{4,7},{5,4},{6,5},{7,6},{8,11},{9,8},{10,9... | collective-permute-start | bytes 2359304 | tf_op jit(solution)/shard_map/ppermute | solution.py:344
  88.7 0.0 all-to-all-done.1
  88.7 1.2 shard_map.156
  89.9 3.5 %all-to-all-start.2 = ((bf16[4,192,512]{2,1,0:T(8,128)(2,1)}), bf16[4,192,512]{2,1,0:T(8,128)(2,1)S(1)}, u32[]{:S(2)}, u32[]{:S(2)}) async-start(bf16[4,192,512]{2,1,0:T(8,128)(2,1)} %shard_map.156), calls=%async_computation.2 | async-start | bytes 1572864 | tf_op jit(solution)/shard_map/all_to_all | solution.py:340
  93.4 0.0 collective-permute-done.7.s1
  93.4 4.5 %collective-permute-start.8 = (bf16[96,2048]{1,0:T(8,128)(2,1)}, bf16[96,2048]{1,0:T(8,128)(2,1)S(1)}, u32[]{:S(2)}, u32[]{:S(2)}) collective-permute-start(bf16[96,2048]{1,0:T(8,128)(2,1)} %collective-permute-done.7.s1), channel_id=1, source_target_pairs={{0,16},{16,0},{32,48},{48,32},{64,80},{80,64},{96,112},{112,96},{1... | collective-permute-start | bytes 1179656 | tf_op jit(solution)/shard_map/ppermute | solution.py:451
  97.9 1.5 collective-permute-done.8.s2
  99.5 3.3 %shard_map.158.begun = bf16[16,320,128]{2,1,0:T(8,128)(2,1)} custom-call(s32[3]{0:T(128)S(1)} %pad_add_fusion.at, bf16[4,256,512]{2,1,0:T(8,128)(2,1)S(1)} %get-tuple-element.21.normed, bf16[192,2048]{1,0:T(8,128)(2,1)} %get-tuple-element.22.s0, bf16[96,2048]{1,0:T(8,128)(2,1)} %collective-permute-done.7.s1, bf16[96,2048]{1,0:T(8,128)(2,1)S(1)} %collective-permute-done.8.s2), custom_call_target="tpu_custom_call" | custom-call | tf_op jit(solution)/shard_map/pallas_call | solution.py:357
  102.8 0.0 collective-permute-done.2.w1
  102.8 0.0 collective-permute-done.3.w2
  102.8 13.2 %collective-permute-done.5.w4 = bf16[3072,128]{1,0:T(8,128)(2,1)} collective-permute-done((bf16[3072,128]{1,0:T(8,128)(2,1)S(1)}, bf16[3072,128]{1,0:T(8,128)(2,1)}, u32[]{:S(2)}, u32[]{:S(2)}) %collective-permute-start.5) | collective-permute-done | bytes 786464 | tf_op jit(solution)/shard_map/ppermute | solution.py:344
  116.0 1.1 collective-permute-done.6.w5
  117.1 0.0 all-to-all-done.2.rows
  117.1 5.5 %shard_map.159 = bf16[16,320,128]{2,1,0:T(8,128)(2,1)} custom-call(bf16[4,192,512]{2,1,0:T(8,128)(2,1)S(1)} %all-to-all-done.2.rows, bf16[3072,128]{1,0:T(8,128)(2,1)S(1)} %get-tuple-element.19.low, bf16[3072,128]{1,0:T(8,128)(2,1)} %get-tuple-element.20.high, bf16[3072,128]{1,0:T(8,128)(2,1)} %copy-done.8, ...), custom_call_target="tpu_custom_call", output_to_operand_aliasing={{}: (9, {})} | custom-call | tf_op jit(solution)/shard_map/pallas_call | solution.py:357
  122.5 23.4 %all_to_all.30.parts = bf16[16,320,128]{2,1,0:T(8,128)(2,1)S(1)} all-to-all(bf16[16,320,128]{2,1,0:T(8,128)(2,1)} %shard_map.159), channel_id=1, replica_groups=mesh['sp'=32,'y'=4,'x'=4] {'y','x'}, dimensions={0} | all-to-all | bytes 2621440 | tf_op jit(solution)/shard_map/all_to_all | solution.py:340
  145.9 1.3 shard_map.160
  147.2 14.3 %all-to-all-start.4 = ((bf16[32,24,128]{2,1,0:T(8,128)(2,1)}), bf16[32,24,128]{2,1,0:T(8,128)(2,1)S(1)}, u32[]{:S(2)}, u32[]{:S(2)}) async-start(bf16[32,24,128]{2,1,0:T(8,128)(2,1)} %bitcast.37), calls=%async_computation.4 | async-start | bytes 393216 | tf_op jit(solution)/shard_map/all_to_all | solution.py:340
  161.6 0.5 shard_map.161
  162.0 18.3 %all-to-all-done.4 = bf16[32,24,128]{2,1,0:T(8,128)(2,1)S(1)} async-done(((bf16[32,24,128]{2,1,0:T(8,128)(2,1)}), bf16[32,24,128]{2,1,0:T(8,128)(2,1)S(1)}, u32[]{:S(2)}, u32[]{:S(2)}) %all-to-all-start.4) | async-done | bytes 196640 | tf_op jit(solution)/shard_map/all_to_all | solution.py:340
  180.3 1.1 shard_map.162
  181.5 9.9 %all_to_all.31.stats = f32[16,2,256]{2,1,0:T(2,128)S(1)} all-to-all(f32[16,2,256]{2,1,0:T(2,128)} %get-tuple-element.30), channel_id=1, replica_groups=mesh['sp'=32,'y'=4,'x'=4] {'y','x'}, dimensions={0} | all-to-all | bytes 65536 | tf_op jit(solution)/shard_map/all_to_all | solution.py:340
  191.3 0.8 shard_map.163
  (13 shorter events, 0.0 us)
Async XLA Ops:
  2.0 7.8 %copy-start.5 = (s32[256]{0:T(256)S(1)}, s32[256]{0:T(256)}, u32[]{:S(2)}) copy-start(s32[256]{0:T(256)} %param.17) | copy-start | bytes 3076
  2.0 31.3 %copy-start = (f32[2048]{0:T(1024)S(1)}, f32[2048]{0:T(1024)}, u32[]{:S(2)}) copy-start(f32[2048]{0:T(1024)} %param.21) | copy-start | bytes 24580
  2.0 31.3 %copy-start.1 = (f32[2048]{0:T(1024)S(1)}, f32[2048]{0:T(1024)}, u32[]{:S(2)}) copy-start(f32[2048]{0:T(1024)} %param.22) | copy-start | bytes 24580
  2.0 31.3 %copy-start.2 = (f32[2048]{0:T(1024)S(1)}, f32[2048]{0:T(1024)}, u32[]{:S(2)}) copy-start(f32[2048]{0:T(1024)} %param.23) | copy-start | bytes 24580
  2.0 31.3 %copy-start.3 = (s32[256,2]{0,1:T(2,128)S(1)}, s32[256,2]{0,1:T(2,128)}, u32[]{:S(2)}) copy-start(s32[256,2]{0,1:T(2,128)} %param.18) | copy-start | bytes 6148
  2.0 22.3 %all-to-all-start = ((bf16[16,256,128]{2,1,0:T(8,128)(2,1)}), bf16[16,256,128]{2,1,0:T(8,128)(2,1)S(1)}, u32[]{:S(2)}, u32[]{:S(2)}) async-start(bf16[16,256,128]{2,1,0:T(8,128)(2,1)} %shard_map.154), calls=%async_computation | async-start | bytes 2097152 | tf_op jit(solution)/shard_map/all_to_all | solution.py:340
  24.5 8.8 %collective-permute-start = (bf16[17,16,128]{2,1,0:T(8,128)(2,1)S(1)}, bf16[17,16,128]{2,1,0:T(8,128)(2,1)S(1)}, u32[]{:S(2)}, u32[]{:S(2)}) collective-permute-start(bf16[17,16,128]{2,1,0:T(8,128)(2,1)S(1)} %pad_maximum_fusion), channel_id=1, source_target_pairs={{0,16},{16,32},{32,48},{48,64},{64,80},{80,96},{96,112},{112,128},... | collective-permute-start | bytes 208904 | tf_op jit(solution)/shard_map/ppermute | solution.py:419
  39.1 49.6 %all-to-all-start.1 = ((bf16[32,8,512]{2,1,0:T(8,128)(2,1)}), bf16[32,8,512]{2,1,0:T(8,128)(2,1)S(1)}, u32[]{:S(2)}, u32[]{:S(2)}) async-start(bf16[32,8,512]{2,1,0:T(8,128)(2,1)} %bitcast.36), calls=%async_computation.1 | async-start | bytes 524288 | tf_op jit(solution)/shard_map/all_to_all | solution.py:340
  60.2 22.0 %collective-permute-start.1 = (bf16[3072,128]{1,0:T(8,128)(2,1)S(1)}, bf16[3072,128]{1,0:T(8,128)(2,1)S(1)}, u32[]{:S(2)}, u32[]{:S(2)}) collective-permute-start(bf16[3072,128]{1,0:T(8,128)(2,1)S(1)} %get-tuple-element.19.low), channel_id=1, source_target_pairs={{0,1},{1,2},{2,3},{3,0},{4,5},{5,6},{6,7},{7,4},{8,9},{9,10},{10,1... | collective-permute-start | bytes 2359304 | tf_op jit(solution)/shard_map/ppermute | solution.py:344
  62.1 22.0 %collective-permute-start.4 = (bf16[3072,128]{1,0:T(8,128)(2,1)}, bf16[3072,128]{1,0:T(8,128)(2,1)}, u32[]{:S(2)}, u32[]{:S(2)}) collective-permute-start(bf16[3072,128]{1,0:T(8,128)(2,1)} %get-tuple-element.20.high), channel_id=1, source_target_pairs={{0,3},{1,0},{2,1},{3,2},{4,7},{5,4},{6,5},{7,6},{8,11},{9,8},{10,9... | collective-permute-start | bytes 2359304 | tf_op jit(solution)/shard_map/ppermute | solution.py:344
  66.7 26.7 %collective-permute-start.7 = (bf16[96,2048]{1,0:T(8,128)(2,1)}, bf16[96,2048]{1,0:T(8,128)(2,1)}, u32[]{:S(2)}, u32[]{:S(2)}) collective-permute-start(bf16[96,2048]{1,0:T(8,128)(2,1)} %get-tuple-element.23), channel_id=1, source_target_pairs={{0,4},{4,0},{8,12},{12,8},{1,5},{5,1},{9,13},{13,9},{2,6},{6,2},{1... | collective-permute-start | bytes 1179656 | tf_op jit(solution)/shard_map/ppermute | solution.py:449
  68.6 34.2 %collective-permute-start.2 = (bf16[3072,128]{1,0:T(8,128)(2,1)}, bf16[3072,128]{1,0:T(8,128)(2,1)}, u32[]{:S(2)}, u32[]{:S(2)}) collective-permute-start(bf16[3072,128]{1,0:T(8,128)(2,1)} %get-tuple-element.20.high), channel_id=1, source_target_pairs={{0,1},{1,2},{2,3},{3,0},{4,5},{5,6},{6,7},{7,4},{8,9},{9,10},{10,1... | collective-permute-start | bytes 2359304 | tf_op jit(solution)/shard_map/ppermute | solution.py:344
  70.5 32.2 %collective-permute-start.3 = (bf16[3072,128]{1,0:T(8,128)(2,1)S(1)}, bf16[3072,128]{1,0:T(8,128)(2,1)}, u32[]{:S(2)}, u32[]{:S(2)}) collective-permute-start(bf16[3072,128]{1,0:T(8,128)(2,1)S(1)} %get-tuple-element.19.low), channel_id=1, source_target_pairs={{0,3},{1,0},{2,1},{3,2},{4,7},{5,4},{6,5},{7,6},{8,11},{9,8},{10,9... | collective-permute-start | bytes 2359304 | tf_op jit(solution)/shard_map/ppermute | solution.py:344
  82.1 7.7 %copy-start.8 = (bf16[3072,128]{1,0:T(8,128)(2,1)}, bf16[3072,128]{1,0:T(8,128)(2,1)S(1)}, u32[]{:S(2)}) copy-start(bf16[3072,128]{1,0:T(8,128)(2,1)S(1)} %collective-permute-done.1.w0) | copy-start | bytes 2359300
  82.1 33.8 %collective-permute-start.5 = (bf16[3072,128]{1,0:T(8,128)(2,1)S(1)}, bf16[3072,128]{1,0:T(8,128)(2,1)}, u32[]{:S(2)}, u32[]{:S(2)}) collective-permute-start(bf16[3072,128]{1,0:T(8,128)(2,1)S(1)} %collective-permute-done.1.w0), channel_id=1, source_target_pairs={{0,1},{1,2},{2,3},{3,0},{4,5},{5,6},{6,7},{7,4},{8,9},{9,10},{10,1... | collective-permute-start | bytes 2359304 | tf_op jit(solution)/shard_map/ppermute | solution.py:344
  84.1 33.0 %collective-permute-start.6 = (bf16[3072,128]{1,0:T(8,128)(2,1)}, bf16[3072,128]{1,0:T(8,128)(2,1)}, u32[]{:S(2)}, u32[]{:S(2)}) collective-permute-start(bf16[3072,128]{1,0:T(8,128)(2,1)} %collective-permute-done.4.w3), channel_id=1, source_target_pairs={{0,3},{1,0},{2,1},{3,2},{4,7},{5,4},{6,5},{7,6},{8,11},{9,8},{10,9... | collective-permute-start | bytes 2359304 | tf_op jit(solution)/shard_map/ppermute | solution.py:344
  89.9 27.2 %all-to-all-start.2 = ((bf16[4,192,512]{2,1,0:T(8,128)(2,1)}), bf16[4,192,512]{2,1,0:T(8,128)(2,1)S(1)}, u32[]{:S(2)}, u32[]{:S(2)}) async-start(bf16[4,192,512]{2,1,0:T(8,128)(2,1)} %shard_map.156), calls=%async_computation.2 | async-start | bytes 1572864 | tf_op jit(solution)/shard_map/all_to_all | solution.py:340
  93.4 6.1 %collective-permute-start.8 = (bf16[96,2048]{1,0:T(8,128)(2,1)}, bf16[96,2048]{1,0:T(8,128)(2,1)S(1)}, u32[]{:S(2)}, u32[]{:S(2)}) collective-permute-start(bf16[96,2048]{1,0:T(8,128)(2,1)} %collective-permute-done.7.s1), channel_id=1, source_target_pairs={{0,16},{16,0},{32,48},{48,32},{64,80},{80,64},{96,112},{112,96},{1... | collective-permute-start | bytes 1179656 | tf_op jit(solution)/shard_map/ppermute | solution.py:451
  145.9 15.6 %copy-start.4 = (f32[256,2]{0,1:T(2,128)S(1)}, f32[256,2]{0,1:T(2,128)}, u32[]{:S(2)}) copy-start(f32[256,2]{0,1:T(2,128)} %param.19) | copy-start | bytes 6148
  145.9 45.4 %copy-start.6 = (f32[128]{0:T(128)S(1)}, f32[128]{0:T(128)}, u32[]{:S(2)}) copy-start(f32[128]{0:T(128)} %param.30) | copy-start | bytes 1540
  145.9 45.4 %copy-start.7 = (f32[128]{0:T(128)S(1)}, f32[128]{0:T(128)}, u32[]{:S(2)}) copy-start(f32[128]{0:T(128)} %param.31) | copy-start | bytes 1540
  147.2 33.1 %all-to-all-start.4 = ((bf16[32,24,128]{2,1,0:T(8,128)(2,1)}), bf16[32,24,128]{2,1,0:T(8,128)(2,1)S(1)}, u32[]{:S(2)}, u32[]{:S(2)}) async-start(bf16[32,24,128]{2,1,0:T(8,128)(2,1)} %bitcast.37), calls=%async_computation.4 | async-start | bytes 393216 | tf_op jit(solution)/shard_map/all_to_all | solution.py:340

commit v3 on v2

--- a/solution.py
+++ b/solution.py
@@ -130,6 +130,7 @@
     normed,
     own,
     weight_v,
+    mixed_v,
     first_v,
     sems,
 ):
@@ -146,19 +147,21 @@
         inside = jnp.where(pltpu.roll(marks, 1 << step, 0) == marks, 1.0, 0.0)
         members = members + inside * pltpu.roll(members, 1 << step, 0)
         insides.append(four(inside))
-        counts.append(four(members[HALO:]))
-    total = jnp.zeros((TOKENS_HERE, 1), F32)
-    squares = jnp.zeros((TOKENS_HERE, 1), F32)
+        counts.append(four(1.0 / members[HALO:]))
     for g in range(4):
-        lanes = slice(g * QUARTER, (g + 1) * QUARTER)
         head = side([halo[4 * g + i] for i in range(4)]).astype(F32)
         mine = side([near[4 * g + i] for i in range(4)]).astype(F32)
         running = jnp.concatenate([head, mine], axis=0)
         for step in range(g + 1):
             running = running + insides[step] * pltpu.roll(running, 1 << step, 0)
-        mixed = (running[HALO:] / counts[g] - mine).astype(BF16)
+        mixed_v[g] = (running[HALO:] * counts[g] - mine).astype(BF16)
+    total = jnp.zeros((TOKENS_HERE, 1), F32)
+    squares = jnp.zeros((TOKENS_HERE, 1), F32)
+    for g in range(4):
+        lanes = slice(g * QUARTER, (g + 1) * QUARTER)
         copies[g].wait()
-        projected = jnp.dot(mixed, weight_v[g], preferred_element_type=F32)
+        projected = jnp.dot(mixed_v[g], weight_v[g], preferred_element_type=F32)
+        mine = side([near[4 * g + i] for i in range(4)]).astype(F32)
         first = RESIDUAL_SCALE * mine + projected * scale[:, lanes]
         first_v[g] = first
         part, part_squares = sums(first)
@@ -227,25 +230,24 @@
     send.wait()
 
 
-def expert_body(rows, low, high, w0, w1, w2, w3, w4, w5, begun, out, wv, part_v, sems):
-    moved = (w0, w1, w2, w3, w4, w5)
+def expert_body(rows, w0, w1, w2, w3, w4, w5, w6, w7, begun, out, wv, part_v, sems):
+    moved = (w1, w2, w3, w4, w5, w6, w7)
     copies = [pltpu.make_async_copy(m, wv.at[i], sems.at[i]) for i, m in enumerate(moved)]
     for c in copies:
         c.start()
+    shards = (w0,) + tuple(wv.at[i] for i in range(7))
 
     def lower(c, start, stop):
-        return wv[2 * c - 2, start:stop, :] if c else low[start:stop, :]
+        return shards[2 * c][start:stop, :]
 
     def upper(c, start, stop):
-        start, stop = start - RELAYED, stop - RELAYED
-        return wv[2 * c - 1, start:stop, :] if c else high[start:stop, :]
+        return shards[2 * c + 1][start - RELAYED : stop - RELAYED, :]
 
     tokens = side([rows[i] for i in range(4)])
     hidden = []
     for c in range(4):
-        if c:
-            copies[2 * c - 2].wait()
-            copies[2 * c - 1].wait()
+        for i in ((0,), (1, 2), (3, 4), (5, 6))[c]:
+            copies[i].wait()
         ups = [lower(c, UP_AT, RELAYED), upper(c, RELAYED, DOWN_AT)]
         both = side([lower(c, 0, UP_AT), jnp.concatenate(ups, axis=0)])
         parts = jnp.dot(tokens, both, preferred_element_type=F32)
@@ -262,7 +264,7 @@
         part_v[b] = part[:, :LANES]
         part_v[b + 1] = part[:, LANES:]
         target = out.at[pl.ds(b, 2), pl.ds(0, ROUTED_ROWS), :]
-        sends.append(pltpu.make_async_copy(part_v.at[pl.ds(b, 2)], target, sems.at[6 + b // 2]))
+        sends.append(pltpu.make_async_copy(part_v.at[pl.ds(b, 2)], target, sems.at[7 + b // 2]))
         sends[-1].start()
     for c in sends:
         c.wait()
@@ -427,6 +429,7 @@
         out_specs=[VMEM] * 3,
         scratch_shapes=[
             pltpu.VMEM((4, QUARTER, QUARTER), BF16),
+            pltpu.VMEM((4, TOKENS_HERE, QUARTER), BF16),
             pltpu.VMEM((4, TOKENS_HERE, QUARTER), F32),
             pltpu.SemaphoreType.DMA((4,)),
         ],
@@ -475,12 +478,12 @@
     partial = kernel(
         expert_body,
         out_shape=struct((16, ROUTED_ROWS + SHARED_ROWS, LANES), BF16),
-        in_specs=[HELD] * 3 + [HBM] * 7,
+        in_specs=[HELD] * 2 + [HBM] * 8,
         out_specs=HBM,
         scratch_shapes=[
-            pltpu.VMEM((6, RELAYED, LANES), BF16),
+            pltpu.VMEM((7, RELAYED, LANES), BF16),
             pltpu.VMEM((16, ROUTED_ROWS, LANES), BF16),
-            pltpu.SemaphoreType.DMA((14,)),
+            pltpu.SemaphoreType.DMA((15,)),
         ],
         input_output_aliases={9: 0},
     )(

time: 193 us -> 192 us (level)
  no operation moved by 1% of the time
where the time goes in v3:
time: 192 us; the launch traced here: 191 us
  starting transfers between devices  76.3 us (40%)
  waiting for transfers between devices  56.9 us (30%)
  blocking collectives  33.2 us (17%)
  Pallas kernels  24.2 us (13%)
    all_to_all x4, starting transfers between devices, exchange(): return lax.all_to_all(parts, axes, split_axis=0, concat_axis=0, tiled=True)  42.9 us
    all_to_all x2, blocking collectives, exchange(): return lax.all_to_all(parts, axes, split_axis=0, concat_axis=0, tiled=True)  33.2 us
    all_to_all x4, waiting for transfers between devices, exchange(): return lax.all_to_all(parts, axes, split_axis=0, concat_axis=0, tiled=True)  32.8 us
    pallas_call x10, Pallas kernels, run(): return call(*args)  24.2 us
    ppermute x6, waiting for transfers between devices, around(): return lax.ppermute(shard, 'x', [(i, (i + by) % 4) for i in range(4)])  21.3 us
    ppermute x6, starting transfers between devices, around(): return lax.ppermute(shard, 'x', [(i, (i + by) % 4) for i in range(4)])  19.5 us
    ppermute x1, starting transfers between devices, layer(): halo = lax.ppermute(tail, 'sp', following)  7.44 us
    ppermute x1, starting transfers between devices, layer(): from_core = lax.ppermute(from_pair, 'sp', cores)  4.53 us
  transfers between devices with their start and end apart: 13, of which 7 were waited for; matrix products, arithmetic and copies ran while one was open for 0% of the time, Pallas kernels for 5%

profile of v3, /device:TPU:1, one launch (start us, length us, event | category | flops | bytes accessed | tf_op | source)
XLA Modules:
  0.0 191.3 jit_solution(11172897821122580529)
XLA Ops:
  0.0 2.0 %shard_map.154 = bf16[16,256,128]{2,1,0:T(8,128)(2,1)} custom-call(bf16[256,128]{1,0:T(8,128)(2,1)} %shard.1), custom_call_target="tpu_custom_call" | custom-call | tf_op jit(solution)/shard_map/pallas_call | solution.py:359
  2.0 0.0 copy-start.5
  2.0 0.0 copy-start
  2.0 0.0 copy-start.1
  2.0 0.0 copy-start.2
  2.0 0.0 copy-start.3
  2.0 7.7 %all-to-all-start = ((bf16[16,256,128]{2,1,0:T(8,128)(2,1)}), bf16[16,256,128]{2,1,0:T(8,128)(2,1)S(1)}, u32[]{:S(2)}, u32[]{:S(2)}) async-start(bf16[16,256,128]{2,1,0:T(8,128)(2,1)} %shard_map.154), calls=%async_computation | async-start | bytes 2097152 | tf_op jit(solution)/shard_map/all_to_all | solution.py:342
  9.8 0.0 copy-done.5
  9.8 0.1 add_convert_fusion
  9.9 14.5 %all-to-all-done.near = bf16[16,256,128]{2,1,0:T(8,128)(2,1)S(1)} async-done(((bf16[16,256,128]{2,1,0:T(8,128)(2,1)}), bf16[16,256,128]{2,1,0:T(8,128)(2,1)S(1)}, u32[]{:S(2)}, u32[]{:S(2)}) %all-to-all-start) | async-done | bytes 1048608 | tf_op jit(solution)/shard_map/all_to_all | solution.py:342
  24.4 0.1 broadcast_in_dim_broadcast_in_dim.2
  24.5 7.4 %collective-permute-start = (bf16[17,16,128]{2,1,0:T(8,128)(2,1)S(1)}, bf16[17,16,128]{2,1,0:T(8,128)(2,1)S(1)}, u32[]{:S(2)}, u32[]{:S(2)}) collective-permute-start(bf16[17,16,128]{2,1,0:T(8,128)(2,1)S(1)} %pad_maximum_fusion), channel_id=1, source_target_pairs={{0,16},{16,32},{32,48},{48,64},{64,80},{80,96},{96,112},{112,128},... | collective-permute-start | bytes 208904 | tf_op jit(solution)/shard_map/ppermute | solution.py:421
  31.9 0.1 pad_add_fusion.at
  32.0 1.3 collective-permute-done.halo
  33.3 0.0 copy-done.3
  33.3 5.7 %shard_map.155 = (bf16[256,512]{1,0:T(8,128)(2,1)}, bf16[4,256,512]{2,1,0:T(8,128)(2,1)S(1)}, bf16[256,128]{1,0:T(8,128)(2,1)S(1)}) custom-call(s32[3]{0:T(128)S(1)} %pad_add_fusion.at, s32[1,256]{1,0:T(1,128)S(1)} %bitcast.28, s32[2,256]{1,0:T(2,128)S(1)} %bitcast.25, f32[1,2048]{1,0:T(1,128)S(1)} %bitcast.22, f32[1,2048]{1,0:T(1,128)S(1)} %bitcast.23, ...), custom_call_target="tpu_custom_call" | custom-call | tf_op jit(solution)/shard_map/pallas_call | solution.py:359
  39.0 17.3 %all-to-all-start.1 = ((bf16[32,8,512]{2,1,0:T(8,128)(2,1)}), bf16[32,8,512]{2,1,0:T(8,128)(2,1)S(1)}, u32[]{:S(2)}, u32[]{:S(2)}) async-start(bf16[32,8,512]{2,1,0:T(8,128)(2,1)} %bitcast.36), calls=%async_computation.1 | async-start | bytes 524288 | tf_op jit(solution)/shard_map/all_to_all | solution.py:342
  56.3 3.8 %shard_map.157 = (bf16[3072,128]{1,0:T(8,128)(2,1)S(1)}, bf16[3072,128]{1,0:T(8,128)(2,1)}, bf16[192,2048]{1,0:T(8,128)(2,1)}, bf16[96,2048]{1,0:T(8,128)(2,1)}) custom-call(s32[3]{0:T(128)S(1)} %pad_add_fusion.at, bf16[2048,128]{1,0:T(8,128)(2,1)} %bitcast.31, bf16[2048,128]{1,0:T(8,128)(2,1)} %bitcast.32, bf16[128,2048]{1,0:T(8,128)(2,1)} %bitcast.33, ...), custom_call_target="tpu_custom_call" | custom-call | flops 10000000 | bytes 3145728 | tf_op jit(solution)/shard_map/pallas_call | solution.py:359
  60.1 1.9 %collective-permute-start.1 = (bf16[3072,128]{1,0:T(8,128)(2,1)S(1)}, bf16[3072,128]{1,0:T(8,128)(2,1)S(1)}, u32[]{:S(2)}, u32[]{:S(2)}) collective-permute-start(bf16[3072,128]{1,0:T(8,128)(2,1)S(1)} %get-tuple-element.19.w0), channel_id=1, source_target_pairs={{0,1},{1,2},{2,3},{3,0},{4,5},{5,6},{6,7},{7,4},{8,9},{9,10},{10,1... | collective-permute-start | bytes 2359304 | tf_op jit(solution)/shard_map/ppermute | solution.py:346
  62.0 4.6 %collective-permute-start.4 = (bf16[3072,128]{1,0:T(8,128)(2,1)}, bf16[3072,128]{1,0:T(8,128)(2,1)}, u32[]{:S(2)}, u32[]{:S(2)}) collective-permute-start(bf16[3072,128]{1,0:T(8,128)(2,1)} %get-tuple-element.20.w1), channel_id=1, source_target_pairs={{0,3},{1,0},{2,1},{3,2},{4,7},{5,4},{6,5},{7,6},{8,11},{9,8},{10,9... | collective-permute-start | bytes 2359304 | tf_op jit(solution)/shard_map/ppermute | solution.py:346
  66.6 1.9 %collective-permute-start.7 = (bf16[96,2048]{1,0:T(8,128)(2,1)}, bf16[96,2048]{1,0:T(8,128)(2,1)}, u32[]{:S(2)}, u32[]{:S(2)}) collective-permute-start(bf16[96,2048]{1,0:T(8,128)(2,1)} %get-tuple-element.23), channel_id=1, source_target_pairs={{0,4},{4,0},{8,12},{12,8},{1,5},{5,1},{9,13},{13,9},{2,6},{6,2},{1... | collective-permute-start | bytes 1179656 | tf_op jit(solution)/shard_map/ppermute | solution.py:452
  68.6 1.9 %collective-permute-start.2 = (bf16[3072,128]{1,0:T(8,128)(2,1)}, bf16[3072,128]{1,0:T(8,128)(2,1)}, u32[]{:S(2)}, u32[]{:S(2)}) collective-permute-start(bf16[3072,128]{1,0:T(8,128)(2,1)} %get-tuple-element.20.w1), channel_id=1, source_target_pairs={{0,1},{1,2},{2,3},{3,0},{4,5},{5,6},{6,7},{7,4},{8,9},{9,10},{10,1... | collective-permute-start | bytes 2359304 | tf_op jit(solution)/shard_map/ppermute | solution.py:346
  70.5 4.6 %collective-permute-start.3 = (bf16[3072,128]{1,0:T(8,128)(2,1)S(1)}, bf16[3072,128]{1,0:T(8,128)(2,1)}, u32[]{:S(2)}, u32[]{:S(2)}) collective-permute-start(bf16[3072,128]{1,0:T(8,128)(2,1)S(1)} %get-tuple-element.19.w0), channel_id=1, source_target_pairs={{0,3},{1,0},{2,1},{3,2},{4,7},{5,4},{6,5},{7,6},{8,11},{9,8},{10,9... | collective-permute-start | bytes 2359304 | tf_op jit(solution)/shard_map/ppermute | solution.py:346
  75.1 7.0 %collective-permute-done.1.w2 = bf16[3072,128]{1,0:T(8,128)(2,1)S(1)} collective-permute-done((bf16[3072,128]{1,0:T(8,128)(2,1)S(1)}, bf16[3072,128]{1,0:T(8,128)(2,1)S(1)}, u32[]{:S(2)}, u32[]{:S(2)}) %collective-permute-start.1) | collective-permute-done | bytes 786464 | tf_op jit(solution)/shard_map/ppermute | solution.py:346
  82.1 1.9 collective-permute-start.5
  84.0 0.0 collective-permute-done.4.w5
  84.0 4.6 %collective-permute-start.6 = (bf16[3072,128]{1,0:T(8,128)(2,1)}, bf16[3072,128]{1,0:T(8,128)(2,1)}, u32[]{:S(2)}, u32[]{:S(2)}) collective-permute-start(bf16[3072,128]{1,0:T(8,128)(2,1)} %collective-permute-done.4.w5), channel_id=1, source_target_pairs={{0,3},{1,0},{2,1},{3,2},{4,7},{5,4},{6,5},{7,6},{8,11},{9,8},{10,9... | collective-permute-start | bytes 2359304 | tf_op jit(solution)/shard_map/ppermute | solution.py:346
  88.6 0.0 all-to-all-done.1
  88.6 1.2 shard_map.156
  89.8 3.5 %all-to-all-start.2 = ((bf16[4,192,512]{2,1,0:T(8,128)(2,1)}), bf16[4,192,512]{2,1,0:T(8,128)(2,1)S(1)}, u32[]{:S(2)}, u32[]{:S(2)}) async-start(bf16[4,192,512]{2,1,0:T(8,128)(2,1)} %shard_map.156), calls=%async_computation.2 | async-start | bytes 1572864 | tf_op jit(solution)/shard_map/all_to_all | solution.py:342
  93.3 0.0 collective-permute-done.7.s1
  93.3 4.5 %collective-permute-start.8 = (bf16[96,2048]{1,0:T(8,128)(2,1)}, bf16[96,2048]{1,0:T(8,128)(2,1)S(1)}, u32[]{:S(2)}, u32[]{:S(2)}) collective-permute-start(bf16[96,2048]{1,0:T(8,128)(2,1)} %collective-permute-done.7.s1), channel_id=1, source_target_pairs={{0,16},{16,0},{32,48},{48,32},{64,80},{80,64},{96,112},{112,96},{1... | collective-permute-start | bytes 1179656 | tf_op jit(solution)/shard_map/ppermute | solution.py:454
  97.9 1.5 collective-permute-done.8.s2
  99.4 3.3 %shard_map.158.begun = bf16[16,320,128]{2,1,0:T(8,128)(2,1)} custom-call(s32[3]{0:T(128)S(1)} %pad_add_fusion.at, bf16[4,256,512]{2,1,0:T(8,128)(2,1)S(1)} %get-tuple-element.21.normed, bf16[192,2048]{1,0:T(8,128)(2,1)} %get-tuple-element.22.s0, bf16[96,2048]{1,0:T(8,128)(2,1)} %collective-permute-done.7.s1, bf16[96,2048]{1,0:T(8,128)(2,1)S(1)} %collective-permute-done.8.s2), custom_call_target="tpu_custom_call" | custom-call | tf_op jit(solution)/shard_map/pallas_call | solution.py:359
  102.7 0.0 collective-permute-done.2.w3
  102.7 0.0 collective-permute-done.3.w4
  102.7 13.1 %collective-permute-done.5.w6 = bf16[3072,128]{1,0:T(8,128)(2,1)} collective-permute-done((bf16[3072,128]{1,0:T(8,128)(2,1)S(1)}, bf16[3072,128]{1,0:T(8,128)(2,1)}, u32[]{:S(2)}, u32[]{:S(2)}) %collective-permute-start.5) | collective-permute-done | bytes 786464 | tf_op jit(solution)/shard_map/ppermute | solution.py:346
  115.9 1.1 collective-permute-done.6.w7
  117.0 0.0 all-to-all-done.2.rows
  117.0 4.7 %shard_map.159 = bf16[16,320,128]{2,1,0:T(8,128)(2,1)} custom-call(bf16[4,192,512]{2,1,0:T(8,128)(2,1)S(1)} %all-to-all-done.2.rows, bf16[3072,128]{1,0:T(8,128)(2,1)S(1)} %get-tuple-element.19.w0, bf16[3072,128]{1,0:T(8,128)(2,1)} %get-tuple-element.20.w1, bf16[3072,128]{1,0:T(8,128)(2,1)} %copy-done.8, ...), custom_call_target="tpu_custom_call", output_to_operand_aliasing={{}: (9, {})} | custom-call | tf_op jit(solution)/shard_map/pallas_call | solution.py:359
  121.7 23.4 %all_to_all.30.parts = bf16[16,320,128]{2,1,0:T(8,128)(2,1)S(1)} all-to-all(bf16[16,320,128]{2,1,0:T(8,128)(2,1)} %shard_map.159), channel_id=1, replica_groups=mesh['sp'=32,'y'=4,'x'=4] {'y','x'}, dimensions={0} | all-to-all | bytes 2621440 | tf_op jit(solution)/shard_map/all_to_all | solution.py:342
  145.1 1.3 shard_map.160
  146.3 14.3 %all-to-all-start.4 = ((bf16[32,24,128]{2,1,0:T(8,128)(2,1)}), bf16[32,24,128]{2,1,0:T(8,128)(2,1)S(1)}, u32[]{:S(2)}, u32[]{:S(2)}) async-start(bf16[32,24,128]{2,1,0:T(8,128)(2,1)} %bitcast.37), calls=%async_computation.4 | async-start | bytes 393216 | tf_op jit(solution)/shard_map/all_to_all | solution.py:342
  160.7 0.5 shard_map.161
  161.2 18.3 %all-to-all-done.4 = bf16[32,24,128]{2,1,0:T(8,128)(2,1)S(1)} async-done(((bf16[32,24,128]{2,1,0:T(8,128)(2,1)}), bf16[32,24,128]{2,1,0:T(8,128)(2,1)S(1)}, u32[]{:S(2)}, u32[]{:S(2)}) %all-to-all-start.4) | async-done | bytes 196640 | tf_op jit(solution)/shard_map/all_to_all | solution.py:342
  179.5 1.1 shard_map.162
  180.6 9.9 %all_to_all.31.stats = f32[16,2,256]{2,1,0:T(2,128)S(1)} all-to-all(f32[16,2,256]{2,1,0:T(2,128)} %get-tuple-element.30), channel_id=1, replica_groups=mesh['sp'=32,'y'=4,'x'=4] {'y','x'}, dimensions={0} | all-to-all | bytes 65536 | tf_op jit(solution)/shard_map/all_to_all | solution.py:342
  190.5 0.8 shard_map.163
  (13 shorter events, 0.0 us)
Async XLA Ops:
  2.0 7.8 %copy-start.5 = (s32[256]{0:T(256)S(1)}, s32[256]{0:T(256)}, u32[]{:S(2)}) copy-start(s32[256]{0:T(256)} %param.17) | copy-start | bytes 3076
  2.0 31.3 %copy-start = (f32[2048]{0:T(1024)S(1)}, f32[2048]{0:T(1024)}, u32[]{:S(2)}) copy-start(f32[2048]{0:T(1024)} %param.21) | copy-start | bytes 24580
  2.0 31.3 %copy-start.1 = (f32[2048]{0:T(1024)S(1)}, f32[2048]{0:T(1024)}, u32[]{:S(2)}) copy-start(f32[2048]{0:T(1024)} %param.22) | copy-start | bytes 24580
  2.0 31.3 %copy-start.2 = (f32[2048]{0:T(1024)S(1)}, f32[2048]{0:T(1024)}, u32[]{:S(2)}) copy-start(f32[2048]{0:T(1024)} %param.23) | copy-start | bytes 24580
  2.0 31.3 %copy-start.3 = (s32[256,2]{0,1:T(2,128)S(1)}, s32[256,2]{0,1:T(2,128)}, u32[]{:S(2)}) copy-start(s32[256,2]{0,1:T(2,128)} %param.18) | copy-start | bytes 6148
  2.0 22.3 %all-to-all-start = ((bf16[16,256,128]{2,1,0:T(8,128)(2,1)}), bf16[16,256,128]{2,1,0:T(8,128)(2,1)S(1)}, u32[]{:S(2)}, u32[]{:S(2)}) async-start(bf16[16,256,128]{2,1,0:T(8,128)(2,1)} %shard_map.154), calls=%async_computation | async-start | bytes 2097152 | tf_op jit(solution)/shard_map/all_to_all | solution.py:342
  24.5 8.8 %collective-permute-start = (bf16[17,16,128]{2,1,0:T(8,128)(2,1)S(1)}, bf16[17,16,128]{2,1,0:T(8,128)(2,1)S(1)}, u32[]{:S(2)}, u32[]{:S(2)}) collective-permute-start(bf16[17,16,128]{2,1,0:T(8,128)(2,1)S(1)} %pad_maximum_fusion), channel_id=1, source_target_pairs={{0,16},{16,32},{32,48},{48,64},{64,80},{80,96},{96,112},{112,128},... | collective-permute-start | bytes 208904 | tf_op jit(solution)/shard_map/ppermute | solution.py:421
  39.0 49.6 %all-to-all-start.1 = ((bf16[32,8,512]{2,1,0:T(8,128)(2,1)}), bf16[32,8,512]{2,1,0:T(8,128)(2,1)S(1)}, u32[]{:S(2)}, u32[]{:S(2)}) async-start(bf16[32,8,512]{2,1,0:T(8,128)(2,1)} %bitcast.36), calls=%async_computation.1 | async-start | bytes 524288 | tf_op jit(solution)/shard_map/all_to_all | solution.py:342
  60.1 22.0 %collective-permute-start.1 = (bf16[3072,128]{1,0:T(8,128)(2,1)S(1)}, bf16[3072,128]{1,0:T(8,128)(2,1)S(1)}, u32[]{:S(2)}, u32[]{:S(2)}) collective-permute-start(bf16[3072,128]{1,0:T(8,128)(2,1)S(1)} %get-tuple-element.19.w0), channel_id=1, source_target_pairs={{0,1},{1,2},{2,3},{3,0},{4,5},{5,6},{6,7},{7,4},{8,9},{9,10},{10,1... | collective-permute-start | bytes 2359304 | tf_op jit(solution)/shard_map/ppermute | solution.py:346
  62.0 22.0 %collective-permute-start.4 = (bf16[3072,128]{1,0:T(8,128)(2,1)}, bf16[3072,128]{1,0:T(8,128)(2,1)}, u32[]{:S(2)}, u32[]{:S(2)}) collective-permute-start(bf16[3072,128]{1,0:T(8,128)(2,1)} %get-tuple-element.20.w1), channel_id=1, source_target_pairs={{0,3},{1,0},{2,1},{3,2},{4,7},{5,4},{6,5},{7,6},{8,11},{9,8},{10,9... | collective-permute-start | bytes 2359304 | tf_op jit(solution)/shard_map/ppermute | solution.py:346
  66.6 26.7 %collective-permute-start.7 = (bf16[96,2048]{1,0:T(8,128)(2,1)}, bf16[96,2048]{1,0:T(8,128)(2,1)}, u32[]{:S(2)}, u32[]{:S(2)}) collective-permute-start(bf16[96,2048]{1,0:T(8,128)(2,1)} %get-tuple-element.23), channel_id=1, source_target_pairs={{0,4},{4,0},{8,12},{12,8},{1,5},{5,1},{9,13},{13,9},{2,6},{6,2},{1... | collective-permute-start | bytes 1179656 | tf_op jit(solution)/shard_map/ppermute | solution.py:452
  68.6 34.2 %collective-permute-start.2 = (bf16[3072,128]{1,0:T(8,128)(2,1)}, bf16[3072,128]{1,0:T(8,128)(2,1)}, u32[]{:S(2)}, u32[]{:S(2)}) collective-permute-start(bf16[3072,128]{1,0:T(8,128)(2,1)} %get-tuple-element.20.w1), channel_id=1, source_target_pairs={{0,1},{1,2},{2,3},{3,0},{4,5},{5,6},{6,7},{7,4},{8,9},{9,10},{10,1... | collective-permute-start | bytes 2359304 | tf_op jit(solution)/shard_map/ppermute | solution.py:346
  70.5 32.3 %collective-permute-start.3 = (bf16[3072,128]{1,0:T(8,128)(2,1)S(1)}, bf16[3072,128]{1,0:T(8,128)(2,1)}, u32[]{:S(2)}, u32[]{:S(2)}) collective-permute-start(bf16[3072,128]{1,0:T(8,128)(2,1)S(1)} %get-tuple-element.19.w0), channel_id=1, source_target_pairs={{0,3},{1,0},{2,1},{3,2},{4,7},{5,4},{6,5},{7,6},{8,11},{9,8},{10,9... | collective-permute-start | bytes 2359304 | tf_op jit(solution)/shard_map/ppermute | solution.py:346
  82.1 7.7 %copy-start.8 = (bf16[3072,128]{1,0:T(8,128)(2,1)}, bf16[3072,128]{1,0:T(8,128)(2,1)S(1)}, u32[]{:S(2)}) copy-start(bf16[3072,128]{1,0:T(8,128)(2,1)S(1)} %collective-permute-done.1.w2) | copy-start | bytes 2359300
  82.1 33.8 %collective-permute-start.5 = (bf16[3072,128]{1,0:T(8,128)(2,1)S(1)}, bf16[3072,128]{1,0:T(8,128)(2,1)}, u32[]{:S(2)}, u32[]{:S(2)}) collective-permute-start(bf16[3072,128]{1,0:T(8,128)(2,1)S(1)} %collective-permute-done.1.w2), channel_id=1, source_target_pairs={{0,1},{1,2},{2,3},{3,0},{4,5},{5,6},{6,7},{7,4},{8,9},{9,10},{10,1... | collective-permute-start | bytes 2359304 | tf_op jit(solution)/shard_map/ppermute | solution.py:346
  84.0 33.0 %collective-permute-start.6 = (bf16[3072,128]{1,0:T(8,128)(2,1)}, bf16[3072,128]{1,0:T(8,128)(2,1)}, u32[]{:S(2)}, u32[]{:S(2)}) collective-permute-start(bf16[3072,128]{1,0:T(8,128)(2,1)} %collective-permute-done.4.w5), channel_id=1, source_target_pairs={{0,3},{1,0},{2,1},{3,2},{4,7},{5,4},{6,5},{7,6},{8,11},{9,8},{10,9... | collective-permute-start | bytes 2359304 | tf_op jit(solution)/shard_map/ppermute | solution.py:346
  89.8 27.2 %all-to-all-start.2 = ((bf16[4,192,512]{2,1,0:T(8,128)(2,1)}), bf16[4,192,512]{2,1,0:T(8,128)(2,1)S(1)}, u32[]{:S(2)}, u32[]{:S(2)}) async-start(bf16[4,192,512]{2,1,0:T(8,128)(2,1)} %shard_map.156), calls=%async_computation.2 | async-start | bytes 1572864 | tf_op jit(solution)/shard_map/all_to_all | solution.py:342
  93.3 6.1 %collective-permute-start.8 = (bf16[96,2048]{1,0:T(8,128)(2,1)}, bf16[96,2048]{1,0:T(8,128)(2,1)S(1)}, u32[]{:S(2)}, u32[]{:S(2)}) collective-permute-start(bf16[96,2048]{1,0:T(8,128)(2,1)} %collective-permute-done.7.s1), channel_id=1, source_target_pairs={{0,16},{16,0},{32,48},{48,32},{64,80},{80,64},{96,112},{112,96},{1... | collective-permute-start | bytes 1179656 | tf_op jit(solution)/shard_map/ppermute | solution.py:454
  145.1 15.6 %copy-start.4 = (f32[256,2]{0,1:T(2,128)S(1)}, f32[256,2]{0,1:T(2,128)}, u32[]{:S(2)}) copy-start(f32[256,2]{0,1:T(2,128)} %param.19) | copy-start | bytes 6148
  145.1 45.4 %copy-start.6 = (f32[128]{0:T(128)S(1)}, f32[128]{0:T(128)}, u32[]{:S(2)}) copy-start(f32[128]{0:T(128)} %param.30) | copy-start | bytes 1540
  145.1 45.4 %copy-start.7 = (f32[128]{0:T(128)S(1)}, f32[128]{0:T(128)}, u32[]{:S(2)}) copy-start(f32[128]{0:T(128)} %param.31) | copy-start | bytes 1540
  146.3 33.1 %all-to-all-start.4 = ((bf16[32,24,128]{2,1,0:T(8,128)(2,1)}), bf16[32,24,128]{2,1,0:T(8,128)(2,1)S(1)}, u32[]{:S(2)}, u32[]{:S(2)}) async-start(bf16[32,24,128]{2,1,0:T(8,128)(2,1)} %bitcast.37), calls=%async_computation.4 | async-start | bytes 393216 | tf_op jit(solution)/shard_map/all_to_all | solution.py:342

commit v4 on v3

--- a/solution.py
+++ b/solution.py
@@ -41,10 +41,6 @@
 
 def side(parts):
     return jnp.concatenate(parts, axis=1)
-
-
-def four(a):
-    return jnp.concatenate([a, a, a, a], axis=1)
 
 
 def as_column(row):
@@ -132,47 +128,60 @@
     weight_v,
     mixed_v,
     first_v,
+    quarter_v,
+    send_v,
     sems,
 ):
     y, x = at[0], at[1]
     copies = [pltpu.make_async_copy(weight.at[g], weight_v.at[g], sems.at[g]) for g in range(4)]
     for c in copies:
         c.start()
-    marks = jnp.concatenate(
-        [halo[16].astype(F32), as_column((docs[...] + 1).astype(F32))], axis=0
-    )
-    members = jnp.ones(marks.shape, F32)
-    insides, counts = [], []
-    for step in range(4):
-        inside = jnp.where(pltpu.roll(marks, 1 << step, 0) == marks, 1.0, 0.0)
-        members = members + inside * pltpu.roll(members, 1 << step, 0)
-        insides.append(four(inside))
-        counts.append(four(1.0 / members[HALO:]))
+    own_row = (docs[...] + 1).astype(F32)
+    own_marks = as_column(own_row)
+    halo_row = halo[16].astype(F32).T[0:1]
+    apart = iota((TOKENS_HERE, TOKENS_HERE), 0) - iota((TOKENS_HERE, TOKENS_HERE), 1)
+    inside = (side([own_marks, own_marks]) == own_row) & (apart >= 0)
+    corner = iota((HALO, HALO), 0) - iota((HALO, HALO), 1) + HALO
+    corner_inside = own_marks[0:HALO, 0:HALO] == halo_row
     for g in range(4):
-        head = side([halo[4 * g + i] for i in range(4)]).astype(F32)
-        mine = side([near[4 * g + i] for i in range(4)]).astype(F32)
-        running = jnp.concatenate([head, mine], axis=0)
-        for step in range(g + 1):
-            running = running + insides[step] * pltpu.roll(running, 1 << step, 0)
-        mixed_v[g] = (running[HALO:] * counts[g] - mine).astype(BF16)
+        window = 2 << g
+        band = jnp.where(inside & (apart < window), 1.0, 0.0)
+        edge = jnp.where(corner_inside & (corner < window), 1.0, 0.0)
+        members = jnp.sum(band, axis=1, keepdims=True)
+        first_members = members[0:HALO] + jnp.sum(edge, axis=1, keepdims=True)
+        scale_by = 1.0 / jnp.concatenate([first_members, members[HALO:]], axis=0)
+        band, edge = band.astype(BF16), edge.astype(BF16)
+        for j in range(2):
+            at_lane = slice(j * 2 * LANES, (j + 1) * 2 * LANES)
+            mine = side([near[4 * g + 2 * j], near[4 * g + 2 * j + 1]])
+            head = side([halo[4 * g + 2 * j], halo[4 * g + 2 * j + 1]])
+            running = jnp.dot(band, mine, preferred_element_type=F32)
+            begin = running[0:HALO] + jnp.dot(edge, head, preferred_element_type=F32)
+            running = jnp.concatenate([begin, running[HALO:]], axis=0)
+            mixed_v[g, :, at_lane] = (running * scale_by - mine.astype(F32)).astype(BF16)
     total = jnp.zeros((TOKENS_HERE, 1), F32)
     squares = jnp.zeros((TOKENS_HERE, 1), F32)
     for g in range(4):
-        lanes = slice(g * QUARTER, (g + 1) * QUARTER)
         copies[g].wait()
-        projected = jnp.dot(mixed_v[g], weight_v[g], preferred_element_type=F32)
-        mine = side([near[4 * g + i] for i in range(4)]).astype(F32)
-        first = RESIDUAL_SCALE * mine + projected * scale[:, lanes]
-        first_v[g] = first
-        part, part_squares = sums(first)
-        total = total + part
-        squares = squares + part_squares
+        for j in range(2):
+            at_lane = slice(j * 2 * LANES, (j + 1) * 2 * LANES)
+            lanes = slice(g * QUARTER + j * 2 * LANES, g * QUARTER + (j + 1) * 2 * LANES)
+            projected = jnp.dot(mixed_v[g], weight_v[g, :, at_lane], preferred_element_type=F32)
+            mine = side([near[4 * g + 2 * j], near[4 * g + 2 * j + 1]]).astype(F32)
+            first = RESIDUAL_SCALE * mine + projected * scale[:, lanes]
+            first_v[g, :, at_lane] = first
+            part, part_squares = sums(first)
+            total = total + part
+            squares = squares + part_squares
     mean = total / MODEL
     inv = lax.rsqrt(squares / MODEL - mean * mean + NORM_EPS)
-    for g in range(4):
-        lanes = slice(g * QUARTER, (g + 1) * QUARTER)
-        normed[g] = ((first_v[g] - mean) * inv * gain[:, lanes] + bias[:, lanes]).astype(BF16)
-    quarter = normed[y]
+    lanes = pl.ds(pl.multiple_of(y * QUARTER, QUARTER), QUARTER)
+    gain_here, bias_here = gain[:, lanes], bias[:, lanes]
+    for r in range(0, TOKENS_HERE, 64):
+        rows = slice(r, r + 64)
+        scaled = (first_v[y, rows, :] - mean[rows]) * inv[rows]
+        quarter_v[rows, :] = (scaled * gain_here + bias_here).astype(BF16)
+    quarter = quarter_v[...]
     named = routes[...]
     dests = []
     for k, rank in enumerate(ranks_of(named)):
@@ -180,11 +189,24 @@
         dests.append(jnp.where((rank & 3) == x, slot, -1))
     slot = iota((EXPERTS * SLOTS_SENT, TOKENS_HERE), 0)
     pick = chosen((slot == dests[0]) | (slot == dests[1]))
-    send[...] = jnp.dot(pick, quarter, preferred_element_type=F32).astype(BF16)
+    send_v[...] = jnp.dot(pick, quarter, preferred_element_type=F32).astype(BF16)
+    leave = pltpu.make_async_copy(send_v, send, sems.at[4])
+    leave.start()
     mine = quarter[:, 0:LANES]
     for i in range(1, 4):
         mine = jnp.where(x == i, quarter[:, i * LANES : (i + 1) * LANES], mine)
     own[...] = mine
+    upper = (y & 1) == 1
+    half = pl.multiple_of((y & 1) * SHARED_ROWS, SHARED_ROWS)
+    mean = jnp.where(upper, mean[SHARED_ROWS:], mean[:SHARED_ROWS])
+    inv = jnp.where(upper, inv[SHARED_ROWS:], inv[:SHARED_ROWS])
+    for r in range(0, SHARED_ROWS, 64):
+        rows = slice(r, r + 64)
+        for g in range(4):
+            lanes = slice(g * QUARTER, (g + 1) * QUARTER)
+            scaled = (first_v[g, pl.ds(half + r, 64), :] - mean[rows]) * inv[rows]
+            normed[g, rows, :] = (scaled * gain[:, lanes] + bias[:, lanes]).astype(BF16)
+    leave.wait()
 
 
 def compact_body(rows, out):
@@ -198,15 +220,14 @@
         out[i] = packed
 
 
-def shared_body(at, normed, s0, s1, s2, out, own_v, near_v, far_v, part_v, sems):
+def shared_body(normed, s0, s1, s2, out, own_v, near_v, far_v, part_v, sems):
     copies = [
         pltpu.make_async_copy(source, target, sems.at[i])
         for i, (source, target) in enumerate(((s0, own_v), (s1, near_v), (s2, far_v)))
     ]
     for c in copies:
         c.start()
-    half = pl.multiple_of((at[0] & 1) * SHARED_ROWS, SHARED_ROWS)
-    shared = side([normed[i, pl.ds(half, SHARED_ROWS), :] for i in range(4)])
+    shared = side([normed[i] for i in range(4)])
     for c in copies:
         c.wait()
 
@@ -426,16 +447,18 @@
     send, normed, own = kernel(
         mixer_body,
         in_specs=[SMEM] + [VMEM] * 5 + [HELD, HELD, HBM],
-        out_specs=[VMEM] * 3,
+        out_specs=[HBM, VMEM, VMEM],
         scratch_shapes=[
             pltpu.VMEM((4, QUARTER, QUARTER), BF16),
             pltpu.VMEM((4, TOKENS_HERE, QUARTER), BF16),
             pltpu.VMEM((4, TOKENS_HERE, QUARTER), F32),
-            pltpu.SemaphoreType.DMA((4,)),
+            pltpu.VMEM((TOKENS_HERE, QUARTER), BF16),
+            pltpu.VMEM((EXPERTS * SLOTS_SENT, QUARTER), BF16),
+            pltpu.SemaphoreType.DMA((5,)),
         ],
         out_shape=[
             struct((EXPERTS * SLOTS_SENT, QUARTER), BF16),
-            held((4, TOKENS_HERE, QUARTER), BF16),
+            held((4, SHARED_ROWS, QUARTER), BF16),
             held((TOKENS_HERE, LANES), BF16),
         ],
     )(
@@ -465,7 +488,7 @@
     begun = kernel(
         shared_body,
         out_shape=struct((16, ROUTED_ROWS + SHARED_ROWS, LANES), BF16),
-        in_specs=[SMEM, HELD, HBM, HBM, ANY],
+        in_specs=[HELD, HBM, HBM, ANY],
         out_specs=HBM,
         scratch_shapes=[
             pltpu.VMEM((3 * SHARED_UNITS, MODEL), BF16),
@@ -474,7 +497,7 @@
             pltpu.VMEM((16, SHARED_ROWS, LANES), BF16),
             pltpu.SemaphoreType.DMA((4,)),
         ],
-    )(at, normed, shared_packed, from_pair, from_core)
+    )(normed, shared_packed, from_pair, from_core)
     partial = kernel(
         expert_body,
         out_shape=struct((16, ROUTED_ROWS + SHARED_ROWS, LANES), BF16),

time: 192 us -> 191 us (level)
  transfers between devices with their start and end apart: 13 -> 13, of which waited for: 7 -> 7; matrix products, arithmetic and copies ran while one was open for 0% -> 0% of each run, Pallas kernels for 5% -> 4%
where the time goes in v4:
time: 191 us; the launch traced here: 190 us
  starting transfers between devices  76 us (40%)
  waiting for transfers between devices  57.6 us (30%)
  blocking collectives  33.2 us (17%)
  Pallas kernels  22.4 us (12%)
    all_to_all x4, starting transfers between devices, exchange(): return lax.all_to_all(parts, axes, split_axis=0, concat_axis=0, tiled=True)  42.9 us
    all_to_all x2, blocking collectives, exchange(): return lax.all_to_all(parts, axes, split_axis=0, concat_axis=0, tiled=True)  33.2 us
    all_to_all x4, waiting for transfers between devices, exchange(): return lax.all_to_all(parts, axes, split_axis=0, concat_axis=0, tiled=True)  32.8 us
    pallas_call x10, Pallas kernels, run(): return call(*args)  22.4 us
    ppermute x6, waiting for transfers between devices, around(): return lax.ppermute(shard, 'x', [(i, (i + by) % 4) for i in range(4)])  22.1 us
    ppermute x6, starting transfers between devices, around(): return lax.ppermute(shard, 'x', [(i, (i + by) % 4) for i in range(4)])  19.5 us
    ppermute x1, starting transfers between devices, layer(): halo = lax.ppermute(tail, 'sp', following)  7.44 us
    ppermute x1, starting transfers between devices, layer(): from_core = lax.ppermute(from_pair, 'sp', cores)  4.25 us
  transfers between devices with their start and end apart: 13, of which 7 were waited for; matrix products, arithmetic and copies ran while one was open for 0% of the time, Pallas kernels for 4%

profile of v4, /device:TPU:1, one launch (start us, length us, event | category | flops | bytes accessed | tf_op | source)
XLA Modules:
  0.0 189.7 jit_solution(12379110595735657591)
XLA Ops:
  0.0 2.0 %shard_map.154 = bf16[16,256,128]{2,1,0:T(8,128)(2,1)} custom-call(bf16[256,128]{1,0:T(8,128)(2,1)} %shard.1), custom_call_target="tpu_custom_call" | custom-call | tf_op jit(solution)/shard_map/pallas_call | solution.py:380
  2.0 0.0 copy-start.6
  2.0 0.0 copy-start.1
  2.0 0.0 copy-start.2
  2.0 0.0 copy-start.3
  2.0 0.0 copy-start.4
  2.0 7.7 %all-to-all-start = ((bf16[16,256,128]{2,1,0:T(8,128)(2,1)}), bf16[16,256,128]{2,1,0:T(8,128)(2,1)S(1)}, u32[]{:S(2)}, u32[]{:S(2)}) async-start(bf16[16,256,128]{2,1,0:T(8,128)(2,1)} %shard_map.154), calls=%async_computation | async-start | bytes 2097152 | tf_op jit(solution)/shard_map/all_to_all | solution.py:363
  9.8 0.1 add_convert_fusion
  9.9 14.5 %all-to-all-done.near = bf16[16,256,128]{2,1,0:T(8,128)(2,1)S(1)} async-done(((bf16[16,256,128]{2,1,0:T(8,128)(2,1)}), bf16[16,256,128]{2,1,0:T(8,128)(2,1)S(1)}, u32[]{:S(2)}, u32[]{:S(2)}) %all-to-all-start) | async-done | bytes 1048608 | tf_op jit(solution)/shard_map/all_to_all | solution.py:363
  24.4 0.1 broadcast_in_dim_broadcast_in_dim.2
  24.5 7.4 %collective-permute-start = (bf16[17,16,128]{2,1,0:T(8,128)(2,1)S(1)}, bf16[17,16,128]{2,1,0:T(8,128)(2,1)S(1)}, u32[]{:S(2)}, u32[]{:S(2)}) collective-permute-start(bf16[17,16,128]{2,1,0:T(8,128)(2,1)S(1)} %pad_maximum_fusion), channel_id=1, source_target_pairs={{0,16},{16,32},{32,48},{48,64},{64,80},{80,96},{96,112},{112,128},... | collective-permute-start | bytes 208904 | tf_op jit(solution)/shard_map/ppermute | solution.py:442
  31.9 0.1 pad_add_fusion.at
  32.0 1.3 collective-permute-done.halo
  33.3 0.0 copy-done.3
  33.3 4.6 %shard_map.155 = (bf16[256,512]{1,0:T(8,128)(2,1)}, bf16[4,128,512]{2,1,0:T(8,128)(2,1)S(1)}, bf16[256,128]{1,0:T(8,128)(2,1)S(1)}) custom-call(s32[3]{0:T(128)S(1)} %pad_add_fusion.at, s32[1,256]{1,0:T(1,128)S(1)} %bitcast.28, s32[2,256]{1,0:T(2,128)S(1)} %bitcast.25, f32[1,2048]{1,0:T(1,128)S(1)} %bitcast.22, f32[1,2048]{1,0:T(1,128)S(1)} %bitcast.23, ...), custom_call_target="tpu_custom_call" | custom-call | tf_op jit(solution)/shard_map/pallas_call | solution.py:380
  37.9 17.3 %all-to-all-start.1 = ((bf16[32,8,512]{2,1,0:T(8,128)(2,1)}), bf16[32,8,512]{2,1,0:T(8,128)(2,1)S(1)}, u32[]{:S(2)}, u32[]{:S(2)}) async-start(bf16[32,8,512]{2,1,0:T(8,128)(2,1)} %bitcast.36), calls=%async_computation.1 | async-start | bytes 524288 | tf_op jit(solution)/shard_map/all_to_all | solution.py:363
  55.3 3.5 %shard_map.157 = (bf16[3072,128]{1,0:T(8,128)(2,1)S(1)}, bf16[3072,128]{1,0:T(8,128)(2,1)S(1)}, bf16[192,2048]{1,0:T(8,128)(2,1)}, bf16[96,2048]{1,0:T(8,128)(2,1)}) custom-call(s32[3]{0:T(128)S(1)} %pad_add_fusion.at, bf16[2048,128]{1,0:T(8,128)(2,1)} %bitcast.31, bf16[2048,128]{1,0:T(8,128)(2,1)} %bitcast.32, bf16[128,2048]{1,0:T(8,128)(2,1)} %bitcast.33, ...), custom_call_target="tpu_custom_call" | custom-call | flops 10000000 | bytes 3145728 | tf_op jit(solution)/shard_map/pallas_call | solution.py:380
  58.8 0.0 copy-start
  58.8 1.9 %collective-permute-start.1 = (bf16[3072,128]{1,0:T(8,128)(2,1)S(1)}, bf16[3072,128]{1,0:T(8,128)(2,1)}, u32[]{:S(2)}, u32[]{:S(2)}) collective-permute-start(bf16[3072,128]{1,0:T(8,128)(2,1)S(1)} %get-tuple-element.19.w0), channel_id=1, source_target_pairs={{0,1},{1,2},{2,3},{3,0},{4,5},{5,6},{6,7},{7,4},{8,9},{9,10},{10,1... | collective-permute-start | bytes 2359304 | tf_op jit(solution)/shard_map/ppermute | solution.py:367
  60.7 4.6 %collective-permute-start.4 = (bf16[3072,128]{1,0:T(8,128)(2,1)S(1)}, bf16[3072,128]{1,0:T(8,128)(2,1)}, u32[]{:S(2)}, u32[]{:S(2)}) collective-permute-start(bf16[3072,128]{1,0:T(8,128)(2,1)S(1)} %get-tuple-element.20.w1), channel_id=1, source_target_pairs={{0,3},{1,0},{2,1},{3,2},{4,7},{5,4},{6,5},{7,6},{8,11},{9,8},{10,9... | collective-permute-start | bytes 2359304 | tf_op jit(solution)/shard_map/ppermute | solution.py:367
  65.3 1.9 %collective-permute-start.7 = (bf16[96,2048]{1,0:T(8,128)(2,1)}, bf16[96,2048]{1,0:T(8,128)(2,1)S(1)}, u32[]{:S(2)}, u32[]{:S(2)}) collective-permute-start(bf16[96,2048]{1,0:T(8,128)(2,1)} %get-tuple-element.23), channel_id=1, source_target_pairs={{0,4},{4,0},{8,12},{12,8},{1,5},{5,1},{9,13},{13,9},{2,6},{6,2},{1... | collective-permute-start | bytes 1179656 | tf_op jit(solution)/shard_map/ppermute | solution.py:475
  67.3 1.9 %collective-permute-start.2 = (bf16[3072,128]{1,0:T(8,128)(2,1)S(1)}, bf16[3072,128]{1,0:T(8,128)(2,1)}, u32[]{:S(2)}, u32[]{:S(2)}) collective-permute-start(bf16[3072,128]{1,0:T(8,128)(2,1)S(1)} %get-tuple-element.20.w1), channel_id=1, source_target_pairs={{0,1},{1,2},{2,3},{3,0},{4,5},{5,6},{6,7},{7,4},{8,9},{9,10},{10,1... | collective-permute-start | bytes 2359304 | tf_op jit(solution)/shard_map/ppermute | solution.py:367
  69.2 4.6 %collective-permute-start.3 = (bf16[3072,128]{1,0:T(8,128)(2,1)S(1)}, bf16[3072,128]{1,0:T(8,128)(2,1)}, u32[]{:S(2)}, u32[]{:S(2)}) collective-permute-start(bf16[3072,128]{1,0:T(8,128)(2,1)S(1)} %get-tuple-element.19.w0), channel_id=1, source_target_pairs={{0,3},{1,0},{2,1},{3,2},{4,7},{5,4},{6,5},{7,6},{8,11},{9,8},{10,9... | collective-permute-start | bytes 2359304 | tf_op jit(solution)/shard_map/ppermute | solution.py:367
  73.8 7.1 %collective-permute-done.1.w2 = bf16[3072,128]{1,0:T(8,128)(2,1)} collective-permute-done((bf16[3072,128]{1,0:T(8,128)(2,1)S(1)}, bf16[3072,128]{1,0:T(8,128)(2,1)}, u32[]{:S(2)}, u32[]{:S(2)}) %collective-permute-start.1) | collective-permute-done | bytes 786464 | tf_op jit(solution)/shard_map/ppermute | solution.py:367
  80.9 1.9 %collective-permute-start.5 = (bf16[3072,128]{1,0:T(8,128)(2,1)}, bf16[3072,128]{1,0:T(8,128)(2,1)}, u32[]{:S(2)}, u32[]{:S(2)}) collective-permute-start(bf16[3072,128]{1,0:T(8,128)(2,1)} %collective-permute-done.1.w2), channel_id=1, source_target_pairs={{0,1},{1,2},{2,3},{3,0},{4,5},{5,6},{6,7},{7,4},{8,9},{9,10},{10,1... | collective-permute-start | bytes 2359304 | tf_op jit(solution)/shard_map/ppermute | solution.py:367
  82.8 0.0 collective-permute-done.4.w5
  82.8 4.6 %collective-permute-start.6 = (bf16[3072,128]{1,0:T(8,128)(2,1)}, bf16[3072,128]{1,0:T(8,128)(2,1)}, u32[]{:S(2)}, u32[]{:S(2)}) collective-permute-start(bf16[3072,128]{1,0:T(8,128)(2,1)} %collective-permute-done.4.w5), channel_id=1, source_target_pairs={{0,3},{1,0},{2,1},{3,2},{4,7},{5,4},{6,5},{7,6},{8,11},{9,8},{10,9... | collective-permute-start | bytes 2359304 | tf_op jit(solution)/shard_map/ppermute | solution.py:367
  87.4 0.0 all-to-all-done.1
  87.4 1.2 shard_map.156
  88.6 3.5 %all-to-all-start.2 = ((bf16[4,192,512]{2,1,0:T(8,128)(2,1)}), bf16[4,192,512]{2,1,0:T(8,128)(2,1)S(1)}, u32[]{:S(2)}, u32[]{:S(2)}) async-start(bf16[4,192,512]{2,1,0:T(8,128)(2,1)} %shard_map.156), calls=%async_computation.2 | async-start | bytes 1572864 | tf_op jit(solution)/shard_map/all_to_all | solution.py:363
  92.1 0.0 collective-permute-done.7.s1
  92.1 4.2 %collective-permute-start.8 = (bf16[96,2048]{1,0:T(8,128)(2,1)S(1)}, bf16[96,2048]{1,0:T(8,128)(2,1)S(1)}, u32[]{:S(2)}, u32[]{:S(2)}) collective-permute-start(bf16[96,2048]{1,0:T(8,128)(2,1)S(1)} %collective-permute-done.7.s1), channel_id=1, source_target_pairs={{0,16},{16,0},{32,48},{48,32},{64,80},{80,64},{96,112},{112,96},{1... | collective-permute-start | bytes 1179656 | tf_op jit(solution)/shard_map/ppermute | solution.py:477
  96.4 1.3 collective-permute-done.8.s2
  97.7 2.8 %shard_map.158.begun = bf16[16,320,128]{2,1,0:T(8,128)(2,1)} custom-call(bf16[4,128,512]{2,1,0:T(8,128)(2,1)S(1)} %get-tuple-element.21.normed, bf16[192,2048]{1,0:T(8,128)(2,1)} %get-tuple-element.22.s0, bf16[96,2048]{1,0:T(8,128)(2,1)} %copy-done.9, bf16[96,2048]{1,0:T(8,128)(2,1)S(1)} %collective-permute-done.8.s2), custom_call_target="tpu_custom_call" | custom-call | tf_op jit(solution)/shard_map/pallas_call | solution.py:380
  100.5 0.0 collective-permute-done.2.w3
  100.5 0.0 collective-permute-done.3.w4
  100.5 14.1 %collective-permute-done.5.w6 = bf16[3072,128]{1,0:T(8,128)(2,1)} collective-permute-done((bf16[3072,128]{1,0:T(8,128)(2,1)}, bf16[3072,128]{1,0:T(8,128)(2,1)}, u32[]{:S(2)}, u32[]{:S(2)}) %collective-permute-start.5) | collective-permute-done | bytes 786464 | tf_op jit(solution)/shard_map/ppermute | solution.py:367
  114.6 0.9 collective-permute-done.6.w7
  115.5 0.0 all-to-all-done.2.rows
  115.5 4.7 %shard_map.159 = bf16[16,320,128]{2,1,0:T(8,128)(2,1)} custom-call(bf16[4,192,512]{2,1,0:T(8,128)(2,1)S(1)} %all-to-all-done.2.rows, bf16[3072,128]{1,0:T(8,128)(2,1)S(1)} %get-tuple-element.19.w0, bf16[3072,128]{1,0:T(8,128)(2,1)} %copy-done, bf16[3072,128]{1,0:T(8,128)(2,1)} %collective-permute-done.1.w2, ...), custom_call_target="tpu_custom_call", output_to_operand_aliasing={{}: (9, {})} | custom-call | tf_op jit(solution)/shard_map/pallas_call | solution.py:380
  120.2 23.4 %all_to_all.30.parts = bf16[16,320,128]{2,1,0:T(8,128)(2,1)S(1)} all-to-all(bf16[16,320,128]{2,1,0:T(8,128)(2,1)} %shard_map.159), channel_id=1, replica_groups=mesh['sp'=32,'y'=4,'x'=4] {'y','x'}, dimensions={0} | all-to-all | bytes 2621440 | tf_op jit(solution)/shard_map/all_to_all | solution.py:363
  143.6 1.3 shard_map.160
  144.8 14.4 %all-to-all-start.4 = ((bf16[32,24,128]{2,1,0:T(8,128)(2,1)}), bf16[32,24,128]{2,1,0:T(8,128)(2,1)S(1)}, u32[]{:S(2)}, u32[]{:S(2)}) async-start(bf16[32,24,128]{2,1,0:T(8,128)(2,1)} %bitcast.37), calls=%async_computation.4 | async-start | bytes 393216 | tf_op jit(solution)/shard_map/all_to_all | solution.py:363
  159.2 0.5 shard_map.161
  159.7 18.3 %all-to-all-done.4 = bf16[32,24,128]{2,1,0:T(8,128)(2,1)S(1)} async-done(((bf16[32,24,128]{2,1,0:T(8,128)(2,1)}), bf16[32,24,128]{2,1,0:T(8,128)(2,1)S(1)}, u32[]{:S(2)}, u32[]{:S(2)}) %all-to-all-start.4) | async-done | bytes 196640 | tf_op jit(solution)/shard_map/all_to_all | solution.py:363
  178.0 1.1 shard_map.162
  179.1 9.9 %all_to_all.31.stats = f32[16,2,256]{2,1,0:T(2,128)S(1)} all-to-all(f32[16,2,256]{2,1,0:T(2,128)} %get-tuple-element.30), channel_id=1, replica_groups=mesh['sp'=32,'y'=4,'x'=4] {'y','x'}, dimensions={0} | all-to-all | bytes 65536 | tf_op jit(solution)/shard_map/all_to_all | solution.py:363
  189.0 0.8 shard_map.163
  (15 shorter events, 0.0 us)
Async XLA Ops:
  2.0 7.8 %copy-start.6 = (s32[256]{0:T(256)S(1)}, s32[256]{0:T(256)}, u32[]{:S(2)}) copy-start(s32[256]{0:T(256)} %param.17) | copy-start | bytes 3076
  2.0 31.3 %copy-start.1 = (f32[2048]{0:T(1024)S(1)}, f32[2048]{0:T(1024)}, u32[]{:S(2)}) copy-start(f32[2048]{0:T(1024)} %param.21) | copy-start | bytes 24580
  2.0 31.3 %copy-start.2 = (f32[2048]{0:T(1024)S(1)}, f32[2048]{0:T(1024)}, u32[]{:S(2)}) copy-start(f32[2048]{0:T(1024)} %param.22) | copy-start | bytes 24580
  2.0 31.3 %copy-start.3 = (f32[2048]{0:T(1024)S(1)}, f32[2048]{0:T(1024)}, u32[]{:S(2)}) copy-start(f32[2048]{0:T(1024)} %param.23) | copy-start | bytes 24580
  2.0 31.3 %copy-start.4 = (s32[256,2]{0,1:T(2,128)S(1)}, s32[256,2]{0,1:T(2,128)}, u32[]{:S(2)}) copy-start(s32[256,2]{0,1:T(2,128)} %param.18) | copy-start | bytes 6148
  2.0 22.3 %all-to-all-start = ((bf16[16,256,128]{2,1,0:T(8,128)(2,1)}), bf16[16,256,128]{2,1,0:T(8,128)(2,1)S(1)}, u32[]{:S(2)}, u32[]{:S(2)}) async-start(bf16[16,256,128]{2,1,0:T(8,128)(2,1)} %shard_map.154), calls=%async_computation | async-start | bytes 2097152 | tf_op jit(solution)/shard_map/all_to_all | solution.py:363
  24.5 8.8 %collective-permute-start = (bf16[17,16,128]{2,1,0:T(8,128)(2,1)S(1)}, bf16[17,16,128]{2,1,0:T(8,128)(2,1)S(1)}, u32[]{:S(2)}, u32[]{:S(2)}) collective-permute-start(bf16[17,16,128]{2,1,0:T(8,128)(2,1)S(1)} %pad_maximum_fusion), channel_id=1, source_target_pairs={{0,16},{16,32},{32,48},{48,64},{64,80},{80,96},{96,112},{112,128},... | collective-permute-start | bytes 208904 | tf_op jit(solution)/shard_map/ppermute | solution.py:442
  37.9 49.5 %all-to-all-start.1 = ((bf16[32,8,512]{2,1,0:T(8,128)(2,1)}), bf16[32,8,512]{2,1,0:T(8,128)(2,1)S(1)}, u32[]{:S(2)}, u32[]{:S(2)}) async-start(bf16[32,8,512]{2,1,0:T(8,128)(2,1)} %bitcast.36), calls=%async_computation.1 | async-start | bytes 524288 | tf_op jit(solution)/shard_map/all_to_all | solution.py:363
  58.8 29.8 %copy-start = (bf16[3072,128]{1,0:T(8,128)(2,1)}, bf16[3072,128]{1,0:T(8,128)(2,1)S(1)}, u32[]{:S(2)}) copy-start(bf16[3072,128]{1,0:T(8,128)(2,1)S(1)} %get-tuple-element.20.w1) | copy-start | bytes 2359300
  58.8 22.1 %collective-permute-start.1 = (bf16[3072,128]{1,0:T(8,128)(2,1)S(1)}, bf16[3072,128]{1,0:T(8,128)(2,1)}, u32[]{:S(2)}, u32[]{:S(2)}) collective-permute-start(bf16[3072,128]{1,0:T(8,128)(2,1)S(1)} %get-tuple-element.19.w0), channel_id=1, source_target_pairs={{0,1},{1,2},{2,3},{3,0},{4,5},{5,6},{6,7},{7,4},{8,9},{9,10},{10,1... | collective-permute-start | bytes 2359304 | tf_op jit(solution)/shard_map/ppermute | solution.py:367
  60.7 22.1 %collective-permute-start.4 = (bf16[3072,128]{1,0:T(8,128)(2,1)S(1)}, bf16[3072,128]{1,0:T(8,128)(2,1)}, u32[]{:S(2)}, u32[]{:S(2)}) collective-permute-start(bf16[3072,128]{1,0:T(8,128)(2,1)S(1)} %get-tuple-element.20.w1), channel_id=1, source_target_pairs={{0,3},{1,0},{2,1},{3,2},{4,7},{5,4},{6,5},{7,6},{8,11},{9,8},{10,9... | collective-permute-start | bytes 2359304 | tf_op jit(solution)/shard_map/ppermute | solution.py:367
  65.3 26.8 %collective-permute-start.7 = (bf16[96,2048]{1,0:T(8,128)(2,1)}, bf16[96,2048]{1,0:T(8,128)(2,1)S(1)}, u32[]{:S(2)}, u32[]{:S(2)}) collective-permute-start(bf16[96,2048]{1,0:T(8,128)(2,1)} %get-tuple-element.23), channel_id=1, source_target_pairs={{0,4},{4,0},{8,12},{12,8},{1,5},{5,1},{9,13},{13,9},{2,6},{6,2},{1... | collective-permute-start | bytes 1179656 | tf_op jit(solution)/shard_map/ppermute | solution.py:475
  67.3 33.2 %collective-permute-start.2 = (bf16[3072,128]{1,0:T(8,128)(2,1)S(1)}, bf16[3072,128]{1,0:T(8,128)(2,1)}, u32[]{:S(2)}, u32[]{:S(2)}) collective-permute-start(bf16[3072,128]{1,0:T(8,128)(2,1)S(1)} %get-tuple-element.20.w1), channel_id=1, source_target_pairs={{0,1},{1,2},{2,3},{3,0},{4,5},{5,6},{6,7},{7,4},{8,9},{9,10},{10,1... | collective-permute-start | bytes 2359304 | tf_op jit(solution)/shard_map/ppermute | solution.py:367
  69.2 31.3 %collective-permute-start.3 = (bf16[3072,128]{1,0:T(8,128)(2,1)S(1)}, bf16[3072,128]{1,0:T(8,128)(2,1)}, u32[]{:S(2)}, u32[]{:S(2)}) collective-permute-start(bf16[3072,128]{1,0:T(8,128)(2,1)S(1)} %get-tuple-element.19.w0), channel_id=1, source_target_pairs={{0,3},{1,0},{2,1},{3,2},{4,7},{5,4},{6,5},{7,6},{8,11},{9,8},{10,9... | collective-permute-start | bytes 2359304 | tf_op jit(solution)/shard_map/ppermute | solution.py:367
  80.9 33.7 %collective-permute-start.5 = (bf16[3072,128]{1,0:T(8,128)(2,1)}, bf16[3072,128]{1,0:T(8,128)(2,1)}, u32[]{:S(2)}, u32[]{:S(2)}) collective-permute-start(bf16[3072,128]{1,0:T(8,128)(2,1)} %collective-permute-done.1.w2), channel_id=1, source_target_pairs={{0,1},{1,2},{2,3},{3,0},{4,5},{5,6},{6,7},{7,4},{8,9},{9,10},{10,1... | collective-permute-start | bytes 2359304 | tf_op jit(solution)/shard_map/ppermute | solution.py:367
  82.8 32.7 %collective-permute-start.6 = (bf16[3072,128]{1,0:T(8,128)(2,1)}, bf16[3072,128]{1,0:T(8,128)(2,1)}, u32[]{:S(2)}, u32[]{:S(2)}) collective-permute-start(bf16[3072,128]{1,0:T(8,128)(2,1)} %collective-permute-done.4.w5), channel_id=1, source_target_pairs={{0,3},{1,0},{2,1},{3,2},{4,7},{5,4},{6,5},{7,6},{8,11},{9,8},{10,9... | collective-permute-start | bytes 2359304 | tf_op jit(solution)/shard_map/ppermute | solution.py:367
  88.6 26.9 %all-to-all-start.2 = ((bf16[4,192,512]{2,1,0:T(8,128)(2,1)}), bf16[4,192,512]{2,1,0:T(8,128)(2,1)S(1)}, u32[]{:S(2)}, u32[]{:S(2)}) async-start(bf16[4,192,512]{2,1,0:T(8,128)(2,1)} %shard_map.156), calls=%async_computation.2 | async-start | bytes 1572864 | tf_op jit(solution)/shard_map/all_to_all | solution.py:363
  92.1 5.6 %copy-start.9 = (bf16[96,2048]{1,0:T(8,128)(2,1)}, bf16[96,2048]{1,0:T(8,128)(2,1)S(1)}, u32[]{:S(2)}) copy-start(bf16[96,2048]{1,0:T(8,128)(2,1)S(1)} %collective-permute-done.7.s1) | copy-start | bytes 1179652
  92.1 5.6 %collective-permute-start.8 = (bf16[96,2048]{1,0:T(8,128)(2,1)S(1)}, bf16[96,2048]{1,0:T(8,128)(2,1)S(1)}, u32[]{:S(2)}, u32[]{:S(2)}) collective-permute-start(bf16[96,2048]{1,0:T(8,128)(2,1)S(1)} %collective-permute-done.7.s1), channel_id=1, source_target_pairs={{0,16},{16,0},{32,48},{48,32},{64,80},{80,64},{96,112},{112,96},{1... | collective-permute-start | bytes 1179656 | tf_op jit(solution)/shard_map/ppermute | solution.py:477
  143.5 15.6 %copy-start.5 = (f32[256,2]{0,1:T(2,128)S(1)}, f32[256,2]{0,1:T(2,128)}, u32[]{:S(2)}) copy-start(f32[256,2]{0,1:T(2,128)} %param.19) | copy-start | bytes 6148
  143.5 45.4 %copy-start.7 = (f32[128]{0:T(128)S(1)}, f32[128]{0:T(128)}, u32[]{:S(2)}) copy-start(f32[128]{0:T(128)} %param.30) | copy-start | bytes 1540
  143.5 45.4 %copy-start.8 = (f32[128]{0:T(128)S(1)}, f32[128]{0:T(128)}, u32[]{:S(2)}) copy-start(f32[128]{0:T(128)} %param.31) | copy-start | bytes 1540
  144.8 33.2 %all-to-all-start.4 = ((bf16[32,24,128]{2,1,0:T(8,128)(2,1)}), bf16[32,24,128]{2,1,0:T(8,128)(2,1)S(1)}, u32[]{:S(2)}, u32[]{:S(2)}) async-start(bf16[32,24,128]{2,1,0:T(8,128)(2,1)} %bitcast.37), calls=%async_computation.4 | async-start | bytes 393216 | tf_op jit(solution)/shard_map/all_to_all | solution.py:363

commit v5 on v4

--- a/solution.py
+++ b/solution.py
@@ -252,11 +252,11 @@
 
 
 def expert_body(rows, w0, w1, w2, w3, w4, w5, w6, w7, begun, out, wv, part_v, sems):
-    moved = (w1, w2, w3, w4, w5, w6, w7)
+    moved = (w2, w3, w4, w5, w6, w7)
     copies = [pltpu.make_async_copy(m, wv.at[i], sems.at[i]) for i, m in enumerate(moved)]
     for c in copies:
         c.start()
-    shards = (w0,) + tuple(wv.at[i] for i in range(7))
+    shards = (w0, w1) + tuple(wv.at[i] for i in range(6))
 
     def lower(c, start, stop):
         return shards[2 * c][start:stop, :]
@@ -267,7 +267,7 @@
     tokens = side([rows[i] for i in range(4)])
     hidden = []
     for c in range(4):
-        for i in ((0,), (1, 2), (3, 4), (5, 6))[c]:
+        for i in ((), (0, 1), (2, 3), (4, 5))[c]:
             copies[i].wait()
         ups = [lower(c, UP_AT, RELAYED), upper(c, RELAYED, DOWN_AT)]
         both = side([lower(c, 0, UP_AT), jnp.concatenate(ups, axis=0)])
@@ -285,7 +285,7 @@
         part_v[b] = part[:, :LANES]
         part_v[b + 1] = part[:, LANES:]
         target = out.at[pl.ds(b, 2), pl.ds(0, ROUTED_ROWS), :]
-        sends.append(pltpu.make_async_copy(part_v.at[pl.ds(b, 2)], target, sems.at[7 + b // 2]))
+        sends.append(pltpu.make_async_copy(part_v.at[pl.ds(b, 2)], target, sems.at[6 + b // 2]))
         sends[-1].start()
     for c in sends:
         c.wait()
@@ -501,12 +501,12 @@
     partial = kernel(
         expert_body,
         out_shape=struct((16, ROUTED_ROWS + SHARED_ROWS, LANES), BF16),
-        in_specs=[HELD] * 2 + [HBM] * 8,
+        in_specs=[HELD] * 3 + [HBM] * 7,
         out_specs=HBM,
         scratch_shapes=[
-            pltpu.VMEM((7, RELAYED, LANES), BF16),
+            pltpu.VMEM((6, RELAYED, LANES), BF16),
             pltpu.VMEM((16, ROUTED_ROWS, LANES), BF16),
-            pltpu.SemaphoreType.DMA((15,)),
+            pltpu.SemaphoreType.DMA((14,)),
         ],
         input_output_aliases={9: 0},
     )(

time: 191 us -> 191 us (level)
  no operation moved by 1% of the time
where the time goes in v5:
time: 191 us; the launch traced here: 189 us
  starting transfers between devices  76 us (40%)
  waiting for transfers between devices  57.7 us (30%)
  blocking collectives  33.2 us (17%)
  Pallas kernels  22 us (12%)
    all_to_all x4, starting transfers between devices, exchange(): return lax.all_to_all(parts, axes, split_axis=0, concat_axis=0, tiled=True)  42.9 us
    all_to_all x2, blocking collectives, exchange(): return lax.all_to_all(parts, axes, split_axis=0, concat_axis=0, tiled=True)  33.2 us
    all_to_all x4, waiting for transfers between devices, exchange(): return lax.all_to_all(parts, axes, split_axis=0, concat_axis=0, tiled=True)  32.8 us
    ppermute x6, waiting for transfers between devices, around(): return lax.ppermute(shard, 'x', [(i, (i + by) % 4) for i in range(4)])  22.2 us
    pallas_call x10, Pallas kernels, run(): return call(*args)  22 us
    ppermute x6, starting transfers between devices, around(): return lax.ppermute(shard, 'x', [(i, (i + by) % 4) for i in range(4)])  19.5 us
    ppermute x1, starting transfers between devices, layer(): halo = lax.ppermute(tail, 'sp', following)  7.44 us
    ppermute x1, starting transfers between devices, layer(): from_core = lax.ppermute(from_pair, 'sp', cores)  4.25 us
  transfers between devices with their start and end apart: 13, of which 7 were waited for; matrix products, arithmetic and copies ran while one was open for 0% of the time, Pallas kernels for 4%

profile of v5, /device:TPU:1, one launch (start us, length us, event | category | flops | bytes accessed | tf_op | source)
XLA Modules:
  0.0 189.5 jit_solution(6758309380813453047)
XLA Ops:
  0.0 2.0 %shard_map.154 = bf16[16,256,128]{2,1,0:T(8,128)(2,1)} custom-call(bf16[256,128]{1,0:T(8,128)(2,1)} %shard.1), custom_call_target="tpu_custom_call" | custom-call | tf_op jit(solution)/shard_map/pallas_call | solution.py:380
  2.0 0.0 copy-start.5
  2.0 0.0 copy-start
  2.0 0.0 copy-start.1
  2.0 0.0 copy-start.2
  2.0 0.0 copy-start.3
  2.0 7.7 %all-to-all-start = ((bf16[16,256,128]{2,1,0:T(8,128)(2,1)}), bf16[16,256,128]{2,1,0:T(8,128)(2,1)S(1)}, u32[]{:S(2)}, u32[]{:S(2)}) async-start(bf16[16,256,128]{2,1,0:T(8,128)(2,1)} %shard_map.154), calls=%async_computation | async-start | bytes 2097152 | tf_op jit(solution)/shard_map/all_to_all | solution.py:363
  9.8 0.0 copy-done.5
  9.8 0.1 add_convert_fusion
  9.9 14.5 %all-to-all-done.near = bf16[16,256,128]{2,1,0:T(8,128)(2,1)S(1)} async-done(((bf16[16,256,128]{2,1,0:T(8,128)(2,1)}), bf16[16,256,128]{2,1,0:T(8,128)(2,1)S(1)}, u32[]{:S(2)}, u32[]{:S(2)}) %all-to-all-start) | async-done | bytes 1048608 | tf_op jit(solution)/shard_map/all_to_all | solution.py:363
  24.4 0.1 broadcast_in_dim_broadcast_in_dim.2
  24.5 7.4 %collective-permute-start = (bf16[17,16,128]{2,1,0:T(8,128)(2,1)S(1)}, bf16[17,16,128]{2,1,0:T(8,128)(2,1)S(1)}, u32[]{:S(2)}, u32[]{:S(2)}) collective-permute-start(bf16[17,16,128]{2,1,0:T(8,128)(2,1)S(1)} %pad_maximum_fusion), channel_id=1, source_target_pairs={{0,16},{16,32},{32,48},{48,64},{64,80},{80,96},{96,112},{112,128},... | collective-permute-start | bytes 208904 | tf_op jit(solution)/shard_map/ppermute | solution.py:442
  31.9 0.1 pad_add_fusion.at
  32.0 1.3 collective-permute-done.halo
  33.3 0.0 copy-done.3
  33.3 4.6 %shard_map.155 = (bf16[256,512]{1,0:T(8,128)(2,1)}, bf16[4,128,512]{2,1,0:T(8,128)(2,1)S(1)}, bf16[256,128]{1,0:T(8,128)(2,1)S(1)}) custom-call(s32[3]{0:T(128)S(1)} %pad_add_fusion.at, s32[1,256]{1,0:T(1,128)S(1)} %bitcast.28, s32[2,256]{1,0:T(2,128)S(1)} %bitcast.25, f32[1,2048]{1,0:T(1,128)S(1)} %bitcast.22, f32[1,2048]{1,0:T(1,128)S(1)} %bitcast.23, ...), custom_call_target="tpu_custom_call" | custom-call | tf_op jit(solution)/shard_map/pallas_call | solution.py:380
  37.9 17.3 %all-to-all-start.1 = ((bf16[32,8,512]{2,1,0:T(8,128)(2,1)}), bf16[32,8,512]{2,1,0:T(8,128)(2,1)S(1)}, u32[]{:S(2)}, u32[]{:S(2)}) async-start(bf16[32,8,512]{2,1,0:T(8,128)(2,1)} %bitcast.36), calls=%async_computation.1 | async-start | bytes 524288 | tf_op jit(solution)/shard_map/all_to_all | solution.py:363
  55.3 3.6 %shard_map.157 = (bf16[3072,128]{1,0:T(8,128)(2,1)S(1)}, bf16[3072,128]{1,0:T(8,128)(2,1)S(1)}, bf16[192,2048]{1,0:T(8,128)(2,1)}, bf16[96,2048]{1,0:T(8,128)(2,1)}) custom-call(s32[3]{0:T(128)S(1)} %pad_add_fusion.at, bf16[2048,128]{1,0:T(8,128)(2,1)} %bitcast.31, bf16[2048,128]{1,0:T(8,128)(2,1)} %bitcast.32, bf16[128,2048]{1,0:T(8,128)(2,1)} %bitcast.33, ...), custom_call_target="tpu_custom_call" | custom-call | flops 10000000 | bytes 3145728 | tf_op jit(solution)/shard_map/pallas_call | solution.py:380
  58.9 1.9 %collective-permute-start.1 = (bf16[3072,128]{1,0:T(8,128)(2,1)S(1)}, bf16[3072,128]{1,0:T(8,128)(2,1)}, u32[]{:S(2)}, u32[]{:S(2)}) collective-permute-start(bf16[3072,128]{1,0:T(8,128)(2,1)S(1)} %get-tuple-element.19.w0), channel_id=1, source_target_pairs={{0,1},{1,2},{2,3},{3,0},{4,5},{5,6},{6,7},{7,4},{8,9},{9,10},{10,1... | collective-permute-start | bytes 2359304 | tf_op jit(solution)/shard_map/ppermute | solution.py:367
  60.8 4.6 %collective-permute-start.4 = (bf16[3072,128]{1,0:T(8,128)(2,1)S(1)}, bf16[3072,128]{1,0:T(8,128)(2,1)}, u32[]{:S(2)}, u32[]{:S(2)}) collective-permute-start(bf16[3072,128]{1,0:T(8,128)(2,1)S(1)} %get-tuple-element.20.w1), channel_id=1, source_target_pairs={{0,3},{1,0},{2,1},{3,2},{4,7},{5,4},{6,5},{7,6},{8,11},{9,8},{10,9... | collective-permute-start | bytes 2359304 | tf_op jit(solution)/shard_map/ppermute | solution.py:367
  65.4 1.9 %collective-permute-start.7 = (bf16[96,2048]{1,0:T(8,128)(2,1)}, bf16[96,2048]{1,0:T(8,128)(2,1)S(1)}, u32[]{:S(2)}, u32[]{:S(2)}) collective-permute-start(bf16[96,2048]{1,0:T(8,128)(2,1)} %get-tuple-element.23), channel_id=1, source_target_pairs={{0,4},{4,0},{8,12},{12,8},{1,5},{5,1},{9,13},{13,9},{2,6},{6,2},{1... | collective-permute-start | bytes 1179656 | tf_op jit(solution)/shard_map/ppermute | solution.py:475
  67.3 1.9 %collective-permute-start.2 = (bf16[3072,128]{1,0:T(8,128)(2,1)S(1)}, bf16[3072,128]{1,0:T(8,128)(2,1)}, u32[]{:S(2)}, u32[]{:S(2)}) collective-permute-start(bf16[3072,128]{1,0:T(8,128)(2,1)S(1)} %get-tuple-element.20.w1), channel_id=1, source_target_pairs={{0,1},{1,2},{2,3},{3,0},{4,5},{5,6},{6,7},{7,4},{8,9},{9,10},{10,1... | collective-permute-start | bytes 2359304 | tf_op jit(solution)/shard_map/ppermute | solution.py:367
  69.2 4.6 %collective-permute-start.3 = (bf16[3072,128]{1,0:T(8,128)(2,1)S(1)}, bf16[3072,128]{1,0:T(8,128)(2,1)}, u32[]{:S(2)}, u32[]{:S(2)}) collective-permute-start(bf16[3072,128]{1,0:T(8,128)(2,1)S(1)} %get-tuple-element.19.w0), channel_id=1, source_target_pairs={{0,3},{1,0},{2,1},{3,2},{4,7},{5,4},{6,5},{7,6},{8,11},{9,8},{10,9... | collective-permute-start | bytes 2359304 | tf_op jit(solution)/shard_map/ppermute | solution.py:367
  73.8 7.1 %collective-permute-done.1.w2 = bf16[3072,128]{1,0:T(8,128)(2,1)} collective-permute-done((bf16[3072,128]{1,0:T(8,128)(2,1)S(1)}, bf16[3072,128]{1,0:T(8,128)(2,1)}, u32[]{:S(2)}, u32[]{:S(2)}) %collective-permute-start.1) | collective-permute-done | bytes 786464 | tf_op jit(solution)/shard_map/ppermute | solution.py:367
  80.9 1.9 %collective-permute-start.5 = (bf16[3072,128]{1,0:T(8,128)(2,1)}, bf16[3072,128]{1,0:T(8,128)(2,1)}, u32[]{:S(2)}, u32[]{:S(2)}) collective-permute-start(bf16[3072,128]{1,0:T(8,128)(2,1)} %collective-permute-done.1.w2), channel_id=1, source_target_pairs={{0,1},{1,2},{2,3},{3,0},{4,5},{5,6},{6,7},{7,4},{8,9},{9,10},{10,1... | collective-permute-start | bytes 2359304 | tf_op jit(solution)/shard_map/ppermute | solution.py:367
  82.8 0.0 collective-permute-done.4.w5
  82.9 4.6 %collective-permute-start.6 = (bf16[3072,128]{1,0:T(8,128)(2,1)}, bf16[3072,128]{1,0:T(8,128)(2,1)}, u32[]{:S(2)}, u32[]{:S(2)}) collective-permute-start(bf16[3072,128]{1,0:T(8,128)(2,1)} %collective-permute-done.4.w5), channel_id=1, source_target_pairs={{0,3},{1,0},{2,1},{3,2},{4,7},{5,4},{6,5},{7,6},{8,11},{9,8},{10,9... | collective-permute-start | bytes 2359304 | tf_op jit(solution)/shard_map/ppermute | solution.py:367
  87.4 0.0 all-to-all-done.1
  87.4 1.1 shard_map.156
  88.5 3.5 %all-to-all-start.2 = ((bf16[4,192,512]{2,1,0:T(8,128)(2,1)}), bf16[4,192,512]{2,1,0:T(8,128)(2,1)S(1)}, u32[]{:S(2)}, u32[]{:S(2)}) async-start(bf16[4,192,512]{2,1,0:T(8,128)(2,1)} %shard_map.156), calls=%async_computation.2 | async-start | bytes 1572864 | tf_op jit(solution)/shard_map/all_to_all | solution.py:363
  92.0 0.0 collective-permute-done.7.s1
  92.1 4.3 %collective-permute-start.8 = (bf16[96,2048]{1,0:T(8,128)(2,1)S(1)}, bf16[96,2048]{1,0:T(8,128)(2,1)S(1)}, u32[]{:S(2)}, u32[]{:S(2)}) collective-permute-start(bf16[96,2048]{1,0:T(8,128)(2,1)S(1)} %collective-permute-done.7.s1), channel_id=1, source_target_pairs={{0,16},{16,0},{32,48},{48,32},{64,80},{80,64},{96,112},{112,96},{1... | collective-permute-start | bytes 1179656 | tf_op jit(solution)/shard_map/ppermute | solution.py:477
  96.3 1.3 collective-permute-done.8.s2
  97.7 2.8 %shard_map.158.begun = bf16[16,320,128]{2,1,0:T(8,128)(2,1)} custom-call(bf16[4,128,512]{2,1,0:T(8,128)(2,1)S(1)} %get-tuple-element.21.normed, bf16[192,2048]{1,0:T(8,128)(2,1)} %get-tuple-element.22.s0, bf16[96,2048]{1,0:T(8,128)(2,1)} %copy-done.8, bf16[96,2048]{1,0:T(8,128)(2,1)S(1)} %collective-permute-done.8.s2), custom_call_target="tpu_custom_call" | custom-call | tf_op jit(solution)/shard_map/pallas_call | solution.py:380
  100.4 0.0 collective-permute-done.2.w3
  100.4 0.0 collective-permute-done.3.w4
  100.5 14.2 %collective-permute-done.5.w6 = bf16[3072,128]{1,0:T(8,128)(2,1)} collective-permute-done((bf16[3072,128]{1,0:T(8,128)(2,1)}, bf16[3072,128]{1,0:T(8,128)(2,1)}, u32[]{:S(2)}, u32[]{:S(2)}) %collective-permute-start.5) | collective-permute-done | bytes 786464 | tf_op jit(solution)/shard_map/ppermute | solution.py:367
  114.6 0.9 collective-permute-done.6.w7
  115.5 0.0 all-to-all-done.2.rows
  115.5 4.3 %shard_map.159 = bf16[16,320,128]{2,1,0:T(8,128)(2,1)} custom-call(bf16[4,192,512]{2,1,0:T(8,128)(2,1)S(1)} %all-to-all-done.2.rows, bf16[3072,128]{1,0:T(8,128)(2,1)S(1)} %get-tuple-element.19.w0, bf16[3072,128]{1,0:T(8,128)(2,1)S(1)} %get-tuple-element.20.w1, bf16[3072,128]{1,0:T(8,128)(2,1)} %collective-permute-done.1.w2, ...), custom_call_target="tpu_custom_call", output_to_operand_aliasing={{}: (9, {})} | custom-call | tf_op jit(solution)/shard_map/pallas_call | solution.py:380
  119.9 23.4 %all_to_all.30.parts = bf16[16,320,128]{2,1,0:T(8,128)(2,1)S(1)} all-to-all(bf16[16,320,128]{2,1,0:T(8,128)(2,1)} %shard_map.159), channel_id=1, replica_groups=mesh['sp'=32,'y'=4,'x'=4] {'y','x'}, dimensions={0} | all-to-all | bytes 2621440 | tf_op jit(solution)/shard_map/all_to_all | solution.py:363
  143.3 1.3 shard_map.160
  144.5 14.4 %all-to-all-start.4 = ((bf16[32,24,128]{2,1,0:T(8,128)(2,1)}), bf16[32,24,128]{2,1,0:T(8,128)(2,1)S(1)}, u32[]{:S(2)}, u32[]{:S(2)}) async-start(bf16[32,24,128]{2,1,0:T(8,128)(2,1)} %bitcast.37), calls=%async_computation.4 | async-start | bytes 393216 | tf_op jit(solution)/shard_map/all_to_all | solution.py:363
  158.9 0.5 shard_map.161
  159.4 18.3 %all-to-all-done.4 = bf16[32,24,128]{2,1,0:T(8,128)(2,1)S(1)} async-done(((bf16[32,24,128]{2,1,0:T(8,128)(2,1)}), bf16[32,24,128]{2,1,0:T(8,128)(2,1)S(1)}, u32[]{:S(2)}, u32[]{:S(2)}) %all-to-all-start.4) | async-done | bytes 196640 | tf_op jit(solution)/shard_map/all_to_all | solution.py:363
  177.7 1.1 shard_map.162
  178.8 9.9 %all_to_all.31.stats = f32[16,2,256]{2,1,0:T(2,128)S(1)} all-to-all(f32[16,2,256]{2,1,0:T(2,128)} %get-tuple-element.30), channel_id=1, replica_groups=mesh['sp'=32,'y'=4,'x'=4] {'y','x'}, dimensions={0} | all-to-all | bytes 65536 | tf_op jit(solution)/shard_map/all_to_all | solution.py:363
  188.7 0.8 shard_map.163
  (13 shorter events, 0.0 us)
Async XLA Ops:
  2.0 7.8 %copy-start.5 = (s32[256]{0:T(256)S(1)}, s32[256]{0:T(256)}, u32[]{:S(2)}) copy-start(s32[256]{0:T(256)} %param.17) | copy-start | bytes 3076
  2.0 31.3 %copy-start = (f32[2048]{0:T(1024)S(1)}, f32[2048]{0:T(1024)}, u32[]{:S(2)}) copy-start(f32[2048]{0:T(1024)} %param.21) | copy-start | bytes 24580
  2.0 31.3 %copy-start.1 = (f32[2048]{0:T(1024)S(1)}, f32[2048]{0:T(1024)}, u32[]{:S(2)}) copy-start(f32[2048]{0:T(1024)} %param.22) | copy-start | bytes 24580
  2.0 31.3 %copy-start.2 = (f32[2048]{0:T(1024)S(1)}, f32[2048]{0:T(1024)}, u32[]{:S(2)}) copy-start(f32[2048]{0:T(1024)} %param.23) | copy-start | bytes 24580
  2.0 31.3 %copy-start.3 = (s32[256,2]{0,1:T(2,128)S(1)}, s32[256,2]{0,1:T(2,128)}, u32[]{:S(2)}) copy-start(s32[256,2]{0,1:T(2,128)} %param.18) | copy-start | bytes 6148
  2.0 22.3 %all-to-all-start = ((bf16[16,256,128]{2,1,0:T(8,128)(2,1)}), bf16[16,256,128]{2,1,0:T(8,128)(2,1)S(1)}, u32[]{:S(2)}, u32[]{:S(2)}) async-start(bf16[16,256,128]{2,1,0:T(8,128)(2,1)} %shard_map.154), calls=%async_computation | async-start | bytes 2097152 | tf_op jit(solution)/shard_map/all_to_all | solution.py:363
  24.5 8.8 %collective-permute-start = (bf16[17,16,128]{2,1,0:T(8,128)(2,1)S(1)}, bf16[17,16,128]{2,1,0:T(8,128)(2,1)S(1)}, u32[]{:S(2)}, u32[]{:S(2)}) collective-permute-start(bf16[17,16,128]{2,1,0:T(8,128)(2,1)S(1)} %pad_maximum_fusion), channel_id=1, source_target_pairs={{0,16},{16,32},{32,48},{48,64},{64,80},{80,96},{96,112},{112,128},... | collective-permute-start | bytes 208904 | tf_op jit(solution)/shard_map/ppermute | solution.py:442
  37.9 49.5 %all-to-all-start.1 = ((bf16[32,8,512]{2,1,0:T(8,128)(2,1)}), bf16[32,8,512]{2,1,0:T(8,128)(2,1)S(1)}, u32[]{:S(2)}, u32[]{:S(2)}) async-start(bf16[32,8,512]{2,1,0:T(8,128)(2,1)} %bitcast.36), calls=%async_computation.1 | async-start | bytes 524288 | tf_op jit(solution)/shard_map/all_to_all | solution.py:363
  58.9 22.1 %collective-permute-start.1 = (bf16[3072,128]{1,0:T(8,128)(2,1)S(1)}, bf16[3072,128]{1,0:T(8,128)(2,1)}, u32[]{:S(2)}, u32[]{:S(2)}) collective-permute-start(bf16[3072,128]{1,0:T(8,128)(2,1)S(1)} %get-tuple-element.19.w0), channel_id=1, source_target_pairs={{0,1},{1,2},{2,3},{3,0},{4,5},{5,6},{6,7},{7,4},{8,9},{9,10},{10,1... | collective-permute-start | bytes 2359304 | tf_op jit(solution)/shard_map/ppermute | solution.py:367
  60.8 22.1 %collective-permute-start.4 = (bf16[3072,128]{1,0:T(8,128)(2,1)S(1)}, bf16[3072,128]{1,0:T(8,128)(2,1)}, u32[]{:S(2)}, u32[]{:S(2)}) collective-permute-start(bf16[3072,128]{1,0:T(8,128)(2,1)S(1)} %get-tuple-element.20.w1), channel_id=1, source_target_pairs={{0,3},{1,0},{2,1},{3,2},{4,7},{5,4},{6,5},{7,6},{8,11},{9,8},{10,9... | collective-permute-start | bytes 2359304 | tf_op jit(solution)/shard_map/ppermute | solution.py:367
  65.4 26.7 %collective-permute-start.7 = (bf16[96,2048]{1,0:T(8,128)(2,1)}, bf16[96,2048]{1,0:T(8,128)(2,1)S(1)}, u32[]{:S(2)}, u32[]{:S(2)}) collective-permute-start(bf16[96,2048]{1,0:T(8,128)(2,1)} %get-tuple-element.23), channel_id=1, source_target_pairs={{0,4},{4,0},{8,12},{12,8},{1,5},{5,1},{9,13},{13,9},{2,6},{6,2},{1... | collective-permute-start | bytes 1179656 | tf_op jit(solution)/shard_map/ppermute | solution.py:475
  67.3 33.1 %collective-permute-start.2 = (bf16[3072,128]{1,0:T(8,128)(2,1)S(1)}, bf16[3072,128]{1,0:T(8,128)(2,1)}, u32[]{:S(2)}, u32[]{:S(2)}) collective-permute-start(bf16[3072,128]{1,0:T(8,128)(2,1)S(1)} %get-tuple-element.20.w1), channel_id=1, source_target_pairs={{0,1},{1,2},{2,3},{3,0},{4,5},{5,6},{6,7},{7,4},{8,9},{9,10},{10,1... | collective-permute-start | bytes 2359304 | tf_op jit(solution)/shard_map/ppermute | solution.py:367
  69.2 31.2 %collective-permute-start.3 = (bf16[3072,128]{1,0:T(8,128)(2,1)S(1)}, bf16[3072,128]{1,0:T(8,128)(2,1)}, u32[]{:S(2)}, u32[]{:S(2)}) collective-permute-start(bf16[3072,128]{1,0:T(8,128)(2,1)S(1)} %get-tuple-element.19.w0), channel_id=1, source_target_pairs={{0,3},{1,0},{2,1},{3,2},{4,7},{5,4},{6,5},{7,6},{8,11},{9,8},{10,9... | collective-permute-start | bytes 2359304 | tf_op jit(solution)/shard_map/ppermute | solution.py:367
  80.9 33.7 %collective-permute-start.5 = (bf16[3072,128]{1,0:T(8,128)(2,1)}, bf16[3072,128]{1,0:T(8,128)(2,1)}, u32[]{:S(2)}, u32[]{:S(2)}) collective-permute-start(bf16[3072,128]{1,0:T(8,128)(2,1)} %collective-permute-done.1.w2), channel_id=1, source_target_pairs={{0,1},{1,2},{2,3},{3,0},{4,5},{5,6},{6,7},{7,4},{8,9},{9,10},{10,1... | collective-permute-start | bytes 2359304 | tf_op jit(solution)/shard_map/ppermute | solution.py:367
  82.9 32.7 %collective-permute-start.6 = (bf16[3072,128]{1,0:T(8,128)(2,1)}, bf16[3072,128]{1,0:T(8,128)(2,1)}, u32[]{:S(2)}, u32[]{:S(2)}) collective-permute-start(bf16[3072,128]{1,0:T(8,128)(2,1)} %collective-permute-done.4.w5), channel_id=1, source_target_pairs={{0,3},{1,0},{2,1},{3,2},{4,7},{5,4},{6,5},{7,6},{8,11},{9,8},{10,9... | collective-permute-start | bytes 2359304 | tf_op jit(solution)/shard_map/ppermute | solution.py:367
  88.5 27.0 %all-to-all-start.2 = ((bf16[4,192,512]{2,1,0:T(8,128)(2,1)}), bf16[4,192,512]{2,1,0:T(8,128)(2,1)S(1)}, u32[]{:S(2)}, u32[]{:S(2)}) async-start(bf16[4,192,512]{2,1,0:T(8,128)(2,1)} %shard_map.156), calls=%async_computation.2 | async-start | bytes 1572864 | tf_op jit(solution)/shard_map/all_to_all | solution.py:363
  92.1 5.6 %copy-start.8 = (bf16[96,2048]{1,0:T(8,128)(2,1)}, bf16[96,2048]{1,0:T(8,128)(2,1)S(1)}, u32[]{:S(2)}) copy-start(bf16[96,2048]{1,0:T(8,128)(2,1)S(1)} %collective-permute-done.7.s1) | copy-start | bytes 1179652
  92.1 5.6 %collective-permute-start.8 = (bf16[96,2048]{1,0:T(8,128)(2,1)S(1)}, bf16[96,2048]{1,0:T(8,128)(2,1)S(1)}, u32[]{:S(2)}, u32[]{:S(2)}) collective-permute-start(bf16[96,2048]{1,0:T(8,128)(2,1)S(1)} %collective-permute-done.7.s1), channel_id=1, source_target_pairs={{0,16},{16,0},{32,48},{48,32},{64,80},{80,64},{96,112},{112,96},{1... | collective-permute-start | bytes 1179656 | tf_op jit(solution)/shard_map/ppermute | solution.py:477
  143.3 15.6 %copy-start.4 = (f32[256,2]{0,1:T(2,128)S(1)}, f32[256,2]{0,1:T(2,128)}, u32[]{:S(2)}) copy-start(f32[256,2]{0,1:T(2,128)} %param.19) | copy-start | bytes 6148
  143.3 45.4 %copy-start.6 = (f32[128]{0:T(128)S(1)}, f32[128]{0:T(128)}, u32[]{:S(2)}) copy-start(f32[128]{0:T(128)} %param.30) | copy-start | bytes 1540
  143.3 45.4 %copy-start.7 = (f32[128]{0:T(128)S(1)}, f32[128]{0:T(128)}, u32[]{:S(2)}) copy-start(f32[128]{0:T(128)} %param.31) | copy-start | bytes 1540
  144.5 33.1 %all-to-all-start.4 = ((bf16[32,24,128]{2,1,0:T(8,128)(2,1)}), bf16[32,24,128]{2,1,0:T(8,128)(2,1)S(1)}, u32[]{:S(2)}, u32[]{:S(2)}) async-start(bf16[32,24,128]{2,1,0:T(8,128)(2,1)} %bitcast.37), calls=%async_computation.4 | async-start | bytes 393216 | tf_op jit(solution)/shard_map/all_to_all | solution.py:363

commit v6 on v4

--- a/solution.py
+++ b/solution.py
@@ -130,12 +130,12 @@
     first_v,
     quarter_v,
     send_v,
+    pick_v,
     sems,
 ):
     y, x = at[0], at[1]
     copies = [pltpu.make_async_copy(weight.at[g], weight_v.at[g], sems.at[g]) for g in range(4)]
-    for c in copies:
-        c.start()
+    copies[0].start()
     own_row = (docs[...] + 1).astype(F32)
     own_marks = as_column(own_row)
     halo_row = halo[16].astype(F32).T[0:1]
@@ -159,6 +159,15 @@
             begin = running[0:HALO] + jnp.dot(edge, head, preferred_element_type=F32)
             running = jnp.concatenate([begin, running[HALO:]], axis=0)
             mixed_v[g, :, at_lane] = (running * scale_by - mine.astype(F32)).astype(BF16)
+        if g < 3:
+            copies[g + 1].start()
+    named = routes[...]
+    dests = []
+    for k, rank in enumerate(ranks_of(named)):
+        slot = named[k : k + 1] * SLOTS_SENT + (rank >> 2)
+        dests.append(jnp.where((rank & 3) == x, slot, -1))
+    slot = iota((EXPERTS * SLOTS_SENT, TOKENS_HERE), 0)
+    pick_v[...] = chosen((slot == dests[0]) | (slot == dests[1]))
     total = jnp.zeros((TOKENS_HERE, 1), F32)
     squares = jnp.zeros((TOKENS_HERE, 1), F32)
     for g in range(4):
@@ -182,14 +191,7 @@
         scaled = (first_v[y, rows, :] - mean[rows]) * inv[rows]
         quarter_v[rows, :] = (scaled * gain_here + bias_here).astype(BF16)
     quarter = quarter_v[...]
-    named = routes[...]
-    dests = []
-    for k, rank in enumerate(ranks_of(named)):
-        slot = named[k : k + 1] * SLOTS_SENT + (rank >> 2)
-        dests.append(jnp.where((rank & 3) == x, slot, -1))
-    slot = iota((EXPERTS * SLOTS_SENT, TOKENS_HERE), 0)
-    pick = chosen((slot == dests[0]) | (slot == dests[1]))
-    send_v[...] = jnp.dot(pick, quarter, preferred_element_type=F32).astype(BF16)
+    send_v[...] = jnp.dot(pick_v[...], quarter, preferred_element_type=F32).astype(BF16)
     leave = pltpu.make_async_copy(send_v, send, sems.at[4])
     leave.start()
     mine = quarter[:, 0:LANES]
@@ -454,6 +456,7 @@
             pltpu.VMEM((4, TOKENS_HERE, QUARTER), F32),
             pltpu.VMEM((TOKENS_HERE, QUARTER), BF16),
             pltpu.VMEM((EXPERTS * SLOTS_SENT, QUARTER), BF16),
+            pltpu.VMEM((EXPERTS * SLOTS_SENT, TOKENS_HERE), BF16),
             pltpu.SemaphoreType.DMA((5,)),
         ],
         out_shape=[

time: 191 us -> 191 us (level)
  no operation moved by 1% of the time
where the time goes in v6:
time: 191 us; the launch traced here: 190 us
  starting transfers between devices  75.9 us (40%)
  waiting for transfers between devices  57.6 us (30%)
  blocking collectives  33.3 us (17%)
  Pallas kernels  22.8 us (12%)
    all_to_all x4, starting transfers between devices, exchange(): return lax.all_to_all(parts, axes, split_axis=0, concat_axis=0, tiled=True)  42.9 us
    all_to_all x2, blocking collectives, exchange(): return lax.all_to_all(parts, axes, split_axis=0, concat_axis=0, tiled=True)  33.3 us
    all_to_all x4, waiting for transfers between devices, exchange(): return lax.all_to_all(parts, axes, split_axis=0, concat_axis=0, tiled=True)  32.8 us
    pallas_call x10, Pallas kernels, run(): return call(*args)  22.8 us
    ppermute x6, waiting for transfers between devices, around(): return lax.ppermute(shard, 'x', [(i, (i + by) % 4) for i in range(4)])  22.1 us
    ppermute x6, starting transfers between devices, around(): return lax.ppermute(shard, 'x', [(i, (i + by) % 4) for i in range(4)])  19.5 us
    ppermute x1, starting transfers between devices, layer(): halo = lax.ppermute(tail, 'sp', following)  7.44 us
    ppermute x1, starting transfers between devices, layer(): from_core = lax.ppermute(from_pair, 'sp', cores)  4.25 us
  transfers between devices with their start and end apart: 13, of which 7 were waited for; matrix products, arithmetic and copies ran while one was open for 0% of the time, Pallas kernels for 4%

profile of v6, /device:TPU:1, one launch (start us, length us, event | category | flops | bytes accessed | tf_op | source)
XLA Modules:
  0.0 190.2 jit_solution(11107121626178960517)
XLA Ops:
  0.0 2.0 %shard_map.154 = bf16[16,256,128]{2,1,0:T(8,128)(2,1)} custom-call(bf16[256,128]{1,0:T(8,128)(2,1)} %shard.1), custom_call_target="tpu_custom_call" | custom-call | tf_op jit(solution)/shard_map/pallas_call | solution.py:382
  2.0 0.0 copy-start.6
  2.0 0.0 copy-start.1
  2.0 0.0 copy-start.2
  2.0 0.0 copy-start.3
  2.0 0.0 copy-start.4
  2.0 7.7 %all-to-all-start = ((bf16[16,256,128]{2,1,0:T(8,128)(2,1)}), bf16[16,256,128]{2,1,0:T(8,128)(2,1)S(1)}, u32[]{:S(2)}, u32[]{:S(2)}) async-start(bf16[16,256,128]{2,1,0:T(8,128)(2,1)} %shard_map.154), calls=%async_computation | async-start | bytes 2097152 | tf_op jit(solution)/shard_map/all_to_all | solution.py:365
  9.8 0.0 copy-done.6
  9.8 0.1 add_convert_fusion
  9.9 14.5 %all-to-all-done.near = bf16[16,256,128]{2,1,0:T(8,128)(2,1)S(1)} async-done(((bf16[16,256,128]{2,1,0:T(8,128)(2,1)}), bf16[16,256,128]{2,1,0:T(8,128)(2,1)S(1)}, u32[]{:S(2)}, u32[]{:S(2)}) %all-to-all-start) | async-done | bytes 1048608 | tf_op jit(solution)/shard_map/all_to_all | solution.py:365
  24.4 0.1 broadcast_in_dim_broadcast_in_dim.2
  24.5 7.4 %collective-permute-start = (bf16[17,16,128]{2,1,0:T(8,128)(2,1)S(1)}, bf16[17,16,128]{2,1,0:T(8,128)(2,1)S(1)}, u32[]{:S(2)}, u32[]{:S(2)}) collective-permute-start(bf16[17,16,128]{2,1,0:T(8,128)(2,1)S(1)} %pad_maximum_fusion), channel_id=1, source_target_pairs={{0,16},{16,32},{32,48},{48,64},{64,80},{80,96},{96,112},{112,128},... | collective-permute-start | bytes 208904 | tf_op jit(solution)/shard_map/ppermute | solution.py:444
  31.9 0.1 pad_add_fusion.at
  32.0 1.3 collective-permute-done.halo
  33.3 0.0 copy-done.3
  33.3 5.1 %shard_map.155 = (bf16[256,512]{1,0:T(8,128)(2,1)}, bf16[4,128,512]{2,1,0:T(8,128)(2,1)S(1)}, bf16[256,128]{1,0:T(8,128)(2,1)S(1)}) custom-call(s32[3]{0:T(128)S(1)} %pad_add_fusion.at, s32[1,256]{1,0:T(1,128)S(1)} %bitcast.28, s32[2,256]{1,0:T(2,128)S(1)} %bitcast.25, f32[1,2048]{1,0:T(1,128)S(1)} %bitcast.22, f32[1,2048]{1,0:T(1,128)S(1)} %bitcast.23, ...), custom_call_target="tpu_custom_call" | custom-call | tf_op jit(solution)/shard_map/pallas_call | solution.py:382
  38.4 17.3 %all-to-all-start.1 = ((bf16[32,8,512]{2,1,0:T(8,128)(2,1)}), bf16[32,8,512]{2,1,0:T(8,128)(2,1)S(1)}, u32[]{:S(2)}, u32[]{:S(2)}) async-start(bf16[32,8,512]{2,1,0:T(8,128)(2,1)} %bitcast.36), calls=%async_computation.1 | async-start | bytes 524288 | tf_op jit(solution)/shard_map/all_to_all | solution.py:365
  55.7 3.5 %shard_map.157 = (bf16[3072,128]{1,0:T(8,128)(2,1)S(1)}, bf16[3072,128]{1,0:T(8,128)(2,1)S(1)}, bf16[192,2048]{1,0:T(8,128)(2,1)}, bf16[96,2048]{1,0:T(8,128)(2,1)}) custom-call(s32[3]{0:T(128)S(1)} %pad_add_fusion.at, bf16[2048,128]{1,0:T(8,128)(2,1)} %bitcast.31, bf16[2048,128]{1,0:T(8,128)(2,1)} %bitcast.32, bf16[128,2048]{1,0:T(8,128)(2,1)} %bitcast.33, ...), custom_call_target="tpu_custom_call" | custom-call | flops 10000000 | bytes 3145728 | tf_op jit(solution)/shard_map/pallas_call | solution.py:382
  59.3 1.9 %collective-permute-start.1 = (bf16[3072,128]{1,0:T(8,128)(2,1)S(1)}, bf16[3072,128]{1,0:T(8,128)(2,1)}, u32[]{:S(2)}, u32[]{:S(2)}) collective-permute-start(bf16[3072,128]{1,0:T(8,128)(2,1)S(1)} %get-tuple-element.19.w0), channel_id=1, source_target_pairs={{0,1},{1,2},{2,3},{3,0},{4,5},{5,6},{6,7},{7,4},{8,9},{9,10},{10,1... | collective-permute-start | bytes 2359304 | tf_op jit(solution)/shard_map/ppermute | solution.py:369
  61.2 4.6 %collective-permute-start.4 = (bf16[3072,128]{1,0:T(8,128)(2,1)S(1)}, bf16[3072,128]{1,0:T(8,128)(2,1)}, u32[]{:S(2)}, u32[]{:S(2)}) collective-permute-start(bf16[3072,128]{1,0:T(8,128)(2,1)S(1)} %get-tuple-element.20.w1), channel_id=1, source_target_pairs={{0,3},{1,0},{2,1},{3,2},{4,7},{5,4},{6,5},{7,6},{8,11},{9,8},{10,9... | collective-permute-start | bytes 2359304 | tf_op jit(solution)/shard_map/ppermute | solution.py:369
  65.8 1.9 %collective-permute-start.7 = (bf16[96,2048]{1,0:T(8,128)(2,1)}, bf16[96,2048]{1,0:T(8,128)(2,1)S(1)}, u32[]{:S(2)}, u32[]{:S(2)}) collective-permute-start(bf16[96,2048]{1,0:T(8,128)(2,1)} %get-tuple-element.23), channel_id=1, source_target_pairs={{0,4},{4,0},{8,12},{12,8},{1,5},{5,1},{9,13},{13,9},{2,6},{6,2},{1... | collective-permute-start | bytes 1179656 | tf_op jit(solution)/shard_map/ppermute | solution.py:478
  67.7 1.9 %collective-permute-start.2 = (bf16[3072,128]{1,0:T(8,128)(2,1)S(1)}, bf16[3072,128]{1,0:T(8,128)(2,1)}, u32[]{:S(2)}, u32[]{:S(2)}) collective-permute-start(bf16[3072,128]{1,0:T(8,128)(2,1)S(1)} %get-tuple-element.20.w1), channel_id=1, source_target_pairs={{0,1},{1,2},{2,3},{3,0},{4,5},{5,6},{6,7},{7,4},{8,9},{9,10},{10,1... | collective-permute-start | bytes 2359304 | tf_op jit(solution)/shard_map/ppermute | solution.py:369
  69.7 4.6 %collective-permute-start.3 = (bf16[3072,128]{1,0:T(8,128)(2,1)S(1)}, bf16[3072,128]{1,0:T(8,128)(2,1)}, u32[]{:S(2)}, u32[]{:S(2)}) collective-permute-start(bf16[3072,128]{1,0:T(8,128)(2,1)S(1)} %get-tuple-element.19.w0), channel_id=1, source_target_pairs={{0,3},{1,0},{2,1},{3,2},{4,7},{5,4},{6,5},{7,6},{8,11},{9,8},{10,9... | collective-permute-start | bytes 2359304 | tf_op jit(solution)/shard_map/ppermute | solution.py:369
  74.2 7.1 %collective-permute-done.1.w2 = bf16[3072,128]{1,0:T(8,128)(2,1)} collective-permute-done((bf16[3072,128]{1,0:T(8,128)(2,1)S(1)}, bf16[3072,128]{1,0:T(8,128)(2,1)}, u32[]{:S(2)}, u32[]{:S(2)}) %collective-permute-start.1) | collective-permute-done | bytes 786464 | tf_op jit(solution)/shard_map/ppermute | solution.py:369
  81.4 1.9 %collective-permute-start.5 = (bf16[3072,128]{1,0:T(8,128)(2,1)}, bf16[3072,128]{1,0:T(8,128)(2,1)}, u32[]{:S(2)}, u32[]{:S(2)}) collective-permute-start(bf16[3072,128]{1,0:T(8,128)(2,1)} %collective-permute-done.1.w2), channel_id=1, source_target_pairs={{0,1},{1,2},{2,3},{3,0},{4,5},{5,6},{6,7},{7,4},{8,9},{9,10},{10,1... | collective-permute-start | bytes 2359304 | tf_op jit(solution)/shard_map/ppermute | solution.py:369
  83.3 0.0 collective-permute-done.4.w5
  83.3 4.6 %collective-permute-start.6 = (bf16[3072,128]{1,0:T(8,128)(2,1)}, bf16[3072,128]{1,0:T(8,128)(2,1)}, u32[]{:S(2)}, u32[]{:S(2)}) collective-permute-start(bf16[3072,128]{1,0:T(8,128)(2,1)} %collective-permute-done.4.w5), channel_id=1, source_target_pairs={{0,3},{1,0},{2,1},{3,2},{4,7},{5,4},{6,5},{7,6},{8,11},{9,8},{10,9... | collective-permute-start | bytes 2359304 | tf_op jit(solution)/shard_map/ppermute | solution.py:369
  87.9 0.0 all-to-all-done.1
  87.9 1.2 shard_map.156
  89.1 3.5 %all-to-all-start.2 = ((bf16[4,192,512]{2,1,0:T(8,128)(2,1)}), bf16[4,192,512]{2,1,0:T(8,128)(2,1)S(1)}, u32[]{:S(2)}, u32[]{:S(2)}) async-start(bf16[4,192,512]{2,1,0:T(8,128)(2,1)} %shard_map.156), calls=%async_computation.2 | async-start | bytes 1572864 | tf_op jit(solution)/shard_map/all_to_all | solution.py:365
  92.6 0.0 collective-permute-done.7.s1
  92.6 4.2 %collective-permute-start.8 = (bf16[96,2048]{1,0:T(8,128)(2,1)S(1)}, bf16[96,2048]{1,0:T(8,128)(2,1)S(1)}, u32[]{:S(2)}, u32[]{:S(2)}) collective-permute-start(bf16[96,2048]{1,0:T(8,128)(2,1)S(1)} %collective-permute-done.7.s1), channel_id=1, source_target_pairs={{0,16},{16,0},{32,48},{48,32},{64,80},{80,64},{96,112},{112,96},{1... | collective-permute-start | bytes 1179656 | tf_op jit(solution)/shard_map/ppermute | solution.py:480
  96.8 1.3 collective-permute-done.8.s2
  98.2 2.8 %shard_map.158.begun = bf16[16,320,128]{2,1,0:T(8,128)(2,1)} custom-call(bf16[4,128,512]{2,1,0:T(8,128)(2,1)S(1)} %get-tuple-element.21.normed, bf16[192,2048]{1,0:T(8,128)(2,1)} %get-tuple-element.22.s0, bf16[96,2048]{1,0:T(8,128)(2,1)} %copy-done.9, bf16[96,2048]{1,0:T(8,128)(2,1)S(1)} %collective-permute-done.8.s2), custom_call_target="tpu_custom_call" | custom-call | tf_op jit(solution)/shard_map/pallas_call | solution.py:382
  100.9 0.0 collective-permute-done.2.w3
  101.0 0.0 collective-permute-done.3.w4
  101.0 14.1 %collective-permute-done.5.w6 = bf16[3072,128]{1,0:T(8,128)(2,1)} collective-permute-done((bf16[3072,128]{1,0:T(8,128)(2,1)}, bf16[3072,128]{1,0:T(8,128)(2,1)}, u32[]{:S(2)}, u32[]{:S(2)}) %collective-permute-start.5) | collective-permute-done | bytes 786464 | tf_op jit(solution)/shard_map/ppermute | solution.py:369
  115.1 0.9 collective-permute-done.6.w7
  116.0 0.0 all-to-all-done.2.rows
  116.0 4.7 %shard_map.159 = bf16[16,320,128]{2,1,0:T(8,128)(2,1)} custom-call(bf16[4,192,512]{2,1,0:T(8,128)(2,1)S(1)} %all-to-all-done.2.rows, bf16[3072,128]{1,0:T(8,128)(2,1)S(1)} %get-tuple-element.19.w0, bf16[3072,128]{1,0:T(8,128)(2,1)} %copy-done, bf16[3072,128]{1,0:T(8,128)(2,1)} %collective-permute-done.1.w2, ...), custom_call_target="tpu_custom_call", output_to_operand_aliasing={{}: (9, {})} | custom-call | tf_op jit(solution)/shard_map/pallas_call | solution.py:382
  120.7 23.4 %all_to_all.30.parts = bf16[16,320,128]{2,1,0:T(8,128)(2,1)S(1)} all-to-all(bf16[16,320,128]{2,1,0:T(8,128)(2,1)} %shard_map.159), channel_id=1, replica_groups=mesh['sp'=32,'y'=4,'x'=4] {'y','x'}, dimensions={0} | all-to-all | bytes 2621440 | tf_op jit(solution)/shard_map/all_to_all | solution.py:365
  144.0 1.3 shard_map.160
  145.3 14.3 %all-to-all-start.4 = ((bf16[32,24,128]{2,1,0:T(8,128)(2,1)}), bf16[32,24,128]{2,1,0:T(8,128)(2,1)S(1)}, u32[]{:S(2)}, u32[]{:S(2)}) async-start(bf16[32,24,128]{2,1,0:T(8,128)(2,1)} %bitcast.37), calls=%async_computation.4 | async-start | bytes 393216 | tf_op jit(solution)/shard_map/all_to_all | solution.py:365
  159.7 0.5 shard_map.161
  160.1 18.3 %all-to-all-done.4 = bf16[32,24,128]{2,1,0:T(8,128)(2,1)S(1)} async-done(((bf16[32,24,128]{2,1,0:T(8,128)(2,1)}), bf16[32,24,128]{2,1,0:T(8,128)(2,1)S(1)}, u32[]{:S(2)}, u32[]{:S(2)}) %all-to-all-start.4) | async-done | bytes 196640 | tf_op jit(solution)/shard_map/all_to_all | solution.py:365
  178.4 1.1 shard_map.162
  179.5 9.9 %all_to_all.31.stats = f32[16,2,256]{2,1,0:T(2,128)S(1)} all-to-all(f32[16,2,256]{2,1,0:T(2,128)} %get-tuple-element.30), channel_id=1, replica_groups=mesh['sp'=32,'y'=4,'x'=4] {'y','x'}, dimensions={0} | all-to-all | bytes 65536 | tf_op jit(solution)/shard_map/all_to_all | solution.py:365
  189.4 0.8 shard_map.163
  (15 shorter events, 0.0 us)
Async XLA Ops:
  2.0 7.8 %copy-start.6 = (s32[256]{0:T(256)S(1)}, s32[256]{0:T(256)}, u32[]{:S(2)}) copy-start(s32[256]{0:T(256)} %param.17) | copy-start | bytes 3076
  2.0 31.3 %copy-start.1 = (f32[2048]{0:T(1024)S(1)}, f32[2048]{0:T(1024)}, u32[]{:S(2)}) copy-start(f32[2048]{0:T(1024)} %param.21) | copy-start | bytes 24580
  2.0 31.3 %copy-start.2 = (f32[2048]{0:T(1024)S(1)}, f32[2048]{0:T(1024)}, u32[]{:S(2)}) copy-start(f32[2048]{0:T(1024)} %param.22) | copy-start | bytes 24580
  2.0 31.3 %copy-start.3 = (f32[2048]{0:T(1024)S(1)}, f32[2048]{0:T(1024)}, u32[]{:S(2)}) copy-start(f32[2048]{0:T(1024)} %param.23) | copy-start | bytes 24580
  2.0 31.3 %copy-start.4 = (s32[256,2]{0,1:T(2,128)S(1)}, s32[256,2]{0,1:T(2,128)}, u32[]{:S(2)}) copy-start(s32[256,2]{0,1:T(2,128)} %param.18) | copy-start | bytes 6148
  2.0 22.3 %all-to-all-start = ((bf16[16,256,128]{2,1,0:T(8,128)(2,1)}), bf16[16,256,128]{2,1,0:T(8,128)(2,1)S(1)}, u32[]{:S(2)}, u32[]{:S(2)}) async-start(bf16[16,256,128]{2,1,0:T(8,128)(2,1)} %shard_map.154), calls=%async_computation | async-start | bytes 2097152 | tf_op jit(solution)/shard_map/all_to_all | solution.py:365
  24.5 8.8 %collective-permute-start = (bf16[17,16,128]{2,1,0:T(8,128)(2,1)S(1)}, bf16[17,16,128]{2,1,0:T(8,128)(2,1)S(1)}, u32[]{:S(2)}, u32[]{:S(2)}) collective-permute-start(bf16[17,16,128]{2,1,0:T(8,128)(2,1)S(1)} %pad_maximum_fusion), channel_id=1, source_target_pairs={{0,16},{16,32},{32,48},{48,64},{64,80},{80,96},{96,112},{112,128},... | collective-permute-start | bytes 208904 | tf_op jit(solution)/shard_map/ppermute | solution.py:444
  38.4 49.5 %all-to-all-start.1 = ((bf16[32,8,512]{2,1,0:T(8,128)(2,1)}), bf16[32,8,512]{2,1,0:T(8,128)(2,1)S(1)}, u32[]{:S(2)}, u32[]{:S(2)}) async-start(bf16[32,8,512]{2,1,0:T(8,128)(2,1)} %bitcast.36), calls=%async_computation.1 | async-start | bytes 524288 | tf_op jit(solution)/shard_map/all_to_all | solution.py:365
  59.3 29.8 %copy-start = (bf16[3072,128]{1,0:T(8,128)(2,1)}, bf16[3072,128]{1,0:T(8,128)(2,1)S(1)}, u32[]{:S(2)}) copy-start(bf16[3072,128]{1,0:T(8,128)(2,1)S(1)} %get-tuple-element.20.w1) | copy-start | bytes 2359300
  59.3 22.1 %collective-permute-start.1 = (bf16[3072,128]{1,0:T(8,128)(2,1)S(1)}, bf16[3072,128]{1,0:T(8,128)(2,1)}, u32[]{:S(2)}, u32[]{:S(2)}) collective-permute-start(bf16[3072,128]{1,0:T(8,128)(2,1)S(1)} %get-tuple-element.19.w0), channel_id=1, source_target_pairs={{0,1},{1,2},{2,3},{3,0},{4,5},{5,6},{6,7},{7,4},{8,9},{9,10},{10,1... | collective-permute-start | bytes 2359304 | tf_op jit(solution)/shard_map/ppermute | solution.py:369
  61.2 22.1 %collective-permute-start.4 = (bf16[3072,128]{1,0:T(8,128)(2,1)S(1)}, bf16[3072,128]{1,0:T(8,128)(2,1)}, u32[]{:S(2)}, u32[]{:S(2)}) collective-permute-start(bf16[3072,128]{1,0:T(8,128)(2,1)S(1)} %get-tuple-element.20.w1), channel_id=1, source_target_pairs={{0,3},{1,0},{2,1},{3,2},{4,7},{5,4},{6,5},{7,6},{8,11},{9,8},{10,9... | collective-permute-start | bytes 2359304 | tf_op jit(solution)/shard_map/ppermute | solution.py:369
  65.8 26.8 %collective-permute-start.7 = (bf16[96,2048]{1,0:T(8,128)(2,1)}, bf16[96,2048]{1,0:T(8,128)(2,1)S(1)}, u32[]{:S(2)}, u32[]{:S(2)}) collective-permute-start(bf16[96,2048]{1,0:T(8,128)(2,1)} %get-tuple-element.23), channel_id=1, source_target_pairs={{0,4},{4,0},{8,12},{12,8},{1,5},{5,1},{9,13},{13,9},{2,6},{6,2},{1... | collective-permute-start | bytes 1179656 | tf_op jit(solution)/shard_map/ppermute | solution.py:478
  67.7 33.2 %collective-permute-start.2 = (bf16[3072,128]{1,0:T(8,128)(2,1)S(1)}, bf16[3072,128]{1,0:T(8,128)(2,1)}, u32[]{:S(2)}, u32[]{:S(2)}) collective-permute-start(bf16[3072,128]{1,0:T(8,128)(2,1)S(1)} %get-tuple-element.20.w1), channel_id=1, source_target_pairs={{0,1},{1,2},{2,3},{3,0},{4,5},{5,6},{6,7},{7,4},{8,9},{9,10},{10,1... | collective-permute-start | bytes 2359304 | tf_op jit(solution)/shard_map/ppermute | solution.py:369
  69.7 31.3 %collective-permute-start.3 = (bf16[3072,128]{1,0:T(8,128)(2,1)S(1)}, bf16[3072,128]{1,0:T(8,128)(2,1)}, u32[]{:S(2)}, u32[]{:S(2)}) collective-permute-start(bf16[3072,128]{1,0:T(8,128)(2,1)S(1)} %get-tuple-element.19.w0), channel_id=1, source_target_pairs={{0,3},{1,0},{2,1},{3,2},{4,7},{5,4},{6,5},{7,6},{8,11},{9,8},{10,9... | collective-permute-start | bytes 2359304 | tf_op jit(solution)/shard_map/ppermute | solution.py:369
  81.4 33.7 %collective-permute-start.5 = (bf16[3072,128]{1,0:T(8,128)(2,1)}, bf16[3072,128]{1,0:T(8,128)(2,1)}, u32[]{:S(2)}, u32[]{:S(2)}) collective-permute-start(bf16[3072,128]{1,0:T(8,128)(2,1)} %collective-permute-done.1.w2), channel_id=1, source_target_pairs={{0,1},{1,2},{2,3},{3,0},{4,5},{5,6},{6,7},{7,4},{8,9},{9,10},{10,1... | collective-permute-start | bytes 2359304 | tf_op jit(solution)/shard_map/ppermute | solution.py:369
  83.3 32.7 %collective-permute-start.6 = (bf16[3072,128]{1,0:T(8,128)(2,1)}, bf16[3072,128]{1,0:T(8,128)(2,1)}, u32[]{:S(2)}, u32[]{:S(2)}) collective-permute-start(bf16[3072,128]{1,0:T(8,128)(2,1)} %collective-permute-done.4.w5), channel_id=1, source_target_pairs={{0,3},{1,0},{2,1},{3,2},{4,7},{5,4},{6,5},{7,6},{8,11},{9,8},{10,9... | collective-permute-start | bytes 2359304 | tf_op jit(solution)/shard_map/ppermute | solution.py:369
  89.1 26.9 %all-to-all-start.2 = ((bf16[4,192,512]{2,1,0:T(8,128)(2,1)}), bf16[4,192,512]{2,1,0:T(8,128)(2,1)S(1)}, u32[]{:S(2)}, u32[]{:S(2)}) async-start(bf16[4,192,512]{2,1,0:T(8,128)(2,1)} %shard_map.156), calls=%async_computation.2 | async-start | bytes 1572864 | tf_op jit(solution)/shard_map/all_to_all | solution.py:365
  92.6 5.6 %copy-start.9 = (bf16[96,2048]{1,0:T(8,128)(2,1)}, bf16[96,2048]{1,0:T(8,128)(2,1)S(1)}, u32[]{:S(2)}) copy-start(bf16[96,2048]{1,0:T(8,128)(2,1)S(1)} %collective-permute-done.7.s1) | copy-start | bytes 1179652
  92.6 5.6 %collective-permute-start.8 = (bf16[96,2048]{1,0:T(8,128)(2,1)S(1)}, bf16[96,2048]{1,0:T(8,128)(2,1)S(1)}, u32[]{:S(2)}, u32[]{:S(2)}) collective-permute-start(bf16[96,2048]{1,0:T(8,128)(2,1)S(1)} %collective-permute-done.7.s1), channel_id=1, source_target_pairs={{0,16},{16,0},{32,48},{48,32},{64,80},{80,64},{96,112},{112,96},{1... | collective-permute-start | bytes 1179656 | tf_op jit(solution)/shard_map/ppermute | solution.py:480
  144.0 15.6 %copy-start.5 = (f32[256,2]{0,1:T(2,128)S(1)}, f32[256,2]{0,1:T(2,128)}, u32[]{:S(2)}) copy-start(f32[256,2]{0,1:T(2,128)} %param.19) | copy-start | bytes 6148
  144.0 45.4 %copy-start.7 = (f32[128]{0:T(128)S(1)}, f32[128]{0:T(128)}, u32[]{:S(2)}) copy-start(f32[128]{0:T(128)} %param.30) | copy-start | bytes 1540
  144.0 45.4 %copy-start.8 = (f32[128]{0:T(128)S(1)}, f32[128]{0:T(128)}, u32[]{:S(2)}) copy-start(f32[128]{0:T(128)} %param.31) | copy-start | bytes 1540
  145.3 33.1 %all-to-all-start.4 = ((bf16[32,24,128]{2,1,0:T(8,128)(2,1)}), bf16[32,24,128]{2,1,0:T(8,128)(2,1)S(1)}, u32[]{:S(2)}, u32[]{:S(2)}) async-start(bf16[32,24,128]{2,1,0:T(8,128)(2,1)} %bitcast.37), calls=%async_computation.4 | async-start | bytes 393216 | tf_op jit(solution)/shard_map/all_to_all | solution.py:365
